TPU v7x, 128 devices: a whole 4x4x4 slice. The times are simulated.
128 devices in a mesh: ep: 64 (over z, y, x), tp: 2 (over core).
Axes of the slice: x: 4, y: 4, z: 4, core: 2. Of those that a mesh axis runs over, the one named last changes fastest.
Arguments:
- inputs: bfloat16 [1024, 2048], P('ep'), may hold values from -6 to 6
- positions: int32 [1024], P('ep'), may hold values from 1024 to 8191
- ret_state: float32 [1024, 12, 128, 128], P('ep', 'tp'), may hold values from -4 to 4
- norm_mix: bfloat16 [2048], replicated, may hold values from 0.099609375 to 1.8984375
- w_query: bfloat16 [2048, 1536], P('ep', 'tp'), may hold values from -0.375 to 0.375
- w_key: bfloat16 [2048, 1536], P('ep', 'tp'), may hold values from -0.375 to 0.375
- w_value: bfloat16 [2048, 1536], P('ep', 'tp'), may hold values from -0.375 to 0.375
- w_gate_in: bfloat16 [2048, 1536], P('ep', 'tp'), may hold values from -0.375 to 0.375
- head_gain: bfloat16 [1536], P('tp'), may hold values from 0.099609375 to 1.8984375
- w_out: bfloat16 [1536, 2048], P('tp', 'ep'), may hold values from -0.15625 to 0.15625
- norm_ffn: bfloat16 [2048], replicated, may hold values from 0.099609375 to 1.8984375
- route_ids: int32 [1024, 4], P('ep'), may hold values from 0 to 63, all different within a row; in each aligned block of 16 rows (0 to 15, 16 to 31, ...) at most 2 rows name the same one
- route_weight: bfloat16 [1024, 4], P('ep'), may hold values from 0.19921875 to 1
- exp_gate: bfloat16 [64, 2048, 1024], P('ep', None, 'tp'), may hold values from -0.125 to 0.125
- exp_up: bfloat16 [64, 2048, 1024], P('ep', None, 'tp'), may hold values from -0.125 to 0.125
- exp_down: bfloat16 [64, 1024, 2048], P('ep', 'tp'), may hold values from -0.1875 to 0.1875
- dense_gate: bfloat16 [2048, 4096], P(None, ('ep', 'tp')), may hold values from -0.125 to 0.125
- dense_up: bfloat16 [2048, 4096], P(None, ('ep', 'tp')), may hold values from -0.125 to 0.125
- dense_down: bfloat16 [4096, 2048], P(('ep', 'tp')), may hold values from -0.375 to 0.375
- branch_gate: bfloat16 [2048], replicated, may hold values from -0.125 to 0.125
Outputs:
- layer_out: bfloat16 [1024, 2048], P('ep')
- new_state: float32 [1024, 12, 128, 128], P('ep', 'tp')
Inputs may be any that keep to these rules, and one draw needn't show every extreme that they name: `route_ids`: each row names 4 different experts. Among the rows of one index of ep no expert is named more than 2 times, a bound that some block reaches.
All inputs are finite; a program needn't handle non-finite values.
Results may differ from a plain program's by a relative error of at most 0.015.
Values may be sent and summed in bfloat16 or wider, within the bound.
No kernel may reach another device: no remote copies, remote signals or barrier semaphores. Data moves between devices by JAX's collectives and lax.ppermute only.
A program may use at most 128 MiB of HBM per device.

v0:
```python
import jax
import jax.numpy as jnp
from jax import lax
from jax.experimental import pallas as pl
from jax.experimental.pallas import tpu as pltpu
from jax.sharding import Mesh, PartitionSpec as P


D = 2048
HEADS = 12
EPS = 1e-06
F32 = jnp.float32
BF16 = jnp.bfloat16

RIGHT = [(i, (i + 1) % 4) for i in range(4)]
LEFT = [(i, (i - 1) % 4) for i in range(4)]
ACROSS = [(i, (i + 2) % 4) for i in range(4)]
SWAP = [(0, 1), (1, 0)]
PLANE = ("z", "y")
NT = (((1,), (1,)), ((), ()))


def ring_gather(own):
    return (
        own,
        lax.ppermute(own, "x", RIGHT),
        lax.ppermute(own, "x", ACROSS),
        lax.ppermute(own, "x", LEFT),
    )


OFFSETS = (0, 3, 2, 1)


def whole(shape):
    return pl.BlockSpec(shape, lambda *s: (0,) * len(shape))


SMEM = pl.BlockSpec(memory_space=pltpu.SMEM)


def prepare_body(x_ref, gain, ids, shares, wq, wk, wv, wg, sent, w4, routes):
    w4[0] = wq[...]
    w4[1] = wk[...]
    w4[2] = wv[...]
    w4[3] = wg[...]
    routes[...] = jnp.zeros((16, 128), F32)
    routes[:, 0:4] = ids[...].astype(F32)
    routes[:, 4:8] = shares[...].astype(F32)
    route = routes[...].astype(BF16)
    x = x_ref[...]
    v = x.astype(F32)
    scaled = v * lax.rsqrt(jnp.mean(v * v, axis=-1, keepdims=True) + EPS)
    normed = (scaled * gain[...].astype(F32).reshape(1, D)).astype(BF16)
    for j in range(16):
        at = slice(j * 128, (j + 1) * 128)
        sent[j, 0:16, :] = normed[:, at]
        sent[j, 16:32, :] = x[:, at]
        sent[j, 32:48, :] = route


def prepare(x, gain, ids, shares, ws):
    return pl.pallas_call(
        prepare_body,
        out_shape=[
            jax.ShapeDtypeStruct((16, 48, 128), BF16),
            jax.ShapeDtypeStruct((4, 32, 768), BF16),
        ],
        scratch_shapes=[pltpu.VMEM((16, 128), F32)],
        name="prepare",
    )(x, gain, ids, shares, *ws)


def project_body(xi_ref, x_ref, c0, c1, c2, c3, out_ref, wide):
    xi = xi_ref[0]
    for offset, chunk in zip(OFFSETS, (c0, c1, c2, c3)):
        at = pl.multiple_of(((xi + offset) % 4) * 32, 32)
        wide[pl.ds(at, 32), :] = chunk[0]
    x = x_ref[:, 0:16, :].reshape(256, 128)
    out = jnp.dot(x, wide[...], preferred_element_type=F32).astype(BF16)
    out_ref[...] = out.reshape(16, 16, 768)


def project(xi, got, chunks):
    one = pl.BlockSpec((1, 32, 768), lambda p: (p, 0, 0))
    return pl.pallas_call(
        project_body,
        grid=(4,),
        in_specs=[SMEM, whole((16, 48, 128)), one, one, one, one],
        out_specs=pl.BlockSpec((16, 16, 768), lambda p: (0, 0, p)),
        out_shape=jax.ShapeDtypeStruct((16, 16, 3072), BF16),
        scratch_shapes=[pltpu.VMEM((128, 768), BF16)],
        name="project",
    )(xi, got, *chunks)


PER_STEP = 2
STEPS = 16 // PER_STEP


def retain_body(
    gamma_ref, parts_ref, cosine, sine, gain, state_ref,
    new_state, sent, parts, buf, queries_keys, values, gates, readouts, sems,
):
    fetch_parts = pltpu.make_async_copy(parts_ref, parts, sems.at[2 * STEPS])
    fetch_parts.start()

    def rows(i):
        return pl.ds(i * PER_STEP, PER_STEP)

    def fetch(i):
        return pltpu.make_async_copy(state_ref.at[rows(i)], buf.at[rows(i)], sems.at[i])

    def store(i):
        return pltpu.make_async_copy(buf.at[rows(i)], new_state.at[rows(i)], sems.at[STEPS + i])

    for i in range(STEPS):
        fetch(i).start()
    fetch_parts.wait()
    cos_v, sin_v = cosine[...], sine[...]
    for h in range(6):
        def total(which):
            at = which * 768 + h * 128
            acc = parts[0, :, at : at + 128].astype(F32)
            for s in range(1, 16):
                acc = acc + parts[s, :, at : at + 128].astype(F32)
            return acc.astype(BF16).astype(F32)

        q, k, v, g = (total(i) for i in range(4))
        queries_keys[:, h, :] = q * cos_v + pltpu.roll(q, 64, 1) * sin_v
        queries_keys[:, 8 + h, :] = (k * cos_v + pltpu.roll(k, 64, 1) * sin_v) * (128.0 ** -0.5)
        values[:, h, :] = v
        gates[:, h * 128 : (h + 1) * 128] = g * jax.nn.sigmoid(g)

    def some(i, carry):
        fetch(i).wait()
        for j in range(PER_STEP):
            t = i * PER_STEP + j
            cols = jnp.transpose(queries_keys[t])
            for h in range(6):
                q_col = cols[:, h : h + 1]
                k_col = cols[:, 8 + h : 9 + h]
                v_row = values[t, h : h + 1, :]
                fresh = gamma_ref[h] * buf[t, h] + k_col * v_row
                buf[t, h] = fresh
                readouts[t, h : h + 1, :] = jnp.sum(q_col * fresh, axis=0, keepdims=True)
        store(i).start()
        return carry

    lax.fori_loop(0, STEPS, some, 0)
    for h in range(6):
        at = slice(h * 128, (h + 1) * 128)
        r = readouts[:, h, :]
        centred = r - jnp.mean(r, axis=-1, keepdims=True)
        unit = centred * lax.rsqrt(jnp.mean(centred * centred, axis=-1, keepdims=True) + EPS)
        kept = (unit * gain[:, at].astype(F32) * gates[:, at]).astype(BF16)
        for s in range(16):
            sent[s, :, at] = kept
    for i in range(STEPS):
        store(i).wait()


def retain(gamma, parts, cosine, sine, gain, state):
    anywhere = pl.BlockSpec(memory_space=pl.ANY)
    vmem = pl.BlockSpec(memory_space=pltpu.VMEM)
    return pl.pallas_call(
        retain_body,
        in_specs=[SMEM, anywhere, vmem, vmem, vmem, anywhere],
        out_specs=[anywhere, vmem],
        out_shape=[
            jax.ShapeDtypeStruct((16, 6, 128, 128), F32),
            jax.ShapeDtypeStruct((16, 16, 768), BF16),
        ],
        scratch_shapes=[
            pltpu.VMEM((16, 16, 3072), BF16),
            pltpu.VMEM((16, 6, 128, 128), F32),
            pltpu.VMEM((16, 16, 128), F32),
            pltpu.VMEM((16, 8, 128), F32),
            pltpu.VMEM((16, 768), F32),
            pltpu.VMEM((16, 8, 128), F32),
            pltpu.SemaphoreType.DMA((2 * STEPS + 1,)),
        ],
        name="retain",
    )(gamma, parts, cosine, sine, gain, state)


def mix_body(xi_ref, kept, c0, c1, c2, c3, out_ref, wide):
    xi = xi_ref[0]
    for offset, chunk in zip(OFFSETS, (c0, c1, c2, c3)):
        at = pl.multiple_of(((xi + offset) % 4) * 32, 32)
        wide[pl.ds(at, 32), :] = chunk[...]
    rows = kept[...].reshape(256, 768)
    out_ref[...] = lax.dot_general(rows, wide[...], NT, preferred_element_type=F32).astype(BF16)


def mix(xi, kept, chunks):
    vmem = pl.BlockSpec(memory_space=pltpu.VMEM)
    return pl.pallas_call(
        mix_body,
        in_specs=[SMEM] + [vmem] * 5,
        out_shape=jax.ShapeDtypeStruct((256, 128), BF16),
        scratch_shapes=[pltpu.VMEM((128, 768), BF16)],
        name="mix",
    )(xi, kept, *chunks)


def spread_body(zy_ref, res, gain, branch, pick, plane, s0, s1, s2, s3, opening, own):
    total = jnp.zeros((256, 128), F32)
    for s in range(16):
        r = res[s].astype(F32)
        total = total + r * r
    scale = lax.rsqrt(jnp.sum(total, axis=-1, keepdims=True) / D + EPS)
    first = pl.multiple_of(zy_ref[0] * 16, 16)
    dots = jnp.zeros((256, 128), F32)
    for s in range(16):
        at = slice(s * 128, (s + 1) * 128)
        n = (res[s].astype(F32) * scale * gain[s : s + 1, :].astype(F32)).astype(BF16)
        plane[:, at] = n
        dots = dots + n.astype(F32) * branch[s : s + 1, :].astype(F32)
        rows = jnp.dot(pick[...], n, preferred_element_type=F32).astype(BF16)
        for k, out in enumerate((s0, s1, s2, s3)):
            out[:, at] = rows[k * 32 : (k + 1) * 32]
        own[:, at] = res[s, pl.ds(first, 16), :]
    opening[...] = jax.nn.sigmoid(jnp.sum(dots, axis=-1, keepdims=True))


def spread(zy, res, gain, branch, pick):
    vmem = pl.BlockSpec(memory_space=pltpu.VMEM)
    rows = jax.ShapeDtypeStruct((32, D), BF16)
    return pl.pallas_call(
        spread_body,
        in_specs=[SMEM] + [vmem] * 4,
        out_shape=[
            jax.ShapeDtypeStruct((256, D), BF16), rows, rows, rows, rows,
            jax.ShapeDtypeStruct((256, 1), F32),
            jax.ShapeDtypeStruct((16, D), BF16),
        ],
        name="spread",
    )(zy, res, gain, branch, pick)


def dense_body(plane, c0, c1, c2, c3, hidden, gate, up):
    for r, chunk in enumerate((c0, c1, c2, c3)):
        at = slice(r * 32, (r + 1) * 32)
        gate[at, :] = chunk[0:32, :]
        up[at, :] = chunk[32:64, :]
    x = plane[...]
    g = lax.dot_general(x, gate[...], NT, preferred_element_type=F32)
    u = lax.dot_general(x, up[...], NT, preferred_element_type=F32)
    hidden[...] = (g * jax.nn.sigmoid(g) * u).astype(BF16)


def dense_first(plane, chunks):
    return pl.pallas_call(
        dense_body,
        out_shape=jax.ShapeDtypeStruct((256, 128), BF16),
        scratch_shapes=[pltpu.VMEM((128, D), BF16), pltpu.VMEM((128, D), BF16)],
        name="dense_first",
    )(plane, *chunks)


CUT = 4


def expert_body(
    a0, a1, a2, a3, gate_ref, up_ref, down_ref, r0, r1, r2, r3, rows, gate, up, down, sems
):
    def fetch(ref, to, i, sem):
        n = to.shape[0] // CUT
        at = pl.ds(i * n, n)
        return pltpu.make_async_copy(ref.at[0, at], to.at[at], sems.at[sem])

    first = [(fetch(gate_ref, gate, i, i), fetch(up_ref, up, i, CUT + i)) for i in range(CUT)]
    second = [fetch(down_ref, down, i, 2 * CUT + i) for i in range(CUT)]
    for g, u in first:
        g.start()
        u.start()
    for d in second:
        d.start()
    for k, a in enumerate((a0, a1, a2, a3)):
        rows[k * 32 : (k + 1) * 32, :] = a[...]
    g_sum = u_sum = None
    n = D // CUT
    for i, (g, u) in enumerate(first):
        at = slice(i * n, (i + 1) * n)
        g.wait()
        g_part = jnp.dot(rows[:, at], gate[at, :], preferred_element_type=F32)
        u.wait()
        u_part = jnp.dot(rows[:, at], up[at, :], preferred_element_type=F32)
        g_sum = g_part if g_sum is None else g_sum + g_part
        u_sum = u_part if u_sum is None else u_sum + u_part
    h = (g_sum * jax.nn.sigmoid(g_sum) * u_sum).astype(BF16)
    for d in second:
        d.wait()
    for j in range(4):
        at = slice(j * 512, (j + 1) * 512)
        out = jnp.dot(h, down[:, at], preferred_element_type=F32).astype(BF16)
        for k, r in enumerate((r0, r1, r2, r3)):
            r[:, at] = out[k * 32 : (k + 1) * 32, :]


def experts(arrived, gate, up, down):
    rows = jax.ShapeDtypeStruct((32, D), BF16)
    anywhere = pl.BlockSpec(memory_space=pl.ANY)
    vmem = pl.BlockSpec(memory_space=pltpu.VMEM)
    return pl.pallas_call(
        expert_body,
        in_specs=[vmem] * 4 + [anywhere] * 3,
        out_shape=[rows] * 4,
        scratch_shapes=[
            pltpu.VMEM((128, D), BF16),
            pltpu.VMEM((D, 512), BF16),
            pltpu.VMEM((D, 512), BF16),
            pltpu.VMEM((512, D), BF16),
            pltpu.SemaphoreType.DMA((3 * CUT,)),
        ],
        name="experts",
    )(*arrived, gate, up, down)


def combine_body(hidden, c0, c1, c2, c3, opening, weigh, b0, b1, b2, b3, out, down, back):
    for r, chunk in enumerate((c0, c1, c2, c3)):
        down[r * 32 : (r + 1) * 32, :] = chunk[64:96, :]
    for k, b in enumerate((b0, b1, b2, b3)):
        back[k * 32 : (k + 1) * 32, :] = b[...]
        back[128 + k * 32 : 128 + (k + 1) * 32, :] = b[...]
    opened = opening[...]
    for j in range(4):
        at = slice(j * 512, (j + 1) * 512)
        term = jnp.dot(hidden[...], down[:, at], preferred_element_type=F32) * opened
        term = term + jnp.dot(weigh[...], back[:, at], preferred_element_type=F32)
        out[:, :, at] = term.astype(BF16).reshape(16, 16, 512)


def combine(hidden, chunks, opening, weigh, back):
    return pl.pallas_call(
        combine_body,
        out_shape=jax.ShapeDtypeStruct((16, 16, D), BF16),
        scratch_shapes=[pltpu.VMEM((128, D), BF16), pltpu.VMEM((256, D), BF16)],
        name="combine",
    )(hidden, *chunks, opening, weigh, *back)


def plane_exchange(array):
    return lax.all_to_all(array, PLANE, split_axis=0, concat_axis=0, tiled=True)


def routing(routed, x_at, zy_at):
    ids = routed[:, :4]
    weights = routed[:, 4:8]
    share = weights / jnp.sum(weights, axis=-1, keepdims=True)
    wanted = (zy_at * 4 + (x_at + jnp.arange(4)) % 4).astype(F32)
    hits = (ids[:, :, None] == wanted[None, None, :]).astype(F32)
    match = jnp.sum(hits, axis=1)
    share_of = jnp.sum(hits * share[:, :, None], axis=1)
    t = jnp.arange(256)
    before = ((t[:, None] // 16 == t[None, :] // 16) & (t[None, :] < t[:, None])).astype(BF16)
    rank = jnp.dot(before, match.astype(BF16), preferred_element_type=F32)
    slot = jnp.arange(32)
    place = (
        (t[:, None, None] // 16 == slot[None, None, :] // 2)
        & (rank[:, :, None] == (slot % 2).astype(F32)[None, None, :])
        & (match[:, :, None] > 0)
    )
    pick = place.astype(BF16).reshape(256, 128).T
    weigh = jnp.where(place, share_of[:, :, None], 0.0).reshape(256, 128)
    high = weigh.astype(BF16)
    low = (weigh - high.astype(F32)).astype(BF16)
    return pick, jnp.concatenate([high, low], axis=1)


def on_device(
    inputs, positions, ret_state, norm_mix, w_query, w_key, w_value, w_gate_in, head_gain, w_out,
    norm_ffn, route_ids, route_weight, exp_gate, exp_up, exp_down, dense_gate, dense_up, dense_down,
    branch_gate,
):
    x_at = lax.axis_index("x")
    zy_at = lax.axis_index(PLANE)
    xi = x_at.astype(jnp.int32).reshape(1)
    zy = zy_at.astype(jnp.int32).reshape(1)

    sent, w4 = prepare(
        inputs, norm_mix, route_ids, route_weight, (w_query, w_key, w_value, w_gate_in)
    )
    chunks = ring_gather(w4)
    got = plane_exchange(sent)
    in_cols = got[:, 16:32].reshape(256, 128)
    routed = got[:, 32:48, :8].reshape(256, 8).astype(F32)

    partial = project(xi, got, chunks)
    parts = plane_exchange(partial)

    out_chunks = ring_gather(w_out.T)
    dense = jnp.concatenate([dense_gate.T, dense_up.T, dense_down], axis=0)
    dense_chunks = ring_gather(dense)
    pick, weigh = routing(routed, x_at, zy_at)
    parts, out_chunks, dense_chunks, pick, weigh = lax.optimization_barrier(
        (parts, out_chunks, dense_chunks, pick, weigh)
    )

    frequency = 10000.0 ** (-jnp.arange(64, dtype=F32) * 2.0 / 128)
    angles = positions.astype(F32)[:, None] * frequency[None, :]
    cos_v, sin_v = jnp.cos(angles), jnp.sin(angles)
    cosine = jnp.concatenate([cos_v, cos_v], axis=1)
    sine = jnp.concatenate([-sin_v, sin_v], axis=1)
    spreading = jnp.arange(HEADS, dtype=F32) * (5.0 / (HEADS - 1))
    gamma = lax.dynamic_slice_in_dim(
        jnp.exp(jnp.log1p(-(2.0 ** (-5.0 - spreading)))), lax.axis_index("tp") * 6, 6
    )
    new_state, kept = retain(gamma, parts, cosine, sine, head_gain.reshape(1, 768), ret_state)
    kept = plane_exchange(kept)
    mixed = mix(xi, kept, out_chunks)
    other = lax.ppermute(mixed, "tp", SWAP)
    mixer_out = (mixed.astype(F32) + other.astype(F32)).astype(BF16)
    res_cols = (in_cols.astype(F32) + mixer_out.astype(F32)).astype(BF16)
    res = plane_exchange(jnp.broadcast_to(res_cols, (16, 256, 128)))

    plane, s0, s1, s2, s3, opening, own_res = spread(
        zy, res, norm_ffn.reshape(16, 128), branch_gate.reshape(16, 128), pick
    )
    arrived = (
        s0,
        lax.ppermute(s1, "x", RIGHT),
        lax.ppermute(s2, "x", ACROSS),
        lax.ppermute(s3, "x", LEFT),
    )
    hidden = dense_first(plane, dense_chunks)
    r0, r1, r2, r3 = experts(arrived, exp_gate, exp_up, exp_down)
    back = (
        r0,
        lax.ppermute(r1, "x", LEFT),
        lax.ppermute(r2, "x", ACROSS),
        lax.ppermute(r3, "x", RIGHT),
    )
    branch = combine(hidden, dense_chunks, opening, weigh, back)
    terms = plane_exchange(branch)
    summed = jnp.sum(terms.astype(F32), axis=0).astype(BF16)
    total = summed.astype(F32) + lax.ppermute(summed, "tp", SWAP).astype(F32)
    layer_out = (own_res.astype(F32) + total).astype(BF16)
    return (layer_out, new_state)


EP = ("z", "y", "x")


def solution(mesh):
    inner = Mesh(mesh.devices.reshape(4, 4, 4, 2), ("z", "y", "x", "tp"))
    in_specs = (
        P(EP, None),
        P(EP),
        P(EP, "tp", None, None),
        P(),
        P(EP, "tp"),
        P(EP, "tp"),
        P(EP, "tp"),
        P(EP, "tp"),
        P("tp"),
        P("tp", EP),
        P(),
        P(EP, None),
        P(EP, None),
        P(EP, None, "tp"),
        P(EP, None, "tp"),
        P(EP, "tp", None),
        P(None, (*EP, "tp")),
        P(None, (*EP, "tp")),
        P((*EP, "tp"), None),
        P(),
    )
    out_specs = (P(EP, None), P(EP, "tp", None, None))
    return jax.shard_map(
        on_device, mesh=inner, in_specs=in_specs, out_specs=out_specs, check_vma=False
    )
```

profile of v0, /device:TPU:1, one launch (start us, length us, event | category | flops | bytes accessed | tf_op | source)
XLA Modules:
  0.0 173.4 jit_solution(1214135358673409953)
XLA Ops:
  0.6 3.4 %collective-permute-start.5 = (bf16[32,768]{1,0:T(8,128)(2,1)}, bf16[32,768]{1,0:T(8,128)(2,1)}, u32[]{:S(2)}, u32[]{:S(2)}) collective-permute-start(bf16[32,768]{1,0:T(8,128)(2,1)} %bitcast.25), channel_id=1, source_target_pairs={{0,6},{2,0},{4,2},{6,4},{1,7},{3,1},{5,3},{7,5},{8,14},{10,8},{12,... | collective-permute-start | bytes 147464 | tf_op jit(solution)/shard_map/ppermute | solution.py:28
  4.0 0.5 collective-permute-start.4
  4.5 1.3 copy.43.shares
  5.9 1.4 copy.42.ids
  7.2 1.7 prepare.1
  9.0 0.7 collective-permute-start.2
  9.7 1.8 %collective-permute-start.1 = (bf16[4,32,768]{2,1,0:T(8,128)(2,1)}, bf16[4,32,768]{2,1,0:T(8,128)(2,1)S(1)}, u32[]{:S(2)}, u32[]{:S(2)}) collective-permute-start(bf16[4,32,768]{2,1,0:T(8,128)(2,1)} %get-tuple-element.29.c0), channel_id=1, source_target_pairs={{0,4},{2,6},{4,0},{6,2},{1,5},{3,7},{5,1},{7,3},{8,12},{10,14},{12... | collective-permute-start | bytes 589832 | tf_op jit(solution)/shard_map/ppermute | solution.py:27
  11.4 0.9 collective-permute-start
  12.3 7.8 %all-to-all-start = ((bf16[16,48,128]{2,1,0:T(8,128)(2,1)}), bf16[16,48,128]{2,1,0:T(8,128)(2,1)S(1)}, u32[]{:S(2)}, u32[]{:S(2)}) async-start(bf16[16,48,128]{2,1,0:T(8,128)(2,1)} %get-tuple-element.28), calls=%async_computation | async-start | bytes 393216 | tf_op jit(solution)/shard_map/all_to_all | solution.py:345
  20.1 0.7 convert_element_type.87
  20.9 1.3 reshape.259.gain
  22.2 0.7 copy.46
  23.0 0.6 dynamic_slice.3.gamma_ref
  23.6 0.1 fusion.8
  23.7 0.7 pad_maximum_fusion.2
  24.4 1.1 pad_maximum_fusion.c0
  25.5 1.8 %all-to-all-done.x_ref = bf16[16,48,128]{2,1,0:T(8,128)(2,1)S(1)} async-done(((bf16[16,48,128]{2,1,0:T(8,128)(2,1)}), bf16[16,48,128]{2,1,0:T(8,128)(2,1)S(1)}, u32[]{:S(2)}, u32[]{:S(2)}) %all-to-all-start) | async-done | bytes 196640 | tf_op jit(solution)/shard_map/all_to_all | solution.py:345
  27.3 0.2 fusion.14
  27.6 1.8 %collective-permute-start.8 = (bf16[96,2048]{1,0:T(8,128)(2,1)S(1)}, bf16[96,2048]{1,0:T(8,128)(2,1)S(1)}, u32[]{:S(2)}, u32[]{:S(2)}) collective-permute-start(bf16[96,2048]{1,0:T(8,128)(2,1)S(1)} %pad_maximum_fusion.c0), channel_id=1, source_target_pairs={{0,6},{2,0},{4,2},{6,4},{1,7},{3,1},{5,3},{7,5},{8,14},{10,8},{12,... | collective-permute-start | bytes 1179656 | tf_op jit(solution)/shard_map/ppermute | solution.py:28
  29.4 0.2 collective-permute-start.7
  29.6 0.6 collective-permute-start.6
  30.3 4.0 %project.1 = bf16[16,16,3072]{2,1,0:T(8,128)(2,1)} custom-call(s32[1]{0:T(128)} %bitcast.2.xi_ref, bf16[16,48,128]{2,1,0:T(8,128)(2,1)} %copy-done.6, bf16[4,32,768]{2,1,0:T(8,128)(2,1)} %get-tuple-element.29.c0, bf16[4,32,768]{2,1,0:T(8,128)(2,1)} %copy-done.9, bf16[4,32,768]{2,1,0:T(8,128)(2,1)} %copy-done.8, bf16[4,32,768]{2,1,0:T(8,128)(2,1)} %copy-done.7), custom_call_target="tpu_custom_call" | custom-call | tf_op jit(solution)/shard_map/project/pallas_call | solution.py:86
  34.3 4.9 %all-to-all-start.1 = ((bf16[16,16,3072]{2,1,0:T(8,128)(2,1)}), bf16[16,16,3072]{2,1,0:T(8,128)(2,1)S(1)}, u32[]{:S(2)}, u32[]{:S(2)}) async-start(bf16[16,16,3072]{2,1,0:T(8,128)(2,1)} %project.1), calls=%async_computation.1 | async-start | bytes 3145728 | tf_op jit(solution)/shard_map/all_to_all | solution.py:345
  39.5 0.7 copy.47
  40.2 0.2 fusion.1
  40.7 0.8 select_convert_fusion
  41.6 1.9 %collective-permute-start.3 = (bf16[32,768]{1,0:T(8,128)(2,1)}, bf16[32,768]{1,0:T(8,128)(2,1)S(1)}, u32[]{:S(2)}, u32[]{:S(2)}) collective-permute-start(bf16[32,768]{1,0:T(8,128)(2,1)} %bitcast.27), channel_id=1, source_target_pairs={{0,2},{2,4},{4,6},{6,0},{1,3},{3,5},{5,7},{7,1},{8,10},{10,12},{12... | collective-permute-start | bytes 147464 | tf_op jit(solution)/shard_map/ppermute | solution.py:26
  43.5 0.7 pad_maximum_fusion.1.weigh
  44.1 7.1 %collective-permute-done.3.c1 = bf16[32,768]{1,0:T(8,128)(2,1)S(1)} collective-permute-done((bf16[32,768]{1,0:T(8,128)(2,1)}, bf16[32,768]{1,0:T(8,128)(2,1)S(1)}, u32[]{:S(2)}, u32[]{:S(2)}) %collective-permute-start.3) | collective-permute-done | bytes 49184 | tf_op jit(solution)/shard_map/ppermute | solution.py:26
  51.3 7.5 %all-to-all-done.1.parts_ref = bf16[16,16,3072]{2,1,0:T(8,128)(2,1)S(1)} async-done(((bf16[16,16,3072]{2,1,0:T(8,128)(2,1)}), bf16[16,16,3072]{2,1,0:T(8,128)(2,1)S(1)}, u32[]{:S(2)}, u32[]{:S(2)}) %all-to-all-start.1) | async-done | bytes 1572896 | tf_op jit(solution)/shard_map/all_to_all | solution.py:345
  58.8 1.2 copy-done
  60.0 9.0 %retain.1 = (f32[16,6,128,128]{3,2,1,0:T(8,128)}, bf16[16,16,768]{2,1,0:T(8,128)(2,1)}) custom-call(f32[6]{0:T(128)} %dynamic_slice.3.gamma_ref, bf16[16,16,3072]{2,1,0:T(8,128)(2,1)} %copy-done, f32[16,128]{1,0:T(8,128)} %get-tuple-element.64.cosine, f32[16,128]{1,0:T(8,128)} %get-tuple-element.65.sine, bf16[1,768]{1,0:T(2,128)(2,1)} %reshape.259.gain, ...), custom_call_target="tpu_custom_call" | custom-call | tf_op jit(solution)/shard_map/retain/pallas_call | solution.py:166
  69.0 13.8 %all_to_all.25.kept = bf16[16,16,768]{2,1,0:T(8,128)(2,1)} all-to-all(bf16[16,16,768]{2,1,0:T(8,128)(2,1)} %get-tuple-element.31), channel_id=1, replica_groups=mesh['z'=4,'y'=4,'x'=4,'tp'=2] {'z','y'}, dimensions={0} | all-to-all | bytes 786432 | tf_op jit(solution)/shard_map/all_to_all | solution.py:345
  82.8 2.0 %mix.1 = bf16[256,128]{1,0:T(8,128)(2,1)} custom-call(s32[1]{0:T(128)} %bitcast.2.xi_ref, bf16[16,16,768]{2,1,0:T(8,128)(2,1)} %all_to_all.25.kept, bf16[32,768]{1,0:T(8,128)(2,1)} %bitcast.28, bf16[32,768]{1,0:T(8,128)(2,1)} %copy-done.17, bf16[32,768]{1,0:T(8,128)(2,1)} %collective-permute-done.4.c2, bf16[32,768]{1,0:T(8,128)(2,1)} %collective-permute-done.5.c3), custom_call_target="tpu_custom_call" | custom-call | tf_op jit(solution)/shard_map/mix/pallas_call | solution.py:198
  84.8 5.2 %collective-permute-start.9 = (bf16[256,128]{1,0:T(8,128)(2,1)}, bf16[256,128]{1,0:T(8,128)(2,1)S(1)}, u32[]{:S(2)}, u32[]{:S(2)}) collective-permute-start(bf16[256,128]{1,0:T(8,128)(2,1)} %mix.1), channel_id=1, source_target_pairs={{0,1},{1,0},{2,3},{3,2},{4,5},{5,4},{6,7},{7,6},{8,9},{9,8},{10,11... | collective-permute-start | bytes 196616 | tf_op jit(solution)/shard_map/ppermute | solution.py:413
  90.0 1.1 collective-permute-done.9
  91.1 0.9 fusion.3
  92.0 1.2 broadcast_in_dim.15
  93.2 3.7 %all-to-all-start.3 = ((bf16[16,256,128]{2,1,0:T(8,128)(2,1)}), bf16[16,256,128]{2,1,0:T(8,128)(2,1)S(1)}, u32[]{:S(2)}, u32[]{:S(2)}) async-start(bf16[16,256,128]{2,1,0:T(8,128)(2,1)} %broadcast_in_dim.15), calls=%async_computation.3 | async-start | bytes 2097152 | tf_op jit(solution)/shard_map/all_to_all | solution.py:345
  96.8 0.7 copy.50.pick
  97.6 16.2 %all-to-all-done.3.res = bf16[16,256,128]{2,1,0:T(8,128)(2,1)S(1)} async-done(((bf16[16,256,128]{2,1,0:T(8,128)(2,1)}), bf16[16,256,128]{2,1,0:T(8,128)(2,1)S(1)}, u32[]{:S(2)}, u32[]{:S(2)}) %all-to-all-start.3) | async-done | bytes 1048608 | tf_op jit(solution)/shard_map/all_to_all | solution.py:345
  113.8 1.0 copy-done.1
  114.8 3.2 %spread.1 = (bf16[256,2048]{1,0:T(8,128)(2,1)}, bf16[32,2048]{1,0:T(8,128)(2,1)}, bf16[32,2048]{1,0:T(8,128)(2,1)}, bf16[32,2048]{1,0:T(8,128)(2,1)}, bf16[32,20...) custom-call(s32[1]{0:T(128)} %bitcast.zy_ref, bf16[16,256,128]{2,1,0:T(8,128)(2,1)} %copy-done.1, ...), custom_call_target="tpu_custom_call" | custom-call | tf_op jit(solution)/shard_map/spread/pallas_call | solution.py:230
  118.0 1.8 %collective-permute-start.10 = (bf16[32,2048]{1,0:T(8,128)(2,1)}, bf16[32,2048]{1,0:T(8,128)(2,1)S(1)}, u32[]{:S(2)}, u32[]{:S(2)}) collective-permute-start(bf16[32,2048]{1,0:T(8,128)(2,1)} %get-tuple-element.46), channel_id=1, source_target_pairs={{0,2},{2,4},{4,6},{6,0},{1,3},{3,5},{5,7},{7,1},{8,10},{10,12},{12... | collective-permute-start | bytes 393224 | tf_op jit(solution)/shard_map/ppermute | solution.py:423
  119.8 1.4 collective-permute-start.11
  121.2 1.7 collective-permute-start.12
  122.9 0.4 collective-permute-done.10.a1
  123.3 2.9 %collective-permute-done.11.a2 = bf16[32,2048]{1,0:T(8,128)(2,1)S(1)} collective-permute-done((bf16[32,2048]{1,0:T(8,128)(2,1)}, bf16[32,2048]{1,0:T(8,128)(2,1)S(1)}, u32[]{:S(2)}, u32[]{:S(2)}) %collective-permute-start.11) | collective-permute-done | bytes 131104 | tf_op jit(solution)/shard_map/ppermute | solution.py:424
  126.1 0.4 collective-permute-done.12.a3
  126.6 0.2 copy-done.14
  126.8 0.4 copy-done.15
  127.2 5.2 %experts.1 = (bf16[32,2048]{1,0:T(8,128)(2,1)}, bf16[32,2048]{1,0:T(8,128)(2,1)}, bf16[32,2048]{1,0:T(8,128)(2,1)}, bf16[32,2048]{1,0:T(8,128)(2,1)}) custom-call(bf16[32,2048]{1,0:T(8,128)(2,1)} %get-tuple-element.45.a0, bf16[32,2048]{1,0:T(8,128)(2,1)} %copy-done.13, bf16[32,2048]{1,0:T(8,128)(2,1)} %copy-done.14, bf16[32,2048]{1,0:T(8,128)(2,1)} %copy-done.15, ...), custom_call_target="tpu_custom_call" | custom-call | tf_op jit(solution)/shard_map/experts/pallas_call | solution.py:306
  132.4 3.4 %collective-permute-start.13 = (bf16[32,2048]{1,0:T(8,128)(2,1)}, bf16[32,2048]{1,0:T(8,128)(2,1)S(1)}, u32[]{:S(2)}, u32[]{:S(2)}) collective-permute-start(bf16[32,2048]{1,0:T(8,128)(2,1)} %get-tuple-element.50), channel_id=1, source_target_pairs={{0,6},{2,0},{4,2},{6,4},{1,7},{3,1},{5,3},{7,5},{8,14},{10,8},{12,... | collective-permute-start | bytes 393224 | tf_op jit(solution)/shard_map/ppermute | solution.py:431
  135.8 0.7 collective-permute-start.15
  136.5 3.0 %dense_first.1.hidden = bf16[256,128]{1,0:T(8,128)(2,1)} custom-call(bf16[256,2048]{1,0:T(8,128)(2,1)} %get-tuple-element.38.plane, bf16[96,2048]{1,0:T(8,128)(2,1)} %copy-done.2, bf16[96,2048]{1,0:T(8,128)(2,1)} %copy-done.5, bf16[96,2048]{1,0:T(8,128)(2,1)} %copy-done.4, bf16[96,2048]{1,0:T(8,128)(2,1)} %copy-done.3), custom_call_target="tpu_custom_call" | custom-call | tf_op jit(solution)/shard_map/dense_first/pallas_call | solution.py:254
  139.5 1.9 %collective-permute-done.14.b2 = bf16[32,2048]{1,0:T(8,128)(2,1)S(1)} collective-permute-done((bf16[32,2048]{1,0:T(8,128)(2,1)}, bf16[32,2048]{1,0:T(8,128)(2,1)S(1)}, u32[]{:S(2)}, u32[]{:S(2)}) %collective-permute-start.14) | collective-permute-done | bytes 131104 | tf_op jit(solution)/shard_map/ppermute | solution.py:432
  141.4 1.3 collective-permute-done.15.b3
  142.7 0.7 copy-done.12
  143.4 3.3 %combine.1 = bf16[16,16,2048]{2,1,0:T(8,128)(2,1)} custom-call(bf16[256,128]{1,0:T(8,128)(2,1)} %dense_first.1.hidden, bf16[96,2048]{1,0:T(8,128)(2,1)} %copy-done.2, bf16[96,2048]{1,0:T(8,128)(2,1)} %copy-done.5, bf16[96,2048]{1,0:T(8,128)(2,1)} %copy-done.4, bf16[96,2048]{1,0:T(8,128)(2,1)} %copy-done.3, f32[256,1]{1,0:T(8,128)} %get-tuple-element.43.opening, ...), custom_call_target="tpu_custom_call" | custom-call | tf_op jit(solution)/shard_map/combine/pallas_call | solution.py:336
  146.7 22.6 %all_to_all.26 = bf16[16,16,2048]{2,1,0:T(8,128)(2,1)S(1)} all-to-all(bf16[16,16,2048]{2,1,0:T(8,128)(2,1)} %combine.1), channel_id=1, replica_groups=mesh['z'=4,'y'=4,'x'=4,'tp'=2] {'z','y'}, dimensions={0} | all-to-all | bytes 2097152 | tf_op jit(solution)/shard_map/all_to_all | solution.py:345
  169.3 0.1 reduce_sum.42
  169.4 2.4 %collective-permute-start.16 = (bf16[16,2048]{1,0:T(8,128)(2,1)S(1)}, bf16[16,2048]{1,0:T(8,128)(2,1)S(1)}, u32[]{:S(2)}, u32[]{:S(2)}) collective-permute-start(bf16[16,2048]{1,0:T(8,128)(2,1)S(1)} %reduce_sum.42), channel_id=1, source_target_pairs={{0,1},{1,0},{2,3},{3,2},{4,5},{5,4},{6,7},{7,6},{8,9},{9,8},{10,11... | collective-permute-start | bytes 196616 | tf_op jit(solution)/shard_map/ppermute | solution.py:438
  171.8 0.9 collective-permute-done.16
  172.7 0.7 add_convert_fusion
  (67 shorter events, 0.9 us)
Async XLA Ops:
  0.6 40.9 %collective-permute-start.5 = (bf16[32,768]{1,0:T(8,128)(2,1)}, bf16[32,768]{1,0:T(8,128)(2,1)}, u32[]{:S(2)}, u32[]{:S(2)}) collective-permute-start(bf16[32,768]{1,0:T(8,128)(2,1)} %bitcast.25), channel_id=1, source_target_pairs={{0,6},{2,0},{4,2},{6,4},{1,7},{3,1},{5,3},{7,5},{8,14},{10,8},{12,... | collective-permute-start | bytes 147464 | tf_op jit(solution)/shard_map/ppermute | solution.py:28
  4.0 40.1 %collective-permute-start.4 = (bf16[32,768]{1,0:T(8,128)(2,1)}, bf16[32,768]{1,0:T(8,128)(2,1)}, u32[]{:S(2)}, u32[]{:S(2)}) collective-permute-start(bf16[32,768]{1,0:T(8,128)(2,1)} %bitcast.26), channel_id=1, source_target_pairs={{0,4},{2,6},{4,0},{6,2},{1,5},{3,7},{5,1},{7,3},{8,12},{10,14},{12... | collective-permute-start | bytes 147464 | tf_op jit(solution)/shard_map/ppermute | solution.py:27
  9.0 18.6 %collective-permute-start.2 = (bf16[4,32,768]{2,1,0:T(8,128)(2,1)}, bf16[4,32,768]{2,1,0:T(8,128)(2,1)S(1)}, u32[]{:S(2)}, u32[]{:S(2)}) collective-permute-start(bf16[4,32,768]{2,1,0:T(8,128)(2,1)} %get-tuple-element.29.c0), channel_id=1, source_target_pairs={{0,6},{2,0},{4,2},{6,4},{1,7},{3,1},{5,3},{7,5},{8,14},{10,8},{12,... | collective-permute-start | bytes 589832 | tf_op jit(solution)/shard_map/ppermute | solution.py:28
  9.7 19.8 %collective-permute-start.1 = (bf16[4,32,768]{2,1,0:T(8,128)(2,1)}, bf16[4,32,768]{2,1,0:T(8,128)(2,1)S(1)}, u32[]{:S(2)}, u32[]{:S(2)}) collective-permute-start(bf16[4,32,768]{2,1,0:T(8,128)(2,1)} %get-tuple-element.29.c0), channel_id=1, source_target_pairs={{0,4},{2,6},{4,0},{6,2},{1,5},{3,7},{5,1},{7,3},{8,12},{10,14},{12... | collective-permute-start | bytes 589832 | tf_op jit(solution)/shard_map/ppermute | solution.py:27
  11.4 18.2 %collective-permute-start = (bf16[4,32,768]{2,1,0:T(8,128)(2,1)}, bf16[4,32,768]{2,1,0:T(8,128)(2,1)S(1)}, u32[]{:S(2)}, u32[]{:S(2)}) collective-permute-start(bf16[4,32,768]{2,1,0:T(8,128)(2,1)} %get-tuple-element.29.c0), channel_id=1, source_target_pairs={{0,2},{2,4},{4,6},{6,0},{1,3},{3,5},{5,7},{7,1},{8,10},{10,12},{12... | collective-permute-start | bytes 589832 | tf_op jit(solution)/shard_map/ppermute | solution.py:26
  12.3 15.0 %all-to-all-start = ((bf16[16,48,128]{2,1,0:T(8,128)(2,1)}), bf16[16,48,128]{2,1,0:T(8,128)(2,1)S(1)}, u32[]{:S(2)}, u32[]{:S(2)}) async-start(bf16[16,48,128]{2,1,0:T(8,128)(2,1)} %get-tuple-element.28), calls=%async_computation | async-start | bytes 393216 | tf_op jit(solution)/shard_map/all_to_all | solution.py:345
  25.5 8.9 %copy-start.2 = (bf16[96,2048]{1,0:T(8,128)(2,1)}, bf16[96,2048]{1,0:T(8,128)(2,1)S(1)}, u32[]{:S(2)}) copy-start(bf16[96,2048]{1,0:T(8,128)(2,1)S(1)} %pad_maximum_fusion.c0) | copy-start | bytes 1179652
  27.3 3.0 %copy-start.6 = (bf16[16,48,128]{2,1,0:T(8,128)(2,1)}, bf16[16,48,128]{2,1,0:T(8,128)(2,1)S(1)}, u32[]{:S(2)}) copy-start(bf16[16,48,128]{2,1,0:T(8,128)(2,1)S(1)} %all-to-all-done.x_ref) | copy-start | bytes 589828
  27.6 2.7 %copy-start.7 = (bf16[4,32,768]{2,1,0:T(8,128)(2,1)}, bf16[4,32,768]{2,1,0:T(8,128)(2,1)S(1)}, u32[]{:S(2)}) copy-start(bf16[4,32,768]{2,1,0:T(8,128)(2,1)S(1)} %collective-permute-done.2.c3) | copy-start | bytes 589828
  27.6 23.7 %collective-permute-start.8 = (bf16[96,2048]{1,0:T(8,128)(2,1)S(1)}, bf16[96,2048]{1,0:T(8,128)(2,1)S(1)}, u32[]{:S(2)}, u32[]{:S(2)}) collective-permute-start(bf16[96,2048]{1,0:T(8,128)(2,1)S(1)} %pad_maximum_fusion.c0), channel_id=1, source_target_pairs={{0,6},{2,0},{4,2},{6,4},{1,7},{3,1},{5,3},{7,5},{8,14},{10,8},{12,... | collective-permute-start | bytes 1179656 | tf_op jit(solution)/shard_map/ppermute | solution.py:28
  29.4 0.8 copy-start.8
  29.4 21.9 %collective-permute-start.7 = (bf16[96,2048]{1,0:T(8,128)(2,1)S(1)}, bf16[96,2048]{1,0:T(8,128)(2,1)S(1)}, u32[]{:S(2)}, u32[]{:S(2)}) collective-permute-start(bf16[96,2048]{1,0:T(8,128)(2,1)S(1)} %pad_maximum_fusion.c0), channel_id=1, source_target_pairs={{0,4},{2,6},{4,0},{6,2},{1,5},{3,7},{5,1},{7,3},{8,12},{10,14},{12... | collective-permute-start | bytes 1179656 | tf_op jit(solution)/shard_map/ppermute | solution.py:27
  29.6 0.7 copy-start.9
  29.6 21.7 %collective-permute-start.6 = (bf16[96,2048]{1,0:T(8,128)(2,1)S(1)}, bf16[96,2048]{1,0:T(8,128)(2,1)S(1)}, u32[]{:S(2)}, u32[]{:S(2)}) collective-permute-start(bf16[96,2048]{1,0:T(8,128)(2,1)S(1)} %pad_maximum_fusion.c0), channel_id=1, source_target_pairs={{0,2},{2,4},{4,6},{6,0},{1,3},{3,5},{5,7},{7,1},{8,10},{10,12},{12... | collective-permute-start | bytes 1179656 | tf_op jit(solution)/shard_map/ppermute | solution.py:26
  34.3 24.5 %all-to-all-start.1 = ((bf16[16,16,3072]{2,1,0:T(8,128)(2,1)}), bf16[16,16,3072]{2,1,0:T(8,128)(2,1)S(1)}, u32[]{:S(2)}, u32[]{:S(2)}) async-start(bf16[16,16,3072]{2,1,0:T(8,128)(2,1)} %project.1), calls=%async_computation.1 | async-start | bytes 3145728 | tf_op jit(solution)/shard_map/all_to_all | solution.py:345
  41.6 9.7 %collective-permute-start.3 = (bf16[32,768]{1,0:T(8,128)(2,1)}, bf16[32,768]{1,0:T(8,128)(2,1)S(1)}, u32[]{:S(2)}, u32[]{:S(2)}) collective-permute-start(bf16[32,768]{1,0:T(8,128)(2,1)} %bitcast.27), channel_id=1, source_target_pairs={{0,2},{2,4},{4,6},{6,0},{1,3},{3,5},{5,7},{7,1},{8,10},{10,12},{12... | collective-permute-start | bytes 147464 | tf_op jit(solution)/shard_map/ppermute | solution.py:26
  51.3 31.5 %copy-start.17 = (bf16[32,768]{1,0:T(8,128)(2,1)}, bf16[32,768]{1,0:T(8,128)(2,1)S(1)}, u32[]{:S(2)}) copy-start(bf16[32,768]{1,0:T(8,128)(2,1)S(1)} %collective-permute-done.3.c1) | copy-start | bytes 147460
  51.3 41.9 %copy-start.3 = (bf16[96,2048]{1,0:T(8,128)(2,1)}, bf16[96,2048]{1,0:T(8,128)(2,1)S(1)}, u32[]{:S(2)}) copy-start(bf16[96,2048]{1,0:T(8,128)(2,1)S(1)} %collective-permute-done.8.c3) | copy-start | bytes 1179652
  51.3 41.9 %copy-start.4 = (bf16[96,2048]{1,0:T(8,128)(2,1)}, bf16[96,2048]{1,0:T(8,128)(2,1)S(1)}, u32[]{:S(2)}) copy-start(bf16[96,2048]{1,0:T(8,128)(2,1)S(1)} %collective-permute-done.7.c2) | copy-start | bytes 1179652
  51.3 41.9 %copy-start.5 = (bf16[96,2048]{1,0:T(8,128)(2,1)}, bf16[96,2048]{1,0:T(8,128)(2,1)S(1)}, u32[]{:S(2)}) copy-start(bf16[96,2048]{1,0:T(8,128)(2,1)S(1)} %collective-permute-done.6.c1) | copy-start | bytes 1179652
  58.8 1.2 copy-start
  60.0 31.1 %slice-start = ((bf16[16,48,128]{2,1,0:T(8,128)(2,1)}), bf16[16,16,128]{2,1,0:T(8,128)(2,1)S(1)}, s32[]{:S(2)}) async-start(bf16[16,48,128]{2,1,0:T(8,128)(2,1)} %copy-done.6), calls=%async_computation.5 | async-start | bytes 131072 | tf_op jit(solution)/shard_map/slice | solution.py:387
  84.8 6.3 %collective-permute-start.9 = (bf16[256,128]{1,0:T(8,128)(2,1)}, bf16[256,128]{1,0:T(8,128)(2,1)S(1)}, u32[]{:S(2)}, u32[]{:S(2)}) collective-permute-start(bf16[256,128]{1,0:T(8,128)(2,1)} %mix.1), channel_id=1, source_target_pairs={{0,1},{1,0},{2,3},{3,2},{4,5},{5,4},{6,7},{7,6},{8,9},{9,8},{10,11... | collective-permute-start | bytes 196616 | tf_op jit(solution)/shard_map/ppermute | solution.py:413
  93.2 20.6 %all-to-all-start.3 = ((bf16[16,256,128]{2,1,0:T(8,128)(2,1)}), bf16[16,256,128]{2,1,0:T(8,128)(2,1)S(1)}, u32[]{:S(2)}, u32[]{:S(2)}) async-start(bf16[16,256,128]{2,1,0:T(8,128)(2,1)} %broadcast_in_dim.15), calls=%async_computation.3 | async-start | bytes 2097152 | tf_op jit(solution)/shard_map/all_to_all | solution.py:345
  113.8 1.0 copy-start.1
  118.0 5.2 %collective-permute-start.10 = (bf16[32,2048]{1,0:T(8,128)(2,1)}, bf16[32,2048]{1,0:T(8,128)(2,1)S(1)}, u32[]{:S(2)}, u32[]{:S(2)}) collective-permute-start(bf16[32,2048]{1,0:T(8,128)(2,1)} %get-tuple-element.46), channel_id=1, source_target_pairs={{0,2},{2,4},{4,6},{6,0},{1,3},{3,5},{5,7},{7,1},{8,10},{10,12},{12... | collective-permute-start | bytes 393224 | tf_op jit(solution)/shard_map/ppermute | solution.py:423
  119.8 6.3 %collective-permute-start.11 = (bf16[32,2048]{1,0:T(8,128)(2,1)}, bf16[32,2048]{1,0:T(8,128)(2,1)S(1)}, u32[]{:S(2)}, u32[]{:S(2)}) collective-permute-start(bf16[32,2048]{1,0:T(8,128)(2,1)} %get-tuple-element.47), channel_id=1, source_target_pairs={{0,4},{2,6},{4,0},{6,2},{1,5},{3,7},{5,1},{7,3},{8,12},{10,14},{12... | collective-permute-start | bytes 393224 | tf_op jit(solution)/shard_map/ppermute | solution.py:424
  121.2 5.3 %collective-permute-start.12 = (bf16[32,2048]{1,0:T(8,128)(2,1)}, bf16[32,2048]{1,0:T(8,128)(2,1)S(1)}, u32[]{:S(2)}, u32[]{:S(2)}) collective-permute-start(bf16[32,2048]{1,0:T(8,128)(2,1)} %get-tuple-element.48), channel_id=1, source_target_pairs={{0,6},{2,0},{4,2},{6,4},{1,7},{3,1},{5,3},{7,5},{8,14},{10,8},{12,... | collective-permute-start | bytes 393224 | tf_op jit(solution)/shard_map/ppermute | solution.py:425
  123.3 3.3 %copy-start.13 = (bf16[32,2048]{1,0:T(8,128)(2,1)}, bf16[32,2048]{1,0:T(8,128)(2,1)S(1)}, u32[]{:S(2)}) copy-start(bf16[32,2048]{1,0:T(8,128)(2,1)S(1)} %collective-permute-done.10.a1) | copy-start | bytes 393220
  126.1 0.7 copy-start.14
  126.5 0.7 copy-start.15
  132.4 7.0 %collective-permute-start.13 = (bf16[32,2048]{1,0:T(8,128)(2,1)}, bf16[32,2048]{1,0:T(8,128)(2,1)S(1)}, u32[]{:S(2)}, u32[]{:S(2)}) collective-permute-start(bf16[32,2048]{1,0:T(8,128)(2,1)} %get-tuple-element.50), channel_id=1, source_target_pairs={{0,6},{2,0},{4,2},{6,4},{1,7},{3,1},{5,3},{7,5},{8,14},{10,8},{12,... | collective-permute-start | bytes 393224 | tf_op jit(solution)/shard_map/ppermute | solution.py:431
  135.8 5.6 %collective-permute-start.14 = (bf16[32,2048]{1,0:T(8,128)(2,1)}, bf16[32,2048]{1,0:T(8,128)(2,1)S(1)}, u32[]{:S(2)}, u32[]{:S(2)}) collective-permute-start(bf16[32,2048]{1,0:T(8,128)(2,1)} %get-tuple-element.51), channel_id=1, source_target_pairs={{0,4},{2,6},{4,0},{6,2},{1,5},{3,7},{5,1},{7,3},{8,12},{10,14},{12... | collective-permute-start | bytes 393224 | tf_op jit(solution)/shard_map/ppermute | solution.py:432
  135.8 6.9 %collective-permute-start.15 = (bf16[32,2048]{1,0:T(8,128)(2,1)}, bf16[32,2048]{1,0:T(8,128)(2,1)S(1)}, u32[]{:S(2)}, u32[]{:S(2)}) collective-permute-start(bf16[32,2048]{1,0:T(8,128)(2,1)} %get-tuple-element.52), channel_id=1, source_target_pairs={{0,2},{2,4},{4,6},{6,0},{1,3},{3,5},{5,7},{7,1},{8,10},{10,12},{12... | collective-permute-start | bytes 393224 | tf_op jit(solution)/shard_map/ppermute | solution.py:433
  139.5 3.3 %copy-start.10 = (bf16[32,2048]{1,0:T(8,128)(2,1)}, bf16[32,2048]{1,0:T(8,128)(2,1)S(1)}, u32[]{:S(2)}) copy-start(bf16[32,2048]{1,0:T(8,128)(2,1)S(1)} %collective-permute-done.13.b1) | copy-start | bytes 393220
  141.4 1.3 copy-start.11
  142.7 0.7 copy-start.12
  146.7 26.0 %copy-start.16 = (bf16[16,2048]{1,0:T(8,128)(2,1)S(1)}, bf16[16,2048]{1,0:T(8,128)(2,1)}, u32[]{:S(2)}) copy-start(bf16[16,2048]{1,0:T(8,128)(2,1)} %get-tuple-element.37) | copy-start | bytes 196612
  169.4 3.3 %collective-permute-start.16 = (bf16[16,2048]{1,0:T(8,128)(2,1)S(1)}, bf16[16,2048]{1,0:T(8,128)(2,1)S(1)}, u32[]{:S(2)}, u32[]{:S(2)}) collective-permute-start(bf16[16,2048]{1,0:T(8,128)(2,1)S(1)} %reduce_sum.42), channel_id=1, source_target_pairs={{0,1},{1,0},{2,3},{3,2},{4,5},{5,4},{6,7},{7,6},{8,9},{9,8},{10,11... | collective-permute-start | bytes 196616 | tf_op jit(solution)/shard_map/ppermute | solution.py:438
where the time goes:
time: 175 us; the launch traced here: 173 us
  starting transfers between devices  44.6 us (25%)
  waiting for transfers between devices  41.6 us (24%)
  blocking collectives  36.4 us (21%)
  Pallas kernels  31.4 us (18%)
  local copies, waits for them, and re-layouts  12.1 us (7%)
  other arithmetic  6.16 us (4%)
    all_to_all x2, blocking collectives, plane_exchange(): return lax.all_to_all(array, PLANE, split_axis=0, concat_axis=0, tiled=True)  36.4 us
    all_to_all x3, waiting for transfers between devices, plane_exchange(): return lax.all_to_all(array, PLANE, split_axis=0, concat_axis=0, tiled=True)  25.5 us
    all_to_all x3, starting transfers between devices, plane_exchange(): return lax.all_to_all(array, PLANE, split_axis=0, concat_axis=0, tiled=True)  16.3 us
    pallas_call x1, Pallas kernels, retain(): pl.pallas_call(retain_body, in_specs=[SMEM, anywhere, vmem, vmem, vmem, a...  9.01 us
    ppermute x3, waiting for transfers between devices, ring_gather(): lax.ppermute(own, 'x', RIGHT)  7.15 us
    unnamed x39, local copies, waits for them, and re-layouts  6.39 us
    ppermute x3, starting transfers between devices, ring_gather(): lax.ppermute(own, 'x', LEFT)  5.91 us
    ppermute x1, starting transfers between devices, on_device(): other = lax.ppermute(mixed, 'tp', SWAP)  5.22 us
  transfers between devices with their start and end apart: 20, of which 11 were waited for; matrix products, arithmetic and copies ran while one was open for 7% of the time, Pallas kernels for 5%

commit v1 on v0

v1 whole, which is shorter than its diff:
```python
import jax
import jax.numpy as jnp
import numpy as np
from jax import lax
from jax.experimental import pallas as pl
from jax.experimental.pallas import tpu as pltpu
from jax.sharding import Mesh, PartitionSpec as P


D = 2048
HEADS = 12
EPS = 1e-06
F32 = jnp.float32
BF16 = jnp.bfloat16

RIGHT = [(i, (i + 1) % 4) for i in range(4)]
LEFT = [(i, (i - 1) % 4) for i in range(4)]
ACROSS = [(i, (i + 2) % 4) for i in range(4)]
SWAP = [(0, 1), (1, 0)]
PLANE = ("z", "y")
NT = (((1,), (1,)), ((), ()))
TN = (((0,), (0,)), ((), ()))
HBM = pl.BlockSpec(memory_space=pltpu.HBM)
VMEM = pl.BlockSpec(memory_space=pltpu.VMEM)


def ring_gather(own):
    return (
        own,
        lax.ppermute(own, "x", RIGHT),
        lax.ppermute(own, "x", ACROSS),
        lax.ppermute(own, "x", LEFT),
    )


OFFSETS = (0, 3, 2, 1)


SMEM = pl.BlockSpec(memory_space=pltpu.SMEM)


def prepare_body(x_ref, gain, ids, shares, wq, wk, wv, wg, sent, w4, routes):
    w4[0] = wq[...]
    w4[1] = wk[...]
    w4[2] = wv[...]
    w4[3] = wg[...]
    half = x_ref[pl.ds(pl.multiple_of(lax.axis_index("tp") * 8, 8), 8), :]
    routes[...] = jnp.zeros((8, 128), F32)
    routes[0:4, 0:16] = ids[...].astype(F32)
    routes[4:8, 0:16] = shares[...].astype(F32)
    first = lax.axis_index(PLANE) * 8
    turned = pltpu.roll(routes[...], (first - lax.axis_index("tp") * 8 + 128) % 128, 1)
    lane = lax.broadcasted_iota(jnp.int32, (8, 128), 1)
    route = jnp.where(lane // 8 == first // 8, turned, 0.0).astype(BF16)
    x = x_ref[...]
    v = x.astype(F32)
    scaled = v * lax.rsqrt(jnp.mean(v * v, axis=-1, keepdims=True) + EPS)
    normed = (scaled * gain[...].astype(F32).reshape(1, D)).astype(BF16)
    for j in range(16):
        at = slice(j * 128, (j + 1) * 128)
        sent[j, 0:16, :] = normed[:, at]
        sent[j, 16:24, :] = half[:, at]
        sent[j, 24:32, :] = route


def prepare(x, gain, ids, shares, ws):
    return pl.pallas_call(
        prepare_body,
        out_shape=[
            jax.ShapeDtypeStruct((16, 32, 128), BF16),
            jax.ShapeDtypeStruct((4, 32, 768), BF16),
        ],
        scratch_shapes=[pltpu.VMEM((8, 128), F32)],
        name="prepare",
    )(x, gain, ids, shares, *ws)


def project_body(x_ref, c0, c1, c2, c3, out_ref, wide, out, sems):
    xi = lax.axis_index("x")
    x = x_ref[:, 0:16, :].reshape(256, 128)
    stores = []
    for p in range(4):
        for offset, chunk in zip(OFFSETS, (c0, c1, c2, c3)):
            at = pl.multiple_of(((xi + offset) % 4) * 32, 32)
            wide[p, pl.ds(at, 32), :] = chunk[p]
        at = pl.ds(p * 768, 768)
        out[:, :, at] = (
            jnp.dot(x, wide[p], preferred_element_type=F32).astype(BF16).reshape(16, 16, 768)
        )
        stores.append(pltpu.make_async_copy(out.at[:, :, at], out_ref.at[:, :, at], sems.at[p]))
        stores[-1].start()
    for store in stores:
        store.wait()


def project(got, chunks):
    return pl.pallas_call(
        project_body,
        in_specs=[VMEM] * 5,
        out_specs=HBM,
        out_shape=jax.ShapeDtypeStruct((16, 16, 3072), BF16),
        scratch_shapes=[
            pltpu.VMEM((4, 128, 768), BF16),
            pltpu.VMEM((16, 16, 3072), BF16),
            pltpu.SemaphoreType.DMA((4,)),
        ],
        name="project",
    )(got, *chunks)


PER_STEP = 2
STEPS = 16 // PER_STEP
FREQUENCY = np.tile(10000.0 ** (-np.arange(64) * 2.0 / 128), 2).astype(np.float32)
TURN = np.repeat([-1.0, 1.0], 64).astype(np.float32)
GAMMA = [float(np.exp(np.log1p(-(2.0 ** (-5.0 - 5.0 * h / (HEADS - 1)))))) for h in range(HEADS)]


def retain_body(
    parts, cosine_ref, sine_ref, gain, state_ref, new_state, sent,
    buf, turns, queries_keys, values, gates, readouts, sems,
):
    fetch_turns = [
        pltpu.make_async_copy(cosine_ref, turns.at[0], sems.at[2 * STEPS]),
        pltpu.make_async_copy(sine_ref, turns.at[1], sems.at[2 * STEPS + 1]),
    ]
    for c in fetch_turns:
        c.start()
    upper = lax.axis_index("tp") == 1
    gamma = [jnp.where(upper, GAMMA[h + 6], GAMMA[h]).astype(F32) for h in range(6)]

    def rows(i):
        return pl.ds(i * PER_STEP, PER_STEP)

    def fetch(i):
        return pltpu.make_async_copy(state_ref.at[rows(i)], buf.at[rows(i)], sems.at[i])

    def store(i):
        return pltpu.make_async_copy(buf.at[rows(i)], new_state.at[rows(i)], sems.at[STEPS + i])

    for i in range(STEPS):
        fetch(i).start()
    for c in fetch_turns:
        c.wait()
    cos_v, sin_v = turns[0], turns[1]
    for h in range(6):
        def total(which):
            at = which * 768 + h * 128
            acc = parts[0, :, at : at + 128].astype(F32)
            for s in range(1, 16):
                acc = acc + parts[s, :, at : at + 128].astype(F32)
            return acc.astype(BF16).astype(F32)

        q, k, v, g = (total(i) for i in range(4))
        queries_keys[:, h, :] = q * cos_v + pltpu.roll(q, 64, 1) * sin_v
        queries_keys[:, 8 + h, :] = (k * cos_v + pltpu.roll(k, 64, 1) * sin_v) * (128.0 ** -0.5)
        values[:, h, :] = v
        gates[:, h * 128 : (h + 1) * 128] = g * jax.nn.sigmoid(g)

    def some(i, carry):
        fetch(i).wait()
        for j in range(PER_STEP):
            t = i * PER_STEP + j
            cols = jnp.transpose(queries_keys[t])
            for h in range(6):
                q_col = cols[:, h : h + 1]
                k_col = cols[:, 8 + h : 9 + h]
                v_row = values[t, h : h + 1, :]
                fresh = gamma[h] * buf[t, h] + k_col * v_row
                buf[t, h] = fresh
                readouts[t, h : h + 1, :] = jnp.sum(q_col * fresh, axis=0, keepdims=True)
        store(i).start()
        return carry

    lax.fori_loop(0, STEPS, some, 0)
    gains = gain[...].astype(F32).reshape(1, 768)
    for h in range(6):
        at = slice(h * 128, (h + 1) * 128)
        r = readouts[:, h, :]
        centred = r - jnp.mean(r, axis=-1, keepdims=True)
        unit = centred * lax.rsqrt(jnp.mean(centred * centred, axis=-1, keepdims=True) + EPS)
        kept = (unit * gains[:, at] * gates[:, at]).astype(BF16)
        for s in range(16):
            sent[s, :, at] = kept
    for i in range(STEPS):
        store(i).wait()


def retain(parts, cosine, sine, gain, state):
    return pl.pallas_call(
        retain_body,
        in_specs=[VMEM, HBM, HBM, VMEM, HBM],
        out_specs=[HBM, VMEM],
        out_shape=[
            jax.ShapeDtypeStruct((16, 6, 128, 128), F32),
            jax.ShapeDtypeStruct((16, 16, 768), BF16),
        ],
        scratch_shapes=[
            pltpu.VMEM((16, 6, 128, 128), F32),
            pltpu.VMEM((2, 16, 128), F32),
            pltpu.VMEM((16, 16, 128), F32),
            pltpu.VMEM((16, 8, 128), F32),
            pltpu.VMEM((16, 768), F32),
            pltpu.VMEM((16, 8, 128), F32),
            pltpu.SemaphoreType.DMA((2 * STEPS + 2,)),
        ],
        name="retain",
    )(parts, cosine, sine, gain, state)


def mix_body(kept, c0, c1, c2, c3, keep, give, wide, mixed):
    xi = lax.axis_index("x")
    core = lax.axis_index("tp")
    for offset, chunk in zip(OFFSETS, (c0, c1, c2, c3)):
        at = pl.multiple_of(((xi + offset) % 4) * 32, 32)
        wide[pl.ds(at, 32), :] = chunk[...]
    rows = kept[...].reshape(256, 768)
    out = lax.dot_general(rows, wide[...], NT, preferred_element_type=F32)
    mixed[...] = out.reshape(16, 16, 128)
    keep[...] = mixed[:, pl.ds(pl.multiple_of(core * 8, 8), 8), :].astype(BF16)
    give[...] = mixed[:, pl.ds(pl.multiple_of((1 - core) * 8, 8), 8), :].astype(BF16)


def mix(kept, chunks):
    half = jax.ShapeDtypeStruct((16, 8, 128), BF16)
    return pl.pallas_call(
        mix_body,
        in_specs=[VMEM] * 5,
        out_shape=[half, half],
        scratch_shapes=[pltpu.VMEM((128, 768), BF16), pltpu.VMEM((16, 16, 128), F32)],
        name="mix",
    )(kept, *chunks)


def settle_body(mine, other, got, out_ref):
    mixer_out = (mine[...].astype(F32) + other[...].astype(F32)).astype(BF16)
    res = (got[:, 16:24, :].astype(F32) + mixer_out.astype(F32)).astype(BF16).reshape(128, 128)
    for s in range(16):
        out_ref[s] = res


def settle(mine, other, got):
    return pl.pallas_call(
        settle_body,
        out_shape=jax.ShapeDtypeStruct((16, 128, 128), BF16),
        name="settle",
    )(mine, other, got)


def spread_body(res, gain, branch, pick, plane, s0, s1, s2, s3, opening, own):
    total = jnp.zeros((128, 128), F32)
    for s in range(16):
        r = res[s].astype(F32)
        total = total + r * r
    scale = lax.rsqrt(jnp.sum(total, axis=-1, keepdims=True) / D + EPS)
    first = pl.multiple_of(lax.axis_index(PLANE) * 8, 8)
    gains = gain[...].astype(F32).reshape(1, D)
    branches = branch[...].astype(F32).reshape(1, D)
    dots = jnp.zeros((128, 128), F32)
    for s in range(16):
        at = slice(s * 128, (s + 1) * 128)
        n = (res[s].astype(F32) * scale * gains[:, at]).astype(BF16)
        plane[:, at] = n
        dots = dots + n.astype(F32) * branches[:, at]
        rows = jnp.dot(pick[...], n, preferred_element_type=F32).astype(BF16)
        for k, out in enumerate((s0, s1, s2, s3)):
            out[:, at] = rows[k * 32 : (k + 1) * 32]
        own[:, at] = res[s, pl.ds(first, 8), :]
    opening[...] = jax.nn.sigmoid(jnp.sum(dots, axis=-1, keepdims=True))


def spread(res, gain, branch, pick):
    rows = jax.ShapeDtypeStruct((32, D), BF16)
    return pl.pallas_call(
        spread_body,
        in_specs=[VMEM] * 4,
        out_shape=[
            jax.ShapeDtypeStruct((128, D), BF16), rows, rows, rows, rows,
            jax.ShapeDtypeStruct((128, 1), F32),
            jax.ShapeDtypeStruct((8, D), BF16),
        ],
        name="spread",
    )(res, gain, branch, pick)


def dense_body(plane, c0, c1, c2, c3, c4, c5, c6, c7, hidden, gate, up):
    for r, chunk in enumerate((c0, c1, c2, c3, c4, c5, c6, c7)):
        at = slice(r * 32, (r + 1) * 32)
        gate[at, :] = chunk[0:32, :]
        up[at, :] = chunk[32:64, :]
    x = plane[...]
    g = lax.dot_general(x, gate[...], NT, preferred_element_type=F32)
    u = lax.dot_general(x, up[...], NT, preferred_element_type=F32)
    hidden[...] = (g * jax.nn.sigmoid(g) * u).astype(BF16)


def dense_first(plane, chunks):
    return pl.pallas_call(
        dense_body,
        out_shape=jax.ShapeDtypeStruct((128, 256), BF16),
        scratch_shapes=[pltpu.VMEM((256, D), BF16), pltpu.VMEM((256, D), BF16)],
        name="dense_first",
    )(plane, *chunks)


CUT = 4


def expert_body(
    a0, a1, a2, a3, gate_a, gate_b, up_a, up_b, down_a, down_b, r0, r1, r2, r3,
    rows, gate, up, down, sems,
):
    halves = []
    for w, (g_ref, u_ref, d_ref) in enumerate(((gate_a, up_a, down_a), (gate_b, up_b, down_b))):
        base = w * 3 * CUT
        gu, dn = [], []
        for i in range(CUT):
            n, m = D // CUT, 512 // CUT
            at, low = pl.ds(i * n, n), pl.ds(i * m, m)
            gu.append((
                pltpu.make_async_copy(g_ref.at[0, at], gate.at[w, at], sems.at[base + i]),
                pltpu.make_async_copy(u_ref.at[0, at], up.at[w, at], sems.at[base + CUT + i]),
            ))
            dn.append(
                pltpu.make_async_copy(d_ref.at[0, low], down.at[w, low], sems.at[base + 2 * CUT + i])
            )
        halves.append((gu, dn))
    for gu, _ in halves:
        for g, u in gu:
            g.start()
            u.start()
    for _, dn in halves:
        for d in dn:
            d.start()
    for k, a in enumerate((a0, a1, a2, a3)):
        rows[k * 32 : (k + 1) * 32, :] = a[...]
    n = D // CUT
    hidden = []
    for w, (gu, _) in enumerate(halves):
        g_sum = u_sum = None
        for i, (g, u) in enumerate(gu):
            at = slice(i * n, (i + 1) * n)
            g.wait()
            g_part = jnp.dot(rows[:, at], gate[w, at, :], preferred_element_type=F32)
            u.wait()
            u_part = jnp.dot(rows[:, at], up[w, at, :], preferred_element_type=F32)
            g_sum = g_part if g_sum is None else g_sum + g_part
            u_sum = u_part if u_sum is None else u_sum + u_part
        hidden.append((g_sum * jax.nn.sigmoid(g_sum) * u_sum).astype(BF16))
    for _, dn in halves:
        for d in dn:
            d.wait()
    for j in range(4):
        at = slice(j * 512, (j + 1) * 512)
        out = jnp.dot(hidden[0], down[0, :, at], preferred_element_type=F32)
        out = (out + jnp.dot(hidden[1], down[1, :, at], preferred_element_type=F32)).astype(BF16)
        for k, r in enumerate((r0, r1, r2, r3)):
            r[:, at] = out[k * 32 : (k + 1) * 32, :]


def experts(arrived, weights):
    rows = jax.ShapeDtypeStruct((32, D), BF16)
    return pl.pallas_call(
        expert_body,
        in_specs=[VMEM] * 4 + [HBM] * 6,
        out_shape=[rows] * 4,
        scratch_shapes=[
            pltpu.VMEM((128, D), BF16),
            pltpu.VMEM((2, D, 512), BF16),
            pltpu.VMEM((2, D, 512), BF16),
            pltpu.VMEM((2, 512, D), BF16),
            pltpu.SemaphoreType.DMA((6 * CUT,)),
        ],
        name="experts",
    )(*arrived, *weights)


def combine_body(
    hidden, c0, c1, c2, c3, c4, c5, c6, c7, opening, weigh, b0, b1, b2, b3, out, down, back
):
    for r, chunk in enumerate((c0, c1, c2, c3, c4, c5, c6, c7)):
        down[r * 32 : (r + 1) * 32, :] = chunk[64:96, :]
    for k, b in enumerate((b0, b1, b2, b3)):
        back[k * 32 : (k + 1) * 32, :] = b[...]
        back[128 + k * 32 : 128 + (k + 1) * 32, :] = b[...]
    opened = opening[...]
    for j in range(4):
        at = slice(j * 512, (j + 1) * 512)
        term = jnp.dot(hidden[...], down[:, at], preferred_element_type=F32) * opened
        term = term + lax.dot_general(weigh[...], back[:, at], TN, preferred_element_type=F32)
        out[:, :, at] = term.astype(BF16).reshape(16, 8, 512)


def combine(hidden, chunks, opening, weigh, back):
    return pl.pallas_call(
        combine_body,
        out_shape=jax.ShapeDtypeStruct((16, 8, D), BF16),
        scratch_shapes=[pltpu.VMEM((256, D), BF16), pltpu.VMEM((256, D), BF16)],
        name="combine",
    )(hidden, *chunks, opening, weigh, *back)


def plane_exchange(array):
    return lax.all_to_all(array, PLANE, split_axis=0, concat_axis=0, tiled=True)


def routing_body(got, pick, weigh):
    total = got[0, 24:32, :].astype(F32)
    for s in range(1, 16):
        total = total + got[s, 24:32, :].astype(F32)
    ids, weights = total[0:4], total[4:8]
    share = weights / jnp.sum(weights, axis=0, keepdims=True)
    a = lax.broadcasted_iota(jnp.int32, (128, 128), 0)
    b = lax.broadcasted_iota(jnp.int32, (128, 128), 1)
    before = ((a // 8 == b // 8) & (a < b)).astype(F32).astype(BF16)
    slot = lax.broadcasted_iota(jnp.int32, (32, 128), 0)
    token = lax.broadcasted_iota(jnp.int32, (32, 128), 1)
    mine = slot // 2 == token // 8
    x_at = lax.axis_index("x")
    zy_at = lax.axis_index(PLANE)
    for k in range(4):
        wanted = (zy_at * 4 + (x_at + k) % 4).astype(F32)
        hits = (ids == wanted).astype(F32)
        match = jnp.sum(hits, axis=0, keepdims=True)
        share_of = jnp.sum(hits * share, axis=0, keepdims=True)
        many = jnp.broadcast_to(match, (32, 128))
        rank = jnp.dot(many.astype(BF16), before, preferred_element_type=F32)
        place = mine & (rank == (slot % 2).astype(F32)) & (many > 0)
        at = slice(k * 32, (k + 1) * 32)
        pick[at, :] = jnp.where(place, 1.0, 0.0).astype(BF16)
        value = jnp.where(place, jnp.broadcast_to(share_of, (32, 128)), 0.0)
        high = value.astype(BF16)
        weigh[at, :] = high
        weigh[k * 32 + 128 : k * 32 + 160, :] = (value - high.astype(F32)).astype(BF16)


def routing(got):
    return pl.pallas_call(
        routing_body,
        out_shape=[
            jax.ShapeDtypeStruct((128, 128), BF16),
            jax.ShapeDtypeStruct((256, 128), BF16),
        ],
        name="routing",
    )(got)


def on_device(
    inputs, positions, ret_state, norm_mix, w_query, w_key, w_value, w_gate_in, head_gain, w_out,
    norm_ffn, route_ids, route_weight, exp_gate, exp_up, exp_down, dense_gate, dense_up, dense_down,
    branch_gate,
):
    core = lax.axis_index("tp")

    sent, w4 = prepare(
        inputs, norm_mix, route_ids.T, route_weight.T, (w_query, w_key, w_value, w_gate_in)
    )
    chunks = ring_gather(w4)
    got = plane_exchange(sent)

    partial = project(got, chunks)
    partial, got, positions, w_out, dense_gate, dense_up, dense_down, expert_own = (
        lax.optimization_barrier(
            (
                partial, got, positions, w_out, dense_gate, dense_up, dense_down,
                (exp_gate, exp_up, exp_down),
            )
        )
    )
    parts = plane_exchange(partial)

    out_chunks = ring_gather(w_out.T)
    dense = jnp.concatenate([dense_gate.T, dense_up.T, dense_down], axis=0)
    dense_chunks = ring_gather(dense)
    expert_other = tuple(lax.ppermute(w, "tp", SWAP) for w in expert_own)
    dense_chunks = dense_chunks + tuple(lax.ppermute(c, "tp", SWAP) for c in dense_chunks)
    pick, weigh = routing(got)

    angles = positions.astype(F32)[:, None] * FREQUENCY[None, :]
    cosine = jnp.cos(angles)
    sine = jnp.sin(angles) * TURN[None, :]
    new_state, kept = retain(parts, cosine, sine, head_gain, ret_state)
    kept = plane_exchange(kept)
    kept, out_chunks, dense_chunks, expert_other, pick, weigh = lax.optimization_barrier(
        (kept, out_chunks, dense_chunks, expert_other, pick, weigh)
    )
    keep, give = mix(kept, out_chunks)
    settled = settle(keep, lax.ppermute(give, "tp", SWAP), got)
    res = plane_exchange(settled)

    plane, s0, s1, s2, s3, opening, own_res = spread(res, norm_ffn, branch_gate, pick)
    arrived = (
        s0,
        lax.ppermute(s1, "x", RIGHT),
        lax.ppermute(s2, "x", ACROSS),
        lax.ppermute(s3, "x", LEFT),
    )
    hidden = dense_first(plane, dense_chunks)
    weights = tuple(w for pair in zip(expert_own, expert_other) for w in pair)
    r0, r1, r2, r3 = experts(arrived, weights)
    back = (
        r0,
        lax.ppermute(r1, "x", LEFT),
        lax.ppermute(r2, "x", ACROSS),
        lax.ppermute(r3, "x", RIGHT),
    )
    branch = combine(hidden, dense_chunks, opening, weigh, back)
    terms = plane_exchange(branch)
    summed = jnp.sum(terms.astype(F32), axis=0)
    mine = (own_res.astype(F32) + summed).astype(BF16)
    other = lax.ppermute(mine, "tp", SWAP)
    layer_out = jnp.concatenate(
        [jnp.where(core == 0, mine, other), jnp.where(core == 0, other, mine)], axis=0
    )
    return (layer_out, new_state)


EP = ("z", "y", "x")


def solution(mesh):
    inner = Mesh(mesh.devices.reshape(4, 4, 4, 2), ("z", "y", "x", "tp"))
    in_specs = (
        P(EP, None),
        P(EP),
        P(EP, "tp", None, None),
        P(),
        P(EP, "tp"),
        P(EP, "tp"),
        P(EP, "tp"),
        P(EP, "tp"),
        P("tp"),
        P("tp", EP),
        P(),
        P(EP, None),
        P(EP, None),
        P(EP, None, "tp"),
        P(EP, None, "tp"),
        P(EP, "tp", None),
        P(None, (*EP, "tp")),
        P(None, (*EP, "tp")),
        P((*EP, "tp"), None),
        P(),
    )
    out_specs = (P(EP, None), P(EP, "tp", None, None))
    return jax.shard_map(
        on_device, mesh=inner, in_specs=in_specs, out_specs=out_specs, check_vma=False
    )
```

time: 175 us -> 182 us (1.040)
  blocking collectives: 36.4 us -> 47.8 us
  waiting for transfers between devices: 41.6 us -> 51.7 us
  starting transfers between devices: 44.6 us -> 36.9 us
  local copies, waits for them, and re-layouts: 12.1 us -> 6.38 us
  other arithmetic: 6.16 us -> 1.48 us
  Pallas kernels: 31.4 us -> 35.7 us
    all_to_all x3 -> x2, waiting for transfers between devices: 25.5 us -> 7.79 us  [plane_exchange(): return lax.all_to_all(array, PLANE, split_axis=0, concat_axis=0, tiled=True)]
    ppermute x3, waiting for transfers between devices: 0.01 us -> 12.3 us  [ring_gather(): lax.ppermute(own, 'x', ACROSS)]
    all_to_all x2 -> x3, blocking collectives: 36.4 us -> 47.8 us  [plane_exchange(): return lax.all_to_all(array, PLANE, split_axis=0, concat_axis=0, tiled=True)]
    ppermute x3, waiting for transfers between devices: 0.01 us -> 8.16 us  [ring_gather(): lax.ppermute(own, 'x', LEFT)]
    all_to_all x3 -> x2, starting transfers between devices: 16.3 us -> 9.95 us  [plane_exchange(): return lax.all_to_all(array, PLANE, split_axis=0, concat_axis=0, tiled=True)]
    ppermute x3, waiting for transfers between devices: 7.15 us -> 12.4 us  [ring_gather(): lax.ppermute(own, 'x', RIGHT)]
    ppermute x2 -> x9, starting transfers between devices: 7.62 us -> 12.7 us  [the longest x4 5.65 us: on_device(): lax.ppermute(c, 'tp', SWAP)]
    pallas_call x8 -> x10, Pallas kernels: 31.4 us -> 35.7 us  [the longest x1 9.04 us: retain(): pl.pallas_call(retain_body, in_specs=[VMEM, HBM, HBM, VMEM, HBM], out_spe...]
  transfers between devices with their start and end apart: 20 -> 26, of which waited for: 11 -> 14; matrix products, arithmetic and copies ran while one was open for 7% -> 0% of each run, Pallas kernels for 5% -> 8%
where the time goes in v1:
time: 182 us; the launch traced here: 181 us
  waiting for transfers between devices  51.7 us (28%)
  blocking collectives  47.8 us (26%)
  starting transfers between devices  36.9 us (20%)
  Pallas kernels  35.7 us (20%)
  local copies, waits for them, and re-layouts  6.38 us (4%)
    all_to_all x3, blocking collectives, plane_exchange(): return lax.all_to_all(array, PLANE, split_axis=0, concat_axis=0, tiled=True)  47.8 us
    ppermute x3, waiting for transfers between devices, ring_gather(): lax.ppermute(own, 'x', RIGHT)  12.4 us
    ppermute x3, waiting for transfers between devices, ring_gather(): lax.ppermute(own, 'x', ACROSS)  12.3 us
    all_to_all x2, starting transfers between devices, plane_exchange(): return lax.all_to_all(array, PLANE, split_axis=0, concat_axis=0, tiled=True)  9.95 us
    pallas_call x1, Pallas kernels, retain(): pl.pallas_call(retain_body, in_specs=[VMEM, HBM, HBM, VMEM, HBM], out_spe...  9.04 us
    ppermute x3, waiting for transfers between devices, ring_gather(): lax.ppermute(own, 'x', LEFT)  8.16 us
    all_to_all x2, waiting for transfers between devices, plane_exchange(): return lax.all_to_all(array, PLANE, split_axis=0, concat_axis=0, tiled=True)  7.79 us
    pallas_call x1, Pallas kernels, experts(): pl.pallas_call(expert_body, in_specs=[VMEM] * 4 + [HBM] * 6, out_shape=[r...  7.38 us
  transfers between devices with their start and end apart: 26, of which 14 were waited for; matrix products, arithmetic and copies ran while one was open for 0% of the time, Pallas kernels for 8%

profile of v1, /device:TPU:1, one launch (start us, length us, event | category | flops | bytes accessed | tf_op | source)
XLA Modules:
  0.0 180.9 jit_solution(7565897102340820372)
XLA Ops:
  0.6 1.7 prepare.1
  2.4 2.0 %collective-permute-start = (bf16[4,32,768]{2,1,0:T(8,128)(2,1)}, bf16[4,32,768]{2,1,0:T(8,128)(2,1)S(1)}, u32[]{:S(2)}, u32[]{:S(2)}) collective-permute-start(bf16[4,32,768]{2,1,0:T(8,128)(2,1)} %get-tuple-element.50.c0), channel_id=1, source_target_pairs={{0,2},{2,4},{4,6},{6,0},{1,3},{3,5},{5,7},{7,1},{8,10},{10,12},{12... | collective-permute-start | bytes 589832 | tf_op jit(solution)/shard_map/ppermute | solution.py:30
  4.4 2.5 %collective-permute-start.1 = (bf16[4,32,768]{2,1,0:T(8,128)(2,1)}, bf16[4,32,768]{2,1,0:T(8,128)(2,1)S(1)}, u32[]{:S(2)}, u32[]{:S(2)}) collective-permute-start(bf16[4,32,768]{2,1,0:T(8,128)(2,1)} %get-tuple-element.50.c0), channel_id=1, source_target_pairs={{0,4},{2,6},{4,0},{6,2},{1,5},{3,7},{5,1},{7,3},{8,12},{10,14},{12... | collective-permute-start | bytes 589832 | tf_op jit(solution)/shard_map/ppermute | solution.py:31
  6.8 1.2 collective-permute-start.2
  8.0 14.7 %all_to_all.25.x_ref.got = bf16[16,32,128]{2,1,0:T(8,128)(2,1)} all-to-all(bf16[16,32,128]{2,1,0:T(8,128)(2,1)} %get-tuple-element.49), channel_id=1, replica_groups=mesh['z'=4,'y'=4,'x'=4,'tp'=2] {'z','y'}, dimensions={0} | all-to-all | bytes 262144 | tf_op jit(solution)/shard_map/all_to_all | solution.py:403
  22.7 0.6 copy-done.8
  23.4 0.1 copy-done.9
  23.5 0.7 copy-done.10
  24.1 2.7 %project.1 = bf16[16,16,3072]{2,1,0:T(8,128)(2,1)} custom-call(bf16[16,32,128]{2,1,0:T(8,128)(2,1)} %all_to_all.25.x_ref.got, bf16[4,32,768]{2,1,0:T(8,128)(2,1)} %get-tuple-element.50.c0, bf16[4,32,768]{2,1,0:T(8,128)(2,1)} %copy-done.8, bf16[4,32,768]{2,1,0:T(8,128)(2,1)} %copy-done.9, bf16[4,32,768]{2,1,0:T(8,128)(2,1)} %copy-done.10), custom_call_target="tpu_custom_call" | custom-call | tf_op jit(solution)/shard_map/project/pallas_call | solution.py:97
  26.9 0.0 copy-start.25
  26.9 0.0 copy-start.26
  27.0 3.0 %collective-permute-start.13 = (bf16[1,2048,512]{2,1,0:T(8,128)(2,1)}, bf16[1,2048,512]{2,1,0:T(8,128)(2,1)}, u32[]{:S(2)}, u32[]{:S(2)}) collective-permute-start(bf16[1,2048,512]{2,1,0:T(8,128)(2,1)} %gate_a), channel_id=1, source_target_pairs={{0,1},{1,0},{2,3},{3,2},{4,5},{5,4},{6,7},{7,6},{8,9},{9,8},{10,11... | collective-permute-start | bytes 6291464 | tf_op jit(solution)/shard_map/ppermute | solution.py:474
  30.0 0.1 collective-permute-start.14
  30.1 0.4 collective-permute-start.15
  30.5 3.7 %all-to-all-start.1 = ((bf16[16,16,3072]{2,1,0:T(8,128)(2,1)}), bf16[16,16,3072]{2,1,0:T(8,128)(2,1)S(1)}, u32[]{:S(2)}, u32[]{:S(2)}) async-start(bf16[16,16,3072]{2,1,0:T(8,128)(2,1)} %project.1), calls=%async_computation.1 | async-start | bytes 3145728 | tf_op jit(solution)/shard_map/all_to_all | solution.py:403
  34.3 0.4 collective-permute-start.6
  34.7 0.1 collective-permute-start.3
  34.8 12.4 %collective-permute-done.3.c1 = bf16[32,768]{1,0:T(8,128)(2,1)S(1)} collective-permute-done((bf16[32,768]{1,0:T(8,128)(2,1)S(1)}, bf16[32,768]{1,0:T(8,128)(2,1)S(1)}, u32[]{:S(2)}, u32[]{:S(2)}) %collective-permute-start.3) | collective-permute-done | bytes 49184 | tf_op jit(solution)/shard_map/ppermute | solution.py:30
  47.2 4.7 %collective-permute-done.4.c2 = bf16[32,768]{1,0:T(8,128)(2,1)S(1)} collective-permute-done((bf16[32,768]{1,0:T(8,128)(2,1)S(1)}, bf16[32,768]{1,0:T(8,128)(2,1)S(1)}, u32[]{:S(2)}, u32[]{:S(2)}) %collective-permute-start.4) | collective-permute-done | bytes 49184 | tf_op jit(solution)/shard_map/ppermute | solution.py:31
  52.0 0.6 copy-done.22
  52.6 2.6 %collective-permute-done.5.c3 = bf16[32,768]{1,0:T(8,128)(2,1)} collective-permute-done((bf16[32,768]{1,0:T(8,128)(2,1)S(1)}, bf16[32,768]{1,0:T(8,128)(2,1)}, u32[]{:S(2)}, u32[]{:S(2)}) %collective-permute-start.5) | collective-permute-done | bytes 49184 | tf_op jit(solution)/shard_map/ppermute | solution.py:32
  55.2 1.8 collective-permute-start.8
  57.0 7.6 %collective-permute-done.7.c2 = bf16[96,2048]{1,0:T(8,128)(2,1)S(1)} collective-permute-done((bf16[96,2048]{1,0:T(8,128)(2,1)S(1)}, bf16[96,2048]{1,0:T(8,128)(2,1)S(1)}, u32[]{:S(2)}, u32[]{:S(2)}) %collective-permute-start.7) | collective-permute-done | bytes 393248 | tf_op jit(solution)/shard_map/ppermute | solution.py:31
  64.6 3.6 %collective-permute-start.9 = (bf16[96,2048]{1,0:T(8,128)(2,1)S(1)}, bf16[96,2048]{1,0:T(8,128)(2,1)S(1)}, u32[]{:S(2)}, u32[]{:S(2)}) collective-permute-start(bf16[96,2048]{1,0:T(8,128)(2,1)S(1)} %pad_maximum_fusion.c0), channel_id=1, source_target_pairs={{0,1},{1,0},{2,3},{3,2},{4,5},{5,4},{6,7},{7,6},{8,9},{9,8},{10,11... | collective-permute-start | bytes 1179656 | tf_op jit(solution)/shard_map/ppermute | solution.py:475
  68.2 5.5 %collective-permute-done.8.c3 = bf16[96,2048]{1,0:T(8,128)(2,1)S(1)} collective-permute-done((bf16[96,2048]{1,0:T(8,128)(2,1)S(1)}, bf16[96,2048]{1,0:T(8,128)(2,1)S(1)}, u32[]{:S(2)}, u32[]{:S(2)}) %collective-permute-start.8) | collective-permute-done | bytes 393248 | tf_op jit(solution)/shard_map/ppermute | solution.py:32
  73.8 1.6 collective-permute-start.10
  75.3 0.1 collective-permute-start.11
  75.4 1.2 collective-permute-done.10.c5
  76.7 0.4 collective-permute-start.12
  77.0 0.4 copy-done.6
  77.4 0.7 fusion
  78.1 1.2 copy-done
  79.4 9.0 %retain.1 = (f32[16,6,128,128]{3,2,1,0:T(8,128)}, bf16[16,16,768]{2,1,0:T(8,128)(2,1)}) custom-call(bf16[16,16,3072]{2,1,0:T(8,128)(2,1)} %copy-done, f32[16,128]{1,0:T(8,128)} %get-tuple-element.99.cosine_ref, f32[16,128]{1,0:T(8,128)} %get-tuple-element.98.sine_ref, bf16[768]{0:T(1024)(128)(2,1)} %gain.4, f32[16,6,128,128]{3,2,1,0:T(8,128)} %state_ref.1), custom_call_target="tpu_custom_call" | custom-call | tf_op jit(solution)/shard_map/retain/pallas_call | solution.py:189
  88.4 6.2 %all-to-all-start.2 = ((bf16[16,16,768]{2,1,0:T(8,128)(2,1)}), bf16[16,16,768]{2,1,0:T(8,128)(2,1)S(1)}, u32[]{:S(2)}, u32[]{:S(2)}) async-start(bf16[16,16,768]{2,1,0:T(8,128)(2,1)} %get-tuple-element.53), calls=%async_computation.2 | async-start | bytes 786432 | tf_op jit(solution)/shard_map/all_to_all | solution.py:403
  94.7 1.7 routing.1
  96.4 7.8 %all-to-all-done.2.kept = bf16[16,16,768]{2,1,0:T(8,128)(2,1)S(1)} async-done(((bf16[16,16,768]{2,1,0:T(8,128)(2,1)}), bf16[16,16,768]{2,1,0:T(8,128)(2,1)S(1)}, u32[]{:S(2)}, u32[]{:S(2)}) %all-to-all-start.2) | async-done | bytes 393248 | tf_op jit(solution)/shard_map/all_to_all | solution.py:403
  104.2 0.7 copy-done.7
  105.0 2.0 %mix.1 = (bf16[16,8,128]{2,1,0:T(8,128)(2,1)}, bf16[16,8,128]{2,1,0:T(8,128)(2,1)}) custom-call(bf16[16,16,768]{2,1,0:T(8,128)(2,1)} %copy-done.7, bf16[32,768]{1,0:T(8,128)(2,1)} %bitcast.7, bf16[32,768]{1,0:T(8,128)(2,1)} %copy-done.21, bf16[32,768]{1,0:T(8,128)(2,1)} %copy-done.22, bf16[32,768]{1,0:T(8,128)(2,1)} %collective-permute-done.5.c3), custom_call_target="tpu_custom_call" | custom-call | tf_op jit(solution)/shard_map/mix/pallas_call | solution.py:225
  107.0 1.5 collective-permute-start.16
  108.5 1.1 collective-permute-done.16.other
  109.5 0.6 copy-done.23
  110.1 1.8 settle.1
  111.9 15.2 %all_to_all.26.res = bf16[16,128,128]{2,1,0:T(8,128)(2,1)} all-to-all(bf16[16,128,128]{2,1,0:T(8,128)(2,1)} %settle.1), channel_id=1, replica_groups=mesh['z'=4,'y'=4,'x'=4,'tp'=2] {'z','y'}, dimensions={0} | all-to-all | bytes 1048576 | tf_op jit(solution)/shard_map/all_to_all | solution.py:403
  127.2 2.5 %spread.1 = (bf16[128,2048]{1,0:T(8,128)(2,1)}, bf16[32,2048]{1,0:T(8,128)(2,1)}, bf16[32,2048]{1,0:T(8,128)(2,1)}, bf16[32,2048]{1,0:T(8,128)(2,1)}, bf16[32,20...) custom-call(bf16[16,128,128]{2,1,0:T(8,128)(2,1)} %all_to_all.26.res, bf16[2048]{0:T(1024)(128)(2,1)} %gain.5, ...), custom_call_target="tpu_custom_call" | custom-call | tf_op jit(solution)/shard_map/spread/pallas_call | solution.py:273
  129.7 0.7 collective-permute-start.17
  130.4 2.9 %collective-permute-start.18 = (bf16[32,2048]{1,0:T(8,128)(2,1)}, bf16[32,2048]{1,0:T(8,128)(2,1)S(1)}, u32[]{:S(2)}, u32[]{:S(2)}) collective-permute-start(bf16[32,2048]{1,0:T(8,128)(2,1)} %get-tuple-element.86), channel_id=1, source_target_pairs={{0,4},{2,6},{4,0},{6,2},{1,5},{3,7},{5,1},{7,3},{8,12},{10,14},{12... | collective-permute-start | bytes 393224 | tf_op jit(solution)/shard_map/ppermute | solution.py:494
  133.2 1.7 collective-permute-done.17.a1
  134.9 3.1 %collective-permute-done.18.a2 = bf16[32,2048]{1,0:T(8,128)(2,1)S(1)} collective-permute-done((bf16[32,2048]{1,0:T(8,128)(2,1)}, bf16[32,2048]{1,0:T(8,128)(2,1)S(1)}, u32[]{:S(2)}, u32[]{:S(2)}) %collective-permute-start.18) | collective-permute-done | bytes 131104 | tf_op jit(solution)/shard_map/ppermute | solution.py:494
  138.0 0.4 collective-permute-done.19.a3
  138.5 0.2 copy-done.12
  138.7 0.4 copy-done.13
  139.1 7.4 %experts.1 = (bf16[32,2048]{1,0:T(8,128)(2,1)}, bf16[32,2048]{1,0:T(8,128)(2,1)}, bf16[32,2048]{1,0:T(8,128)(2,1)}, bf16[32,2048]{1,0:T(8,128)(2,1)}) custom-call(bf16[32,2048]{1,0:T(8,128)(2,1)} %get-tuple-element.84.a0, bf16[32,2048]{1,0:T(8,128)(2,1)} %copy-done.11, bf16[32,2048]{1,0:T(8,128)(2,1)} %copy-done.12, bf16[32,2048]{1,0:T(8,128)(2,1)} %copy-done.13, ...), custom_call_target="tpu_custom_call" | custom-call | tf_op jit(solution)/shard_map/experts/pallas_call | solution.py:362
  146.6 2.2 %collective-permute-start.20 = (bf16[32,2048]{1,0:T(8,128)(2,1)}, bf16[32,2048]{1,0:T(8,128)(2,1)S(1)}, u32[]{:S(2)}, u32[]{:S(2)}) collective-permute-start(bf16[32,2048]{1,0:T(8,128)(2,1)} %get-tuple-element.92), channel_id=1, source_target_pairs={{0,6},{2,0},{4,2},{6,4},{1,7},{3,1},{5,3},{7,5},{8,14},{10,8},{12,... | collective-permute-start | bytes 393224 | tf_op jit(solution)/shard_map/ppermute | solution.py:502
  148.8 0.7 collective-permute-start.22
  149.5 3.4 %dense_first.1.hidden = bf16[128,256]{1,0:T(8,128)(2,1)} custom-call(bf16[128,2048]{1,0:T(8,128)(2,1)} %get-tuple-element.73.plane, bf16[96,2048]{1,0:T(8,128)(2,1)} %copy-done.1, bf16[96,2048]{1,0:T(8,128)(2,1)} %copy-done.2, bf16[96,2048]{1,0:T(8,128)(2,1)} %copy-done.3, bf16[96,2048]{1,0:T(8,128)(2,1)} %copy-done.4, bf16[96,2048]{1,0:T(8,128)(2,1)} %copy-done.5, ...), custom_call_target="tpu_custom_call" | custom-call | tf_op jit(solution)/shard_map/dense_first/pallas_call | solution.py:297
  152.9 1.5 collective-permute-done.21.b2
  154.4 1.0 collective-permute-done.22.b3
  155.4 0.7 copy-done.16
  156.1 3.3 %combine.1 = bf16[16,8,2048]{2,1,0:T(8,128)(2,1)} custom-call(bf16[128,256]{1,0:T(8,128)(2,1)} %dense_first.1.hidden, bf16[96,2048]{1,0:T(8,128)(2,1)} %copy-done.1, bf16[96,2048]{1,0:T(8,128)(2,1)} %copy-done.2, bf16[96,2048]{1,0:T(8,128)(2,1)} %copy-done.3, bf16[96,2048]{1,0:T(8,128)(2,1)} %copy-done.4, bf16[96,2048]{1,0:T(8,128)(2,1)} %copy-done.5, ...), custom_call_target="tpu_custom_call" | custom-call | tf_op jit(solution)/shard_map/combine/pallas_call | solution.py:394
  159.4 17.9 %all_to_all.27 = bf16[16,8,2048]{2,1,0:T(8,128)(2,1)S(1)} all-to-all(bf16[16,8,2048]{2,1,0:T(8,128)(2,1)} %combine.1), channel_id=1, replica_groups=mesh['z'=4,'y'=4,'x'=4,'tp'=2] {'z','y'}, dimensions={0} | all-to-all | bytes 1048576 | tf_op jit(solution)/shard_map/all_to_all | solution.py:403
  177.3 0.1 convert_reduce_fusion
  177.4 2.0 %collective-permute-start.23 = (bf16[8,2048]{1,0:T(8,128)(2,1)S(1)}, bf16[8,2048]{1,0:T(8,128)(2,1)S(1)}, u32[]{:S(2)}, u32[]{:S(2)}) collective-permute-start(bf16[8,2048]{1,0:T(8,128)(2,1)S(1)} %add_convert_fusion), channel_id=1, source_target_pairs={{0,1},{1,0},{2,3},{3,2},{4,5},{5,4},{6,7},{7,6},{8,9},{9,8},{10,11... | collective-permute-start | bytes 98312 | tf_op jit(solution)/shard_map/ppermute | solution.py:510
  179.3 0.9 collective-permute-done.23
  180.2 0.6 pad_maximum_fusion.1
  (64 shorter events, 0.2 us)
Async XLA Ops:
  2.4 20.4 %collective-permute-start = (bf16[4,32,768]{2,1,0:T(8,128)(2,1)}, bf16[4,32,768]{2,1,0:T(8,128)(2,1)S(1)}, u32[]{:S(2)}, u32[]{:S(2)}) collective-permute-start(bf16[4,32,768]{2,1,0:T(8,128)(2,1)} %get-tuple-element.50.c0), channel_id=1, source_target_pairs={{0,2},{2,4},{4,6},{6,0},{1,3},{3,5},{5,7},{7,1},{8,10},{10,12},{12... | collective-permute-start | bytes 589832 | tf_op jit(solution)/shard_map/ppermute | solution.py:30
  4.4 18.3 %collective-permute-start.1 = (bf16[4,32,768]{2,1,0:T(8,128)(2,1)}, bf16[4,32,768]{2,1,0:T(8,128)(2,1)S(1)}, u32[]{:S(2)}, u32[]{:S(2)}) collective-permute-start(bf16[4,32,768]{2,1,0:T(8,128)(2,1)} %get-tuple-element.50.c0), channel_id=1, source_target_pairs={{0,4},{2,6},{4,0},{6,2},{1,5},{3,7},{5,1},{7,3},{8,12},{10,14},{12... | collective-permute-start | bytes 589832 | tf_op jit(solution)/shard_map/ppermute | solution.py:31
  6.8 15.9 %collective-permute-start.2 = (bf16[4,32,768]{2,1,0:T(8,128)(2,1)}, bf16[4,32,768]{2,1,0:T(8,128)(2,1)S(1)}, u32[]{:S(2)}, u32[]{:S(2)}) collective-permute-start(bf16[4,32,768]{2,1,0:T(8,128)(2,1)} %get-tuple-element.50.c0), channel_id=1, source_target_pairs={{0,6},{2,0},{4,2},{6,4},{1,7},{3,1},{5,3},{7,5},{8,14},{10,8},{12,... | collective-permute-start | bytes 589832 | tf_op jit(solution)/shard_map/ppermute | solution.py:32
  22.7 0.7 copy-start.8
  22.7 0.8 copy-start.9
  23.5 0.7 copy-start.10
  26.9 7.3 %copy-start.17 = (bf16[32,2048]{1,0:T(8,128)(2,1)S(1)}, bf16[32,2048]{1,0:T(8,128)(2,1)}, u32[]{:S(2)}) copy-start(bf16[32,2048]{1,0:T(8,128)(2,1)} %param.40) | copy-start | bytes 393220
  26.9 7.3 %copy-start.18 = (bf16[2048,32]{0,1:T(8,128)(2,1)S(1)}, bf16[2048,32]{0,1:T(8,128)(2,1)}, u32[]{:S(2)}) copy-start(bf16[2048,32]{0,1:T(8,128)(2,1)} %param.39) | copy-start | bytes 393220
  26.9 7.3 %copy-start.19 = (bf16[2048,32]{0,1:T(8,128)(2,1)S(1)}, bf16[2048,32]{0,1:T(8,128)(2,1)}, u32[]{:S(2)}) copy-start(bf16[2048,32]{0,1:T(8,128)(2,1)} %param.38) | copy-start | bytes 393220
  26.9 7.8 %copy-start.20 = (bf16[768,32]{0,1:T(8,128)(2,1)S(1)}, bf16[768,32]{0,1:T(8,128)(2,1)}, u32[]{:S(2)}) copy-start(bf16[768,32]{0,1:T(8,128)(2,1)} %param.31) | copy-start | bytes 147460
  26.9 48.4 %copy-start.27 = (s32[16]{0:T(128)S(1)}, s32[16]{0:T(128)}, u32[]{:S(2)}) copy-start(s32[16]{0:T(128)} %param.23) | copy-start | bytes 196
  26.9 50.5 %copy-start.25 = (f32[128]{0:T(128)S(1)}, f32[128]{0:T(128)}, u32[]{:S(2)}) copy-start(f32[128]{0:T(128)} %constant.30) | copy-start | bytes 1540
  26.9 50.5 %copy-start.26 = (f32[128]{0:T(128)S(1)}, f32[128]{0:T(128)}, u32[]{:S(2)}) copy-start(f32[128]{0:T(128)} %constant.31) | copy-start | bytes 1540
  27.0 77.3 %collective-permute-start.13 = (bf16[1,2048,512]{2,1,0:T(8,128)(2,1)}, bf16[1,2048,512]{2,1,0:T(8,128)(2,1)}, u32[]{:S(2)}, u32[]{:S(2)}) collective-permute-start(bf16[1,2048,512]{2,1,0:T(8,128)(2,1)} %gate_a), channel_id=1, source_target_pairs={{0,1},{1,0},{2,3},{3,2},{4,5},{5,4},{6,7},{7,6},{8,9},{9,8},{10,11... | collective-permute-start | bytes 6291464 | tf_op jit(solution)/shard_map/ppermute | solution.py:474
  30.0 74.2 %collective-permute-start.14 = (bf16[1,2048,512]{2,1,0:T(8,128)(2,1)}, bf16[1,2048,512]{2,1,0:T(8,128)(2,1)}, u32[]{:S(2)}, u32[]{:S(2)}) collective-permute-start(bf16[1,2048,512]{2,1,0:T(8,128)(2,1)} %up_a), channel_id=1, source_target_pairs={{0,1},{1,0},{2,3},{3,2},{4,5},{5,4},{6,7},{7,6},{8,9},{9,8},{10,11... | collective-permute-start | bytes 6291464 | tf_op jit(solution)/shard_map/ppermute | solution.py:474
  30.1 74.2 %collective-permute-start.15 = (bf16[1,512,2048]{2,1,0:T(8,128)(2,1)}, bf16[1,512,2048]{2,1,0:T(8,128)(2,1)}, u32[]{:S(2)}, u32[]{:S(2)}) collective-permute-start(bf16[1,512,2048]{2,1,0:T(8,128)(2,1)} %down_a), channel_id=1, source_target_pairs={{0,1},{1,0},{2,3},{3,2},{4,5},{5,4},{6,7},{7,6},{8,9},{9,8},{10,11... | collective-permute-start | bytes 6291464 | tf_op jit(solution)/shard_map/ppermute | solution.py:474
  30.5 47.6 %all-to-all-start.1 = ((bf16[16,16,3072]{2,1,0:T(8,128)(2,1)}), bf16[16,16,3072]{2,1,0:T(8,128)(2,1)S(1)}, u32[]{:S(2)}, u32[]{:S(2)}) async-start(bf16[16,16,3072]{2,1,0:T(8,128)(2,1)} %project.1), calls=%async_computation.1 | async-start | bytes 3145728 | tf_op jit(solution)/shard_map/all_to_all | solution.py:403
  34.3 112.2 %copy-start.1 = (bf16[96,2048]{1,0:T(8,128)(2,1)}, bf16[96,2048]{1,0:T(8,128)(2,1)S(1)}, u32[]{:S(2)}) copy-start(bf16[96,2048]{1,0:T(8,128)(2,1)S(1)} %pad_maximum_fusion.c0) | copy-start | bytes 1179652
  34.3 20.9 %collective-permute-start.6 = (bf16[96,2048]{1,0:T(8,128)(2,1)S(1)}, bf16[96,2048]{1,0:T(8,128)(2,1)S(1)}, u32[]{:S(2)}, u32[]{:S(2)}) collective-permute-start(bf16[96,2048]{1,0:T(8,128)(2,1)S(1)} %pad_maximum_fusion.c0), channel_id=1, source_target_pairs={{0,2},{2,4},{4,6},{6,0},{1,3},{3,5},{5,7},{7,1},{8,10},{10,12},{12... | collective-permute-start | bytes 1179656 | tf_op jit(solution)/shard_map/ppermute | solution.py:30
  34.7 12.5 %collective-permute-start.3 = (bf16[32,768]{1,0:T(8,128)(2,1)S(1)}, bf16[32,768]{1,0:T(8,128)(2,1)S(1)}, u32[]{:S(2)}, u32[]{:S(2)}) collective-permute-start(bf16[32,768]{1,0:T(8,128)(2,1)S(1)} %bitcast.8), channel_id=1, source_target_pairs={{0,2},{2,4},{4,6},{6,0},{1,3},{3,5},{5,7},{7,1},{8,10},{10,12},{12... | collective-permute-start | bytes 147464 | tf_op jit(solution)/shard_map/ppermute | solution.py:30
  47.2 4.7 %copy-start.21 = (bf16[32,768]{1,0:T(8,128)(2,1)}, bf16[32,768]{1,0:T(8,128)(2,1)S(1)}, u32[]{:S(2)}) copy-start(bf16[32,768]{1,0:T(8,128)(2,1)S(1)} %collective-permute-done.3.c1) | copy-start | bytes 147460
  47.2 4.7 %collective-permute-start.4 = (bf16[32,768]{1,0:T(8,128)(2,1)S(1)}, bf16[32,768]{1,0:T(8,128)(2,1)S(1)}, u32[]{:S(2)}, u32[]{:S(2)}) collective-permute-start(bf16[32,768]{1,0:T(8,128)(2,1)S(1)} %bitcast.9), channel_id=1, source_target_pairs={{0,4},{2,6},{4,0},{6,2},{1,5},{3,7},{5,1},{7,3},{8,12},{10,14},{12... | collective-permute-start | bytes 147464 | tf_op jit(solution)/shard_map/ppermute | solution.py:31
  51.9 0.6 copy-start.22
  51.9 3.2 %collective-permute-start.5 = (bf16[32,768]{1,0:T(8,128)(2,1)S(1)}, bf16[32,768]{1,0:T(8,128)(2,1)}, u32[]{:S(2)}, u32[]{:S(2)}) collective-permute-start(bf16[32,768]{1,0:T(8,128)(2,1)S(1)} %bitcast.10), channel_id=1, source_target_pairs={{0,6},{2,0},{4,2},{6,4},{1,7},{3,1},{5,3},{7,5},{8,14},{10,8},{12,... | collective-permute-start | bytes 147464 | tf_op jit(solution)/shard_map/ppermute | solution.py:32
  55.2 9.4 %collective-permute-start.7 = (bf16[96,2048]{1,0:T(8,128)(2,1)S(1)}, bf16[96,2048]{1,0:T(8,128)(2,1)S(1)}, u32[]{:S(2)}, u32[]{:S(2)}) collective-permute-start(bf16[96,2048]{1,0:T(8,128)(2,1)S(1)} %pad_maximum_fusion.c0), channel_id=1, source_target_pairs={{0,4},{2,6},{4,0},{6,2},{1,5},{3,7},{5,1},{7,3},{8,12},{10,14},{12... | collective-permute-start | bytes 1179656 | tf_op jit(solution)/shard_map/ppermute | solution.py:31
  55.2 91.3 %copy-start.2 = (bf16[96,2048]{1,0:T(8,128)(2,1)}, bf16[96,2048]{1,0:T(8,128)(2,1)S(1)}, u32[]{:S(2)}) copy-start(bf16[96,2048]{1,0:T(8,128)(2,1)S(1)} %collective-permute-done.6.c1) | copy-start | bytes 1179652
  55.2 18.6 %collective-permute-start.8 = (bf16[96,2048]{1,0:T(8,128)(2,1)S(1)}, bf16[96,2048]{1,0:T(8,128)(2,1)S(1)}, u32[]{:S(2)}, u32[]{:S(2)}) collective-permute-start(bf16[96,2048]{1,0:T(8,128)(2,1)S(1)} %pad_maximum_fusion.c0), channel_id=1, source_target_pairs={{0,6},{2,0},{4,2},{6,4},{1,7},{3,1},{5,3},{7,5},{8,14},{10,8},{12,... | collective-permute-start | bytes 1179656 | tf_op jit(solution)/shard_map/ppermute | solution.py:32
  64.6 82.0 %copy-start.3 = (bf16[96,2048]{1,0:T(8,128)(2,1)}, bf16[96,2048]{1,0:T(8,128)(2,1)S(1)}, u32[]{:S(2)}) copy-start(bf16[96,2048]{1,0:T(8,128)(2,1)S(1)} %collective-permute-done.7.c2) | copy-start | bytes 1179652
  64.6 10.7 %collective-permute-start.9 = (bf16[96,2048]{1,0:T(8,128)(2,1)S(1)}, bf16[96,2048]{1,0:T(8,128)(2,1)S(1)}, u32[]{:S(2)}, u32[]{:S(2)}) collective-permute-start(bf16[96,2048]{1,0:T(8,128)(2,1)S(1)} %pad_maximum_fusion.c0), channel_id=1, source_target_pairs={{0,1},{1,0},{2,3},{3,2},{4,5},{5,4},{6,7},{7,6},{8,9},{9,8},{10,11... | collective-permute-start | bytes 1179656 | tf_op jit(solution)/shard_map/ppermute | solution.py:475
  73.8 72.8 %copy-start.4 = (bf16[96,2048]{1,0:T(8,128)(2,1)}, bf16[96,2048]{1,0:T(8,128)(2,1)S(1)}, u32[]{:S(2)}) copy-start(bf16[96,2048]{1,0:T(8,128)(2,1)S(1)} %collective-permute-done.8.c3) | copy-start | bytes 1179652
  73.8 2.9 %collective-permute-start.10 = (bf16[96,2048]{1,0:T(8,128)(2,1)S(1)}, bf16[96,2048]{1,0:T(8,128)(2,1)S(1)}, u32[]{:S(2)}, u32[]{:S(2)}) collective-permute-start(bf16[96,2048]{1,0:T(8,128)(2,1)S(1)} %collective-permute-done.6.c1), channel_id=1, source_target_pairs={{0,1},{1,0},{2,3},{3,2},{4,5},{5,4},{6,7},{7,6},{8,9},{9,8},{10,11... | collective-permute-start | bytes 1179656 | tf_op jit(solution)/shard_map/ppermute | solution.py:475
  75.3 71.2 %copy-start.5 = (bf16[96,2048]{1,0:T(8,128)(2,1)}, bf16[96,2048]{1,0:T(8,128)(2,1)S(1)}, u32[]{:S(2)}) copy-start(bf16[96,2048]{1,0:T(8,128)(2,1)S(1)} %collective-permute-done.9.c4) | copy-start | bytes 1179652
  75.3 21.1 %collective-permute-start.11 = (bf16[96,2048]{1,0:T(8,128)(2,1)S(1)}, bf16[96,2048]{1,0:T(8,128)(2,1)}, u32[]{:S(2)}, u32[]{:S(2)}) collective-permute-start(bf16[96,2048]{1,0:T(8,128)(2,1)S(1)} %collective-permute-done.7.c2), channel_id=1, source_target_pairs={{0,1},{1,0},{2,3},{3,2},{4,5},{5,4},{6,7},{7,6},{8,9},{9,8},{10,11... | collective-permute-start | bytes 1179656 | tf_op jit(solution)/shard_map/ppermute | solution.py:475
  76.7 0.7 copy-start.6
  76.7 19.8 %collective-permute-start.12 = (bf16[96,2048]{1,0:T(8,128)(2,1)S(1)}, bf16[96,2048]{1,0:T(8,128)(2,1)}, u32[]{:S(2)}, u32[]{:S(2)}) collective-permute-start(bf16[96,2048]{1,0:T(8,128)(2,1)S(1)} %collective-permute-done.8.c3), channel_id=1, source_target_pairs={{0,1},{1,0},{2,3},{3,2},{4,5},{5,4},{6,7},{7,6},{8,9},{9,8},{10,11... | collective-permute-start | bytes 1179656 | tf_op jit(solution)/shard_map/ppermute | solution.py:475
  78.1 1.2 copy-start
  88.4 15.8 %all-to-all-start.2 = ((bf16[16,16,768]{2,1,0:T(8,128)(2,1)}), bf16[16,16,768]{2,1,0:T(8,128)(2,1)S(1)}, u32[]{:S(2)}, u32[]{:S(2)}) async-start(bf16[16,16,768]{2,1,0:T(8,128)(2,1)} %get-tuple-element.53), calls=%async_computation.2 | async-start | bytes 786432 | tf_op jit(solution)/shard_map/all_to_all | solution.py:403
  104.2 0.8 copy-start.7
  107.0 2.6 %collective-permute-start.16 = (bf16[16,8,128]{2,1,0:T(8,128)(2,1)}, bf16[16,8,128]{2,1,0:T(8,128)(2,1)S(1)}, u32[]{:S(2)}, u32[]{:S(2)}) collective-permute-start(bf16[16,8,128]{2,1,0:T(8,128)(2,1)} %get-tuple-element.70), channel_id=1, source_target_pairs={{0,1},{1,0},{2,3},{3,2},{4,5},{5,4},{6,7},{7,6},{8,9},{9,8},{10,11... | collective-permute-start | bytes 98312 | tf_op jit(solution)/shard_map/ppermute | solution.py:487
  109.5 0.6 copy-start.23
  129.7 5.2 %collective-permute-start.17 = (bf16[32,2048]{1,0:T(8,128)(2,1)}, bf16[32,2048]{1,0:T(8,128)(2,1)S(1)}, u32[]{:S(2)}, u32[]{:S(2)}) collective-permute-start(bf16[32,2048]{1,0:T(8,128)(2,1)} %get-tuple-element.85), channel_id=1, source_target_pairs={{0,2},{2,4},{4,6},{6,0},{1,3},{3,5},{5,7},{7,1},{8,10},{10,12},{12... | collective-permute-start | bytes 393224 | tf_op jit(solution)/shard_map/ppermute | solution.py:493
  130.4 7.7 %collective-permute-start.18 = (bf16[32,2048]{1,0:T(8,128)(2,1)}, bf16[32,2048]{1,0:T(8,128)(2,1)S(1)}, u32[]{:S(2)}, u32[]{:S(2)}) collective-permute-start(bf16[32,2048]{1,0:T(8,128)(2,1)} %get-tuple-element.86), channel_id=1, source_target_pairs={{0,4},{2,6},{4,0},{6,2},{1,5},{3,7},{5,1},{7,3},{8,12},{10,14},{12... | collective-permute-start | bytes 393224 | tf_op jit(solution)/shard_map/ppermute | solution.py:494
  133.2 5.2 %collective-permute-start.19 = (bf16[32,2048]{1,0:T(8,128)(2,1)}, bf16[32,2048]{1,0:T(8,128)(2,1)S(1)}, u32[]{:S(2)}, u32[]{:S(2)}) collective-permute-start(bf16[32,2048]{1,0:T(8,128)(2,1)} %get-tuple-element.87), channel_id=1, source_target_pairs={{0,6},{2,0},{4,2},{6,4},{1,7},{3,1},{5,3},{7,5},{8,14},{10,8},{12,... | collective-permute-start | bytes 393224 | tf_op jit(solution)/shard_map/ppermute | solution.py:495
  134.9 3.5 %copy-start.11 = (bf16[32,2048]{1,0:T(8,128)(2,1)}, bf16[32,2048]{1,0:T(8,128)(2,1)S(1)}, u32[]{:S(2)}) copy-start(bf16[32,2048]{1,0:T(8,128)(2,1)S(1)} %collective-permute-done.17.a1) | copy-start | bytes 393220
  138.0 0.7 copy-start.12
  138.5 0.7 copy-start.13
  146.6 6.3 %collective-permute-start.20 = (bf16[32,2048]{1,0:T(8,128)(2,1)}, bf16[32,2048]{1,0:T(8,128)(2,1)S(1)}, u32[]{:S(2)}, u32[]{:S(2)}) collective-permute-start(bf16[32,2048]{1,0:T(8,128)(2,1)} %get-tuple-element.92), channel_id=1, source_target_pairs={{0,6},{2,0},{4,2},{6,4},{1,7},{3,1},{5,3},{7,5},{8,14},{10,8},{12,... | collective-permute-start | bytes 393224 | tf_op jit(solution)/shard_map/ppermute | solution.py:502
  148.8 5.6 %collective-permute-start.21 = (bf16[32,2048]{1,0:T(8,128)(2,1)}, bf16[32,2048]{1,0:T(8,128)(2,1)S(1)}, u32[]{:S(2)}, u32[]{:S(2)}) collective-permute-start(bf16[32,2048]{1,0:T(8,128)(2,1)} %get-tuple-element.93), channel_id=1, source_target_pairs={{0,4},{2,6},{4,0},{6,2},{1,5},{3,7},{5,1},{7,3},{8,12},{10,14},{12... | collective-permute-start | bytes 393224 | tf_op jit(solution)/shard_map/ppermute | solution.py:503
  148.8 6.6 %collective-permute-start.22 = (bf16[32,2048]{1,0:T(8,128)(2,1)}, bf16[32,2048]{1,0:T(8,128)(2,1)S(1)}, u32[]{:S(2)}, u32[]{:S(2)}) collective-permute-start(bf16[32,2048]{1,0:T(8,128)(2,1)} %get-tuple-element.94), channel_id=1, source_target_pairs={{0,2},{2,4},{4,6},{6,0},{1,3},{3,5},{5,7},{7,1},{8,10},{10,12},{12... | collective-permute-start | bytes 393224 | tf_op jit(solution)/shard_map/ppermute | solution.py:504
  152.9 2.5 %copy-start.14 = (bf16[32,2048]{1,0:T(8,128)(2,1)}, bf16[32,2048]{1,0:T(8,128)(2,1)S(1)}, u32[]{:S(2)}) copy-start(bf16[32,2048]{1,0:T(8,128)(2,1)S(1)} %collective-permute-done.20.b1) | copy-start | bytes 393220
  154.4 1.0 copy-start.15
  155.4 0.7 copy-start.16
  156.1 21.3 %copy-start.24 = (bf16[8,2048]{1,0:T(8,128)(2,1)S(1)}, bf16[8,2048]{1,0:T(8,128)(2,1)}, u32[]{:S(2)}) copy-start(bf16[8,2048]{1,0:T(8,128)(2,1)} %get-tuple-element.72) | copy-start | bytes 98308
  177.4 2.8 %collective-permute-start.23 = (bf16[8,2048]{1,0:T(8,128)(2,1)S(1)}, bf16[8,2048]{1,0:T(8,128)(2,1)S(1)}, u32[]{:S(2)}, u32[]{:S(2)}) collective-permute-start(bf16[8,2048]{1,0:T(8,128)(2,1)S(1)} %add_convert_fusion), channel_id=1, source_target_pairs={{0,1},{1,0},{2,3},{3,2},{4,5},{5,4},{6,7},{7,6},{8,9},{9,8},{10,11... | collective-permute-start | bytes 98312 | tf_op jit(solution)/shard_map/ppermute | solution.py:510

commit v2 on v1

--- a/solution.py
+++ b/solution.py
@@ -104,6 +104,7 @@
             pltpu.VMEM((16, 16, 3072), BF16),
             pltpu.SemaphoreType.DMA((4,)),
         ],
+        compiler_params=pltpu.CompilerParams(vmem_limit_bytes=12 * 2**20),
         name="project",
     )(got, *chunks)
 
@@ -115,33 +116,44 @@
 GAMMA = [float(np.exp(np.log1p(-(2.0 ** (-5.0 - 5.0 * h / (HEADS - 1)))))) for h in range(HEADS)]
 
 
-def retain_body(
-    parts, cosine_ref, sine_ref, gain, state_ref, new_state, sent,
-    buf, turns, queries_keys, values, gates, readouts, sems,
+def gammas():
+    upper = lax.axis_index("tp") == 1
+    return [jnp.where(upper, GAMMA[h + 6], GAMMA[h]).astype(F32) for h in range(6)]
+
+
+def as_columns(row):
+    return jnp.transpose(jnp.broadcast_to(row, (128, 128)))
+
+
+def some_rows(i):
+    return pl.ds(i * PER_STEP, PER_STEP)
+
+
+def recall_body(
+    parts, cosine_ref, sine_ref, gain, state_ref, sent, keys, values,
+    buf, turns, queries, gates, readouts, sems,
 ):
     fetch_turns = [
-        pltpu.make_async_copy(cosine_ref, turns.at[0], sems.at[2 * STEPS]),
-        pltpu.make_async_copy(sine_ref, turns.at[1], sems.at[2 * STEPS + 1]),
+        pltpu.make_async_copy(cosine_ref, turns.at[0], sems.at[STEPS]),
+        pltpu.make_async_copy(sine_ref, turns.at[1], sems.at[STEPS + 1]),
     ]
     for c in fetch_turns:
         c.start()
-    upper = lax.axis_index("tp") == 1
-    gamma = [jnp.where(upper, GAMMA[h + 6], GAMMA[h]).astype(F32) for h in range(6)]
-
-    def rows(i):
-        return pl.ds(i * PER_STEP, PER_STEP)
 
     def fetch(i):
-        return pltpu.make_async_copy(state_ref.at[rows(i)], buf.at[rows(i)], sems.at[i])
-
-    def store(i):
-        return pltpu.make_async_copy(buf.at[rows(i)], new_state.at[rows(i)], sems.at[STEPS + i])
+        return pltpu.make_async_copy(
+            state_ref.at[some_rows(i)], buf.at[some_rows(i)], sems.at[i]
+        )
 
     for i in range(STEPS):
         fetch(i).start()
+    gamma = gammas()
     for c in fetch_turns:
         c.wait()
     cos_v, sin_v = turns[0], turns[1]
+    keys[...] = jnp.zeros((16, 8, 128), F32)
+    values[...] = jnp.zeros((16, 8, 128), F32)
+    added = []
     for h in range(6):
         def total(which):
             at = which * 768 + h * 128
@@ -151,60 +163,101 @@
             return acc.astype(BF16).astype(F32)
 
         q, k, v, g = (total(i) for i in range(4))
-        queries_keys[:, h, :] = q * cos_v + pltpu.roll(q, 64, 1) * sin_v
-        queries_keys[:, 8 + h, :] = (k * cos_v + pltpu.roll(k, 64, 1) * sin_v) * (128.0 ** -0.5)
+        query = q * cos_v + pltpu.roll(q, 64, 1) * sin_v
+        key = (k * cos_v + pltpu.roll(k, 64, 1) * sin_v) * (128.0 ** -0.5)
+        queries[:, h, :] = gamma[h] * query
+        keys[:, h, :] = key
         values[:, h, :] = v
+        added.append(jnp.sum(query * key, axis=-1, keepdims=True) * v)
         gates[:, h * 128 : (h + 1) * 128] = g * jax.nn.sigmoid(g)
 
     def some(i, carry):
         fetch(i).wait()
         for j in range(PER_STEP):
             t = i * PER_STEP + j
-            cols = jnp.transpose(queries_keys[t])
             for h in range(6):
-                q_col = cols[:, h : h + 1]
-                k_col = cols[:, 8 + h : 9 + h]
-                v_row = values[t, h : h + 1, :]
-                fresh = gamma[h] * buf[t, h] + k_col * v_row
-                buf[t, h] = fresh
-                readouts[t, h : h + 1, :] = jnp.sum(q_col * fresh, axis=0, keepdims=True)
-        store(i).start()
+                q_full = as_columns(queries[t, h : h + 1, :])
+                readouts[t, h : h + 1, :] = jnp.sum(q_full * buf[t, h], axis=0, keepdims=True)
         return carry
 
     lax.fori_loop(0, STEPS, some, 0)
     gains = gain[...].astype(F32).reshape(1, 768)
     for h in range(6):
         at = slice(h * 128, (h + 1) * 128)
-        r = readouts[:, h, :]
+        r = readouts[:, h, :] + added[h]
         centred = r - jnp.mean(r, axis=-1, keepdims=True)
         unit = centred * lax.rsqrt(jnp.mean(centred * centred, axis=-1, keepdims=True) + EPS)
         kept = (unit * gains[:, at] * gates[:, at]).astype(BF16)
         for s in range(16):
             sent[s, :, at] = kept
-    for i in range(STEPS):
-        store(i).wait()
-
-
-def retain(parts, cosine, sine, gain, state):
-    return pl.pallas_call(
-        retain_body,
+
+
+def recall(parts, cosine, sine, gain, state):
+    return pl.pallas_call(
+        recall_body,
         in_specs=[VMEM, HBM, HBM, VMEM, HBM],
-        out_specs=[HBM, VMEM],
+        out_specs=[VMEM] * 3,
         out_shape=[
-            jax.ShapeDtypeStruct((16, 6, 128, 128), F32),
             jax.ShapeDtypeStruct((16, 16, 768), BF16),
+            jax.ShapeDtypeStruct((16, 8, 128), F32),
+            jax.ShapeDtypeStruct((16, 8, 128), F32),
         ],
         scratch_shapes=[
             pltpu.VMEM((16, 6, 128, 128), F32),
             pltpu.VMEM((2, 16, 128), F32),
-            pltpu.VMEM((16, 16, 128), F32),
             pltpu.VMEM((16, 8, 128), F32),
             pltpu.VMEM((16, 768), F32),
             pltpu.VMEM((16, 8, 128), F32),
-            pltpu.SemaphoreType.DMA((2 * STEPS + 2,)),
-        ],
-        name="retain",
+            pltpu.SemaphoreType.DMA((STEPS + 2,)),
+        ],
+        compiler_params=pltpu.CompilerParams(vmem_limit_bytes=57 * 2**20),
+        name="recall",
     )(parts, cosine, sine, gain, state)
+
+
+def renew_body(keys, values, state_ref, new_state, buf, sems):
+    def fetch(i):
+        return pltpu.make_async_copy(
+            state_ref.at[some_rows(i)], buf.at[some_rows(i)], sems.at[i]
+        )
+
+    def store(i):
+        return pltpu.make_async_copy(
+            buf.at[some_rows(i)], new_state.at[some_rows(i)], sems.at[STEPS + i]
+        )
+
+    for i in range(STEPS):
+        fetch(i).start()
+    gamma = gammas()
+
+    def some(i, carry):
+        fetch(i).wait()
+        for j in range(PER_STEP):
+            t = i * PER_STEP + j
+            for h in range(6):
+                k_full = as_columns(keys[t, h : h + 1, :])
+                buf[t, h] = gamma[h] * buf[t, h] + k_full * values[t, h : h + 1, :]
+        store(i).start()
+        return carry
+
+    lax.fori_loop(0, STEPS, some, 0)
+    for i in range(STEPS):
+        store(i).wait()
+
+
+def renew(keys, values, state):
+    return pl.pallas_call(
+        renew_body,
+        in_specs=[VMEM, VMEM, HBM],
+        out_specs=HBM,
+        out_shape=jax.ShapeDtypeStruct((16, 6, 128, 128), F32),
+        scratch_shapes=[
+            pltpu.VMEM((16, 6, 128, 128), F32),
+            pltpu.SemaphoreType.DMA((2 * STEPS,)),
+        ],
+        compiler_params=pltpu.CompilerParams(vmem_limit_bytes=57 * 2**20),
+        name="renew",
+    )(keys, values, state)
 
 
 def mix_body(kept, c0, c1, c2, c3, keep, give, wide, mixed):
@@ -227,6 +280,7 @@
         in_specs=[VMEM] * 5,
         out_shape=[half, half],
         scratch_shapes=[pltpu.VMEM((128, 768), BF16), pltpu.VMEM((16, 16, 128), F32)],
+        compiler_params=pltpu.CompilerParams(vmem_limit_bytes=6 * 2**20),
         name="mix",
     )(kept, *chunks)
 
@@ -242,6 +296,7 @@
     return pl.pallas_call(
         settle_body,
         out_shape=jax.ShapeDtypeStruct((16, 128, 128), BF16),
+        compiler_params=pltpu.CompilerParams(vmem_limit_bytes=4 * 2**20),
         name="settle",
     )(mine, other, got)
 
@@ -278,6 +333,7 @@
             jax.ShapeDtypeStruct((128, 1), F32),
             jax.ShapeDtypeStruct((8, D), BF16),
         ],
+        compiler_params=pltpu.CompilerParams(vmem_limit_bytes=10 * 2**20),
         name="spread",
     )(res, gain, branch, pick)
 
@@ -298,61 +354,25 @@
         dense_body,
         out_shape=jax.ShapeDtypeStruct((128, 256), BF16),
         scratch_shapes=[pltpu.VMEM((256, D), BF16), pltpu.VMEM((256, D), BF16)],
+        compiler_params=pltpu.CompilerParams(vmem_limit_bytes=12 * 2**20),
         name="dense_first",
     )(plane, *chunks)
 
 
-CUT = 4
-
-
 def expert_body(
-    a0, a1, a2, a3, gate_a, gate_b, up_a, up_b, down_a, down_b, r0, r1, r2, r3,
-    rows, gate, up, down, sems,
+    a0, a1, a2, a3, gate_a, gate_b, up_a, up_b, down_a, down_b, r0, r1, r2, r3, rows
 ):
-    halves = []
-    for w, (g_ref, u_ref, d_ref) in enumerate(((gate_a, up_a, down_a), (gate_b, up_b, down_b))):
-        base = w * 3 * CUT
-        gu, dn = [], []
-        for i in range(CUT):
-            n, m = D // CUT, 512 // CUT
-            at, low = pl.ds(i * n, n), pl.ds(i * m, m)
-            gu.append((
-                pltpu.make_async_copy(g_ref.at[0, at], gate.at[w, at], sems.at[base + i]),
-                pltpu.make_async_copy(u_ref.at[0, at], up.at[w, at], sems.at[base + CUT + i]),
-            ))
-            dn.append(
-                pltpu.make_async_copy(d_ref.at[0, low], down.at[w, low], sems.at[base + 2 * CUT + i])
-            )
-        halves.append((gu, dn))
-    for gu, _ in halves:
-        for g, u in gu:
-            g.start()
-            u.start()
-    for _, dn in halves:
-        for d in dn:
-            d.start()
     for k, a in enumerate((a0, a1, a2, a3)):
         rows[k * 32 : (k + 1) * 32, :] = a[...]
-    n = D // CUT
     hidden = []
-    for w, (gu, _) in enumerate(halves):
-        g_sum = u_sum = None
-        for i, (g, u) in enumerate(gu):
-            at = slice(i * n, (i + 1) * n)
-            g.wait()
-            g_part = jnp.dot(rows[:, at], gate[w, at, :], preferred_element_type=F32)
-            u.wait()
-            u_part = jnp.dot(rows[:, at], up[w, at, :], preferred_element_type=F32)
-            g_sum = g_part if g_sum is None else g_sum + g_part
-            u_sum = u_part if u_sum is None else u_sum + u_part
-        hidden.append((g_sum * jax.nn.sigmoid(g_sum) * u_sum).astype(BF16))
-    for _, dn in halves:
-        for d in dn:
-            d.wait()
+    for gate, up in ((gate_a, up_a), (gate_b, up_b)):
+        g = jnp.dot(rows[...], gate[0], preferred_element_type=F32)
+        u = jnp.dot(rows[...], up[0], preferred_element_type=F32)
+        hidden.append((g * jax.nn.sigmoid(g) * u).astype(BF16))
     for j in range(4):
         at = slice(j * 512, (j + 1) * 512)
-        out = jnp.dot(hidden[0], down[0, :, at], preferred_element_type=F32)
-        out = (out + jnp.dot(hidden[1], down[1, :, at], preferred_element_type=F32)).astype(BF16)
+        out = jnp.dot(hidden[0], down_a[0, :, at], preferred_element_type=F32)
+        out = (out + jnp.dot(hidden[1], down_b[0, :, at], preferred_element_type=F32)).astype(BF16)
         for k, r in enumerate((r0, r1, r2, r3)):
             r[:, at] = out[k * 32 : (k + 1) * 32, :]
 
@@ -361,15 +381,10 @@
     rows = jax.ShapeDtypeStruct((32, D), BF16)
     return pl.pallas_call(
         expert_body,
-        in_specs=[VMEM] * 4 + [HBM] * 6,
+        in_specs=[VMEM] * 10,
         out_shape=[rows] * 4,
-        scratch_shapes=[
-            pltpu.VMEM((128, D), BF16),
-            pltpu.VMEM((2, D, 512), BF16),
-            pltpu.VMEM((2, D, 512), BF16),
-            pltpu.VMEM((2, 512, D), BF16),
-            pltpu.SemaphoreType.DMA((6 * CUT,)),
-        ],
+        scratch_shapes=[pltpu.VMEM((128, D), BF16)],
+        compiler_params=pltpu.CompilerParams(vmem_limit_bytes=24 * 2**20),
         name="experts",
     )(*arrived, *weights)
 
@@ -395,8 +410,35 @@
         combine_body,
         out_shape=jax.ShapeDtypeStruct((16, 8, D), BF16),
         scratch_shapes=[pltpu.VMEM((256, D), BF16), pltpu.VMEM((256, D), BF16)],
+        compiler_params=pltpu.CompilerParams(vmem_limit_bytes=12 * 2**20),
         name="combine",
     )(hidden, *chunks, opening, weigh, *back)
+
+
+def hoist_body(*refs):
+    n = len(refs) // 2
+    ins, outs, sems = refs[:n], refs[n : 2 * n], refs[2 * n]
+    moves = [
+        pltpu.make_async_copy(a.at[0, half], b.at[0, half], sems.at[2 * i + j])
+        for i, (a, b) in enumerate(zip(ins, outs))
+        for j, half in enumerate((pl.ds(0, a.shape[1] // 2), pl.ds(a.shape[1] // 2, a.shape[1] // 2)))
+    ]
+    for m in moves:
+        m.start()
+    for m in moves:
+        m.wait()
+
+
+def hoist(*arrays):
+    return pl.pallas_call(
+        hoist_body,
+        in_specs=[HBM] * len(arrays),
+        out_specs=[VMEM] * len(arrays),
+        out_shape=[jax.ShapeDtypeStruct(a.shape, a.dtype) for a in arrays],
+        scratch_shapes=[pltpu.SemaphoreType.DMA((2 * len(arrays),))],
+        compiler_params=pltpu.CompilerParams(vmem_limit_bytes=40 * 2**20),
+        name="hoist",
+    )(*arrays)
 
 
 def plane_exchange(array):
@@ -440,6 +482,7 @@
             jax.ShapeDtypeStruct((128, 128), BF16),
             jax.ShapeDtypeStruct((256, 128), BF16),
         ],
+        compiler_params=pltpu.CompilerParams(vmem_limit_bytes=4 * 2**20),
         name="routing",
     )(got)
 
@@ -457,28 +500,24 @@
     chunks = ring_gather(w4)
     got = plane_exchange(sent)
 
+    angles = positions.astype(F32)[:, None] * FREQUENCY[None, :]
+    cosine = jnp.cos(angles)
+    sine = jnp.sin(angles) * TURN[None, :]
+    dense = jnp.concatenate([dense_gate.T, dense_up.T, dense_down], axis=0)
     partial = project(got, chunks)
-    partial, got, positions, w_out, dense_gate, dense_up, dense_down, expert_own = (
-        lax.optimization_barrier(
-            (
-                partial, got, positions, w_out, dense_gate, dense_up, dense_down,
-                (exp_gate, exp_up, exp_down),
-            )
-        )
-    )
+    partial, got, cosine, sine, dense = lax.optimization_barrier(
+        (partial, got, cosine, sine, dense)
+    )
+    expert_own = (exp_gate, exp_up, exp_down)
     parts = plane_exchange(partial)
 
     out_chunks = ring_gather(w_out.T)
-    dense = jnp.concatenate([dense_gate.T, dense_up.T, dense_down], axis=0)
     dense_chunks = ring_gather(dense)
     expert_other = tuple(lax.ppermute(w, "tp", SWAP) for w in expert_own)
     dense_chunks = dense_chunks + tuple(lax.ppermute(c, "tp", SWAP) for c in dense_chunks)
     pick, weigh = routing(got)
 
-    angles = positions.astype(F32)[:, None] * FREQUENCY[None, :]
-    cosine = jnp.cos(angles)
-    sine = jnp.sin(angles) * TURN[None, :]
-    new_state, kept = retain(parts, cosine, sine, head_gain, ret_state)
+    kept, keys, values = recall(parts, cosine, sine, head_gain, ret_state)
     kept = plane_exchange(kept)
     kept, out_chunks, dense_chunks, expert_other, pick, weigh = lax.optimization_barrier(
         (kept, out_chunks, dense_chunks, expert_other, pick, weigh)
@@ -486,6 +525,7 @@
     keep, give = mix(kept, out_chunks)
     settled = settle(keep, lax.ppermute(give, "tp", SWAP), got)
     res = plane_exchange(settled)
+    new_state = renew(keys, values, ret_state)
 
     plane, s0, s1, s2, s3, opening, own_res = spread(res, norm_ffn, branch_gate, pick)
     arrived = (
@@ -496,6 +536,7 @@
     )
     hidden = dense_first(plane, dense_chunks)
     weights = tuple(w for pair in zip(expert_own, expert_other) for w in pair)
+    weights = hoist(*weights)
     r0, r1, r2, r3 = experts(arrived, weights)
     back = (
         r0,

time: 182 us -> 164 us (0.901)
  blocking collectives: 47.8 us -> 29.6 us
  starting transfers between devices: 36.9 us -> 52.3 us
  Pallas kernels: 35.7 us -> 25.2 us
  local copies, waits for them, and re-layouts: 6.38 us -> 1.56 us
  other arithmetic: 1.48 us -> 3.85 us
    all_to_all x3 -> x2, blocking collectives: 47.8 us -> 29.6 us  [plane_exchange(): return lax.all_to_all(array, PLANE, split_axis=0, concat_axis=0, tiled=True)]
    all_to_all x2 -> x3, starting transfers between devices: 9.95 us -> 21.1 us  [plane_exchange(): return lax.all_to_all(array, PLANE, split_axis=0, concat_axis=0, tiled=True)]
    unnamed x56 -> x12, local copies, waits for them, and re-layouts: 6.38 us -> 1.56 us
    ppermute x3, waiting for transfers between devices: 8.16 us -> 11.7 us  [ring_gather(): lax.ppermute(own, 'x', LEFT)]
    ppermute x1, waiting for transfers between devices: 3.1 us -> 0.01 us  [on_device(): lax.ppermute(s2, 'x', ACROSS)]
    pallas_call x1, Pallas kernels: 3.31 us -> 0.45 us  [combine(): pl.pallas_call(combine_body, out_shape=jax.ShapeDtypeStruct((16, 8, D), B...]
    pallas_call x1, Pallas kernels: 3.44 us -> 0.83 us  [dense_first(): pl.pallas_call(dense_body, out_shape=jax.ShapeDtypeStruct((128, 256), BF1...]
    pallas_call x2 -> x4, Pallas kernels: 16.4 us -> 18.6 us  [the longest x1 6.08 us: renew(): pl.pallas_call(renew_body, in_specs=[VMEM, VMEM, HBM], out_specs=HBM, out...]
  transfers between devices with their start and end apart: 26 -> 27, of which waited for: 14 -> 13; matrix products, arithmetic and copies ran while one was open for 0% -> 2% of each run, Pallas kernels for 8% -> 12%
where the time goes in v2:
time: 164 us; the launch traced here: 163 us
  starting transfers between devices  52.3 us (32%)
  waiting for transfers between devices  49.9 us (30%)
  blocking collectives  29.6 us (18%)
  Pallas kernels  25.2 us (15%)
  other arithmetic  3.85 us (2%)
    all_to_all x2, blocking collectives, plane_exchange(): return lax.all_to_all(array, PLANE, split_axis=0, concat_axis=0, tiled=True)  29.6 us
    all_to_all x3, starting transfers between devices, plane_exchange(): return lax.all_to_all(array, PLANE, split_axis=0, concat_axis=0, tiled=True)  21.1 us
    ppermute x3, waiting for transfers between devices, ring_gather(): lax.ppermute(own, 'x', LEFT)  11.7 us
    ppermute x3, waiting for transfers between devices, ring_gather(): lax.ppermute(own, 'x', RIGHT)  11 us
    ppermute x3, waiting for transfers between devices, ring_gather(): lax.ppermute(own, 'x', ACROSS)  10.4 us
    all_to_all x3, waiting for transfers between devices, plane_exchange(): return lax.all_to_all(array, PLANE, split_axis=0, concat_axis=0, tiled=True)  9.18 us
    ppermute x4, starting transfers between devices, on_device(): lax.ppermute(c, 'tp', SWAP)  7.43 us
    pallas_call x1, Pallas kernels, renew(): pl.pallas_call(renew_body, in_specs=[VMEM, VMEM, HBM], out_specs=HBM, out...  6.08 us
  transfers between devices with their start and end apart: 27, of which 13 were waited for; matrix products, arithmetic and copies ran while one was open for 2% of the time, Pallas kernels for 12%

profile of v2, /device:TPU:1, one launch (start us, length us, event | category | flops | bytes accessed | tf_op | source)
XLA Modules:
  0.0 163.3 jit_solution(7338294851783046159)
XLA Ops:
  0.6 1.7 %prepare.1 = (bf16[16,32,128]{2,1,0:T(8,128)(2,1)}, bf16[4,32,768]{2,1,0:T(8,128)(2,1)}) custom-call(bf16[16,2048]{1,0:T(8,128)(2,1)} %x_ref.1, bf16[2048]{0:T(1024)(128)(2,1)} %gain.3, s32[4,16]{1,0:T(4,128)} %bitcast.11, bf16[4,16]{1,0:T(4,128)(2,1)} %bitcast.12, bf16[32,768]{1,0:T(8,128)(2,1)} %wq.1, bf16[32,768]{1,0:T(8,128)(2,1)} %wk.1, ...), custom_call_target="tpu_custom_call" | custom-call | tf_op jit(solution)/shard_map/prepare/pallas_call | solution.py:67
  2.3 2.0 %collective-permute-start = (bf16[4,32,768]{2,1,0:T(8,128)(2,1)}, bf16[4,32,768]{2,1,0:T(8,128)(2,1)S(1)}, u32[]{:S(2)}, u32[]{:S(2)}) collective-permute-start(bf16[4,32,768]{2,1,0:T(8,128)(2,1)} %get-tuple-element.52.c0), channel_id=1, source_target_pairs={{0,2},{2,4},{4,6},{6,0},{1,3},{3,5},{5,7},{7,1},{8,10},{10,12},{12... | collective-permute-start | bytes 589832 | tf_op jit(solution)/shard_map/ppermute | solution.py:30
  4.4 2.5 %collective-permute-start.1 = (bf16[4,32,768]{2,1,0:T(8,128)(2,1)}, bf16[4,32,768]{2,1,0:T(8,128)(2,1)S(1)}, u32[]{:S(2)}, u32[]{:S(2)}) collective-permute-start(bf16[4,32,768]{2,1,0:T(8,128)(2,1)} %get-tuple-element.52.c0), channel_id=1, source_target_pairs={{0,4},{2,6},{4,0},{6,2},{1,5},{3,7},{5,1},{7,3},{8,12},{10,14},{12... | collective-permute-start | bytes 589832 | tf_op jit(solution)/shard_map/ppermute | solution.py:31
  6.8 7.8 %all-to-all-start = ((bf16[16,32,128]{2,1,0:T(8,128)(2,1)}), bf16[16,32,128]{2,1,0:T(8,128)(2,1)S(1)}, u32[]{:S(2)}, u32[]{:S(2)}) async-start(bf16[16,32,128]{2,1,0:T(8,128)(2,1)} %get-tuple-element.51), calls=%async_computation | async-start | bytes 262144 | tf_op jit(solution)/shard_map/all_to_all | solution.py:445
  14.6 1.6 collective-permute-start.13
  16.2 0.1 collective-permute-start.14
  16.3 0.4 collective-permute-start.15
  16.7 1.1 pad_maximum_fusion.c0
  17.8 0.7 convert_element_type.12
  18.4 1.2 collective-permute-start.2
  19.6 1.4 fusion
  21.0 0.5 all-to-all-done.x_ref.got
  21.4 0.0 collective-permute-done.1.c2
  21.4 3.6 %collective-permute-done.2.c3 = bf16[4,32,768]{2,1,0:T(8,128)(2,1)S(1)} collective-permute-done((bf16[4,32,768]{2,1,0:T(8,128)(2,1)}, bf16[4,32,768]{2,1,0:T(8,128)(2,1)S(1)}, u32[]{:S(2)}, u32[]{:S(2)}) %collective-permute-start.2) | collective-permute-done | bytes 196640 | tf_op jit(solution)/shard_map/ppermute | solution.py:32
  25.0 0.9 copy-done
  25.9 1.5 project.1
  27.4 0.0 copy-start.1
  27.4 7.0 %all-to-all-start.1 = ((bf16[16,16,3072]{2,1,0:T(8,128)(2,1)}), bf16[16,16,3072]{2,1,0:T(8,128)(2,1)}, u32[]{:S(2)}, u32[]{:S(2)}) async-start(bf16[16,16,3072]{2,1,0:T(8,128)(2,1)} %project.1), calls=%async_computation.1 | async-start | bytes 3145728 | tf_op jit(solution)/shard_map/all_to_all | solution.py:445
  34.5 0.1 collective-permute-start.6
  34.6 0.8 collective-permute-start.3
  35.4 11.0 %collective-permute-done.3.c1 = bf16[32,768]{1,0:T(8,128)(2,1)S(1)} collective-permute-done((bf16[32,768]{1,0:T(8,128)(2,1)S(1)}, bf16[32,768]{1,0:T(8,128)(2,1)S(1)}, u32[]{:S(2)}, u32[]{:S(2)}) %collective-permute-start.3) | collective-permute-done | bytes 49184 | tf_op jit(solution)/shard_map/ppermute | solution.py:30
  46.4 0.2 collective-permute-start.4
  46.6 4.6 %collective-permute-done.4.c2 = bf16[32,768]{1,0:T(8,128)(2,1)S(1)} collective-permute-done((bf16[32,768]{1,0:T(8,128)(2,1)S(1)}, bf16[32,768]{1,0:T(8,128)(2,1)S(1)}, u32[]{:S(2)}, u32[]{:S(2)}) %collective-permute-start.4) | collective-permute-done | bytes 49184 | tf_op jit(solution)/shard_map/ppermute | solution.py:31
  51.2 1.2 collective-permute-start.5
  52.4 1.9 %collective-permute-done.5.c3 = bf16[32,768]{1,0:T(8,128)(2,1)S(1)} collective-permute-done((bf16[32,768]{1,0:T(8,128)(2,1)S(1)}, bf16[32,768]{1,0:T(8,128)(2,1)S(1)}, u32[]{:S(2)}, u32[]{:S(2)}) %collective-permute-start.5) | collective-permute-done | bytes 49184 | tf_op jit(solution)/shard_map/ppermute | solution.py:32
  54.3 0.9 collective-permute-start.7
  55.2 1.5 collective-permute-start.8
  56.6 5.8 %collective-permute-done.7.c2 = bf16[96,2048]{1,0:T(8,128)(2,1)S(1)} collective-permute-done((bf16[96,2048]{1,0:T(8,128)(2,1)S(1)}, bf16[96,2048]{1,0:T(8,128)(2,1)S(1)}, u32[]{:S(2)}, u32[]{:S(2)}) %collective-permute-start.7) | collective-permute-done | bytes 393248 | tf_op jit(solution)/shard_map/ppermute | solution.py:31
  62.4 4.9 %collective-permute-start.9 = (bf16[96,2048]{1,0:T(8,128)(2,1)S(1)}, bf16[96,2048]{1,0:T(8,128)(2,1)S(1)}, u32[]{:S(2)}, u32[]{:S(2)}) collective-permute-start(bf16[96,2048]{1,0:T(8,128)(2,1)S(1)} %pad_maximum_fusion.c0), channel_id=1, source_target_pairs={{0,1},{1,0},{2,3},{3,2},{4,5},{5,4},{6,7},{7,6},{8,9},{9,8},{10,11... | collective-permute-start | bytes 1179656 | tf_op jit(solution)/shard_map/ppermute | solution.py:517
  67.3 6.3 %collective-permute-done.8.c3 = bf16[96,2048]{1,0:T(8,128)(2,1)S(1)} collective-permute-done((bf16[96,2048]{1,0:T(8,128)(2,1)S(1)}, bf16[96,2048]{1,0:T(8,128)(2,1)S(1)}, u32[]{:S(2)}, u32[]{:S(2)}) %collective-permute-start.8) | collective-permute-done | bytes 393248 | tf_op jit(solution)/shard_map/ppermute | solution.py:32
  73.6 2.1 %collective-permute-start.10 = (bf16[96,2048]{1,0:T(8,128)(2,1)S(1)}, bf16[96,2048]{1,0:T(8,128)(2,1)S(1)}, u32[]{:S(2)}, u32[]{:S(2)}) collective-permute-start(bf16[96,2048]{1,0:T(8,128)(2,1)S(1)} %collective-permute-done.6.c1), channel_id=1, source_target_pairs={{0,1},{1,0},{2,3},{3,2},{4,5},{5,4},{6,7},{7,6},{8,9},{9,8},{10,11... | collective-permute-start | bytes 1179656 | tf_op jit(solution)/shard_map/ppermute | solution.py:517
  75.7 0.0 collective-permute-done.9.c4
  75.8 0.0 collective-permute-start.11
  75.8 1.3 collective-permute-done.10.c5
  77.1 0.4 collective-permute-start.12
  77.5 0.0 all-to-all-done.1.parts
  77.5 5.9 %recall.1 = (bf16[16,16,768]{2,1,0:T(8,128)(2,1)}, f32[16,8,128]{2,1,0:T(8,128)}, f32[16,8,128]{2,1,0:T(8,128)}) custom-call(bf16[16,16,3072]{2,1,0:T(8,128)(2,1)} %all-to-all-done.1.parts, f32[16,128]{1,0:T(8,128)} %get-tuple-element.54.cosine_ref, f32[16,128]{1,0:T(8,128)} %get-tuple-element.55.sine_ref, bf16[768]{0:T(1024)(128)(2,1)} %gain.4, ...), custom_call_target="tpu_custom_call" | custom-call | tf_op jit(solution)/shard_map/recall/pallas_call | solution.py:196
  83.3 0.0 copy-start.4
  83.4 0.0 copy-start.5
  83.4 6.3 %all-to-all-start.2 = ((bf16[16,16,768]{2,1,0:T(8,128)(2,1)}), bf16[16,16,768]{2,1,0:T(8,128)(2,1)}, u32[]{:S(2)}, u32[]{:S(2)}) async-start(bf16[16,16,768]{2,1,0:T(8,128)(2,1)} %get-tuple-element.56), calls=%async_computation.2 | async-start | bytes 786432 | tf_op jit(solution)/shard_map/all_to_all | solution.py:445
  89.7 0.2 routing.1
  89.9 0.6 copy-done.2
  90.5 8.7 %all-to-all-done.2.kept = bf16[16,16,768]{2,1,0:T(8,128)(2,1)} async-done(((bf16[16,16,768]{2,1,0:T(8,128)(2,1)}), bf16[16,16,768]{2,1,0:T(8,128)(2,1)}, u32[]{:S(2)}, u32[]{:S(2)}) %all-to-all-start.2) | async-done | bytes 393248 | tf_op jit(solution)/shard_map/all_to_all | solution.py:445
  99.3 1.3 mix.1
  100.6 1.6 %collective-permute-start.16 = (bf16[16,8,128]{2,1,0:T(8,128)(2,1)S(1)}, bf16[16,8,128]{2,1,0:T(8,128)(2,1)S(1)}, u32[]{:S(2)}, u32[]{:S(2)}) collective-permute-start(bf16[16,8,128]{2,1,0:T(8,128)(2,1)S(1)} %get-tuple-element.67), channel_id=1, source_target_pairs={{0,1},{1,0},{2,3},{3,2},{4,5},{5,4},{6,7},{7,6},{8,9},{9,8},{10,11... | collective-permute-start | bytes 98312 | tf_op jit(solution)/shard_map/ppermute | solution.py:526
  102.2 0.9 collective-permute-done.16.other
  103.1 13.4 %all_to_all.25.res = bf16[16,128,128]{2,1,0:T(8,128)(2,1)S(1)} all-to-all(bf16[16,128,128]{2,1,0:T(8,128)(2,1)S(1)} %settle.1), channel_id=1, replica_groups=mesh['z'=4,'y'=4,'x'=4,'tp'=2] {'z','y'}, dimensions={0} | all-to-all | bytes 1048576 | tf_op jit(solution)/shard_map/all_to_all | solution.py:445
  116.5 0.6 spread.1
  117.2 0.1 collective-permute-start.17
  117.2 3.2 %collective-permute-start.18 = (bf16[32,2048]{1,0:T(8,128)(2,1)S(1)}, bf16[32,2048]{1,0:T(8,128)(2,1)S(1)}, u32[]{:S(2)}, u32[]{:S(2)}) collective-permute-start(bf16[32,2048]{1,0:T(8,128)(2,1)S(1)} %get-tuple-element.83), channel_id=1, source_target_pairs={{0,4},{2,6},{4,0},{6,2},{1,5},{3,7},{5,1},{7,3},{8,12},{10,14},{12... | collective-permute-start | bytes 393224 | tf_op jit(solution)/shard_map/ppermute | solution.py:534
  120.5 4.7 %hoist.1 = (bf16[1,2048,512]{2,1,0:T(8,128)(2,1)S(1)}, bf16[1,2048,512]{2,1,0:T(8,128)(2,1)S(1)}, bf16[1,2048,512]{2,1,0:T(8,128)(2,1)S(1)}, bf16[1,2048,512]{2,...) custom-call(bf16[1,2048,512]{2,1,0:T(8,128)(2,1)} %refs_0_.1, ...), custom_call_target="tpu_custom_call" | custom-call | tf_op jit(solution)/shard_map/hoist/pallas_call | solution.py:433
  125.2 1.9 %experts.1 = (bf16[32,2048]{1,0:T(8,128)(2,1)S(1)}, bf16[32,2048]{1,0:T(8,128)(2,1)S(1)}, bf16[32,2048]{1,0:T(8,128)(2,1)S(1)}, bf16[32,2048]{1,0:T(8,128)(2,1)S(1)}) custom-call(bf16[32,2048]{1,0:T(8,128)(2,1)S(1)} %get-tuple-element.81.a0, bf16[32,2048]{1,0:T(8,128)(2,1)S(1)} %collective-permute-done.17.a1, ...), custom_call_target="tpu_custom_call" | custom-call | tf_op jit(solution)/shard_map/experts/pallas_call | solution.py:382
  127.1 3.6 %collective-permute-start.20 = (bf16[32,2048]{1,0:T(8,128)(2,1)S(1)}, bf16[32,2048]{1,0:T(8,128)(2,1)S(1)}, u32[]{:S(2)}, u32[]{:S(2)}) collective-permute-start(bf16[32,2048]{1,0:T(8,128)(2,1)S(1)} %get-tuple-element.95), channel_id=1, source_target_pairs={{0,6},{2,0},{4,2},{6,4},{1,7},{3,1},{5,3},{7,5},{8,14},{10,8},{12,... | collective-permute-start | bytes 393224 | tf_op jit(solution)/shard_map/ppermute | solution.py:543
  130.7 0.7 collective-permute-start.22
  131.4 0.8 dense_first.1.hidden
  132.2 2.1 %collective-permute-done.20.b1 = bf16[32,2048]{1,0:T(8,128)(2,1)S(1)} collective-permute-done((bf16[32,2048]{1,0:T(8,128)(2,1)S(1)}, bf16[32,2048]{1,0:T(8,128)(2,1)S(1)}, u32[]{:S(2)}, u32[]{:S(2)}) %collective-permute-start.20) | collective-permute-done | bytes 131104 | tf_op jit(solution)/shard_map/ppermute | solution.py:543
  134.3 1.8 %collective-permute-done.21.b2 = bf16[32,2048]{1,0:T(8,128)(2,1)S(1)} collective-permute-done((bf16[32,2048]{1,0:T(8,128)(2,1)S(1)}, bf16[32,2048]{1,0:T(8,128)(2,1)S(1)}, u32[]{:S(2)}, u32[]{:S(2)}) %collective-permute-start.21) | collective-permute-done | bytes 131104 | tf_op jit(solution)/shard_map/ppermute | solution.py:544
  136.1 1.5 collective-permute-done.22.b3
  137.6 0.5 combine.1
  138.1 16.2 %all_to_all.26 = bf16[16,8,2048]{2,1,0:T(8,128)(2,1)S(1)} all-to-all(bf16[16,8,2048]{2,1,0:T(8,128)(2,1)S(1)} %combine.1), channel_id=1, replica_groups=mesh['z'=4,'y'=4,'x'=4,'tp'=2] {'z','y'}, dimensions={0} | all-to-all | bytes 1048576 | tf_op jit(solution)/shard_map/all_to_all | solution.py:445
  154.3 0.1 convert_reduce_fusion
  154.3 2.2 %collective-permute-start.23 = (bf16[8,2048]{1,0:T(8,128)(2,1)S(1)}, bf16[8,2048]{1,0:T(8,128)(2,1)S(1)}, u32[]{:S(2)}, u32[]{:S(2)}) collective-permute-start(bf16[8,2048]{1,0:T(8,128)(2,1)S(1)} %add_convert_fusion), channel_id=1, source_target_pairs={{0,1},{1,0},{2,3},{3,2},{4,5},{5,4},{6,7},{7,6},{8,9},{9,8},{10,11... | collective-permute-start | bytes 98312 | tf_op jit(solution)/shard_map/ppermute | solution.py:551
  156.5 6.1 %renew.1 = f32[16,6,128,128]{3,2,1,0:T(8,128)} custom-call(f32[16,8,128]{2,1,0:T(8,128)} %get-tuple-element.98.keys, f32[16,8,128]{2,1,0:T(8,128)} %get-tuple-element.99.values, f32[16,6,128,128]{3,2,1,0:T(8,128)} %state_ref.3), custom_call_target="tpu_custom_call" | custom-call | tf_op jit(solution)/shard_map/renew/pallas_call | solution.py:249
  162.7 0.6 pad_maximum_fusion.1
  (23 shorter events, 0.1 us)
Async XLA Ops:
  2.3 16.1 %collective-permute-start = (bf16[4,32,768]{2,1,0:T(8,128)(2,1)}, bf16[4,32,768]{2,1,0:T(8,128)(2,1)S(1)}, u32[]{:S(2)}, u32[]{:S(2)}) collective-permute-start(bf16[4,32,768]{2,1,0:T(8,128)(2,1)} %get-tuple-element.52.c0), channel_id=1, source_target_pairs={{0,2},{2,4},{4,6},{6,0},{1,3},{3,5},{5,7},{7,1},{8,10},{10,12},{12... | collective-permute-start | bytes 589832 | tf_op jit(solution)/shard_map/ppermute | solution.py:30
  4.4 17.1 %collective-permute-start.1 = (bf16[4,32,768]{2,1,0:T(8,128)(2,1)}, bf16[4,32,768]{2,1,0:T(8,128)(2,1)S(1)}, u32[]{:S(2)}, u32[]{:S(2)}) collective-permute-start(bf16[4,32,768]{2,1,0:T(8,128)(2,1)} %get-tuple-element.52.c0), channel_id=1, source_target_pairs={{0,4},{2,6},{4,0},{6,2},{1,5},{3,7},{5,1},{7,3},{8,12},{10,14},{12... | collective-permute-start | bytes 589832 | tf_op jit(solution)/shard_map/ppermute | solution.py:31
  6.8 14.6 %all-to-all-start = ((bf16[16,32,128]{2,1,0:T(8,128)(2,1)}), bf16[16,32,128]{2,1,0:T(8,128)(2,1)S(1)}, u32[]{:S(2)}, u32[]{:S(2)}) async-start(bf16[16,32,128]{2,1,0:T(8,128)(2,1)} %get-tuple-element.51), calls=%async_computation | async-start | bytes 262144 | tf_op jit(solution)/shard_map/all_to_all | solution.py:445
  14.6 84.6 %collective-permute-start.13 = (bf16[1,2048,512]{2,1,0:T(8,128)(2,1)}, bf16[1,2048,512]{2,1,0:T(8,128)(2,1)}, u32[]{:S(2)}, u32[]{:S(2)}) collective-permute-start(bf16[1,2048,512]{2,1,0:T(8,128)(2,1)} %refs_0_.1), channel_id=1, source_target_pairs={{0,1},{1,0},{2,3},{3,2},{4,5},{5,4},{6,7},{7,6},{8,9},{9,8},{10,11... | collective-permute-start | bytes 6291464 | tf_op jit(solution)/shard_map/ppermute | solution.py:516
  16.2 83.1 %collective-permute-start.14 = (bf16[1,2048,512]{2,1,0:T(8,128)(2,1)}, bf16[1,2048,512]{2,1,0:T(8,128)(2,1)}, u32[]{:S(2)}, u32[]{:S(2)}) collective-permute-start(bf16[1,2048,512]{2,1,0:T(8,128)(2,1)} %refs_2_.1), channel_id=1, source_target_pairs={{0,1},{1,0},{2,3},{3,2},{4,5},{5,4},{6,7},{7,6},{8,9},{9,8},{10,11... | collective-permute-start | bytes 6291464 | tf_op jit(solution)/shard_map/ppermute | solution.py:516
  16.3 83.0 %collective-permute-start.15 = (bf16[1,512,2048]{2,1,0:T(8,128)(2,1)}, bf16[1,512,2048]{2,1,0:T(8,128)(2,1)}, u32[]{:S(2)}, u32[]{:S(2)}) collective-permute-start(bf16[1,512,2048]{2,1,0:T(8,128)(2,1)} %refs_4_.1), channel_id=1, source_target_pairs={{0,1},{1,0},{2,3},{3,2},{4,5},{5,4},{6,7},{7,6},{8,9},{9,8},{10,11... | collective-permute-start | bytes 6291464 | tf_op jit(solution)/shard_map/ppermute | solution.py:516
  18.4 6.6 %collective-permute-start.2 = (bf16[4,32,768]{2,1,0:T(8,128)(2,1)}, bf16[4,32,768]{2,1,0:T(8,128)(2,1)S(1)}, u32[]{:S(2)}, u32[]{:S(2)}) collective-permute-start(bf16[4,32,768]{2,1,0:T(8,128)(2,1)} %get-tuple-element.52.c0), channel_id=1, source_target_pairs={{0,6},{2,0},{4,2},{6,4},{1,7},{3,1},{5,3},{7,5},{8,14},{10,8},{12,... | collective-permute-start | bytes 589832 | tf_op jit(solution)/shard_map/ppermute | solution.py:32
  25.0 0.9 copy-start
  27.4 7.2 %copy-start.1 = (bf16[768,32]{0,1:T(8,128)(2,1)S(1)}, bf16[768,32]{0,1:T(8,128)(2,1)}, u32[]{:S(2)}) copy-start(bf16[768,32]{0,1:T(8,128)(2,1)} %param.31) | copy-start | bytes 147460
  27.4 50.0 %all-to-all-start.1 = ((bf16[16,16,3072]{2,1,0:T(8,128)(2,1)}), bf16[16,16,3072]{2,1,0:T(8,128)(2,1)}, u32[]{:S(2)}, u32[]{:S(2)}) async-start(bf16[16,16,3072]{2,1,0:T(8,128)(2,1)} %project.1), calls=%async_computation.1 | async-start | bytes 3145728 | tf_op jit(solution)/shard_map/all_to_all | solution.py:445
  34.5 20.7 %collective-permute-start.6 = (bf16[96,2048]{1,0:T(8,128)(2,1)S(1)}, bf16[96,2048]{1,0:T(8,128)(2,1)S(1)}, u32[]{:S(2)}, u32[]{:S(2)}) collective-permute-start(bf16[96,2048]{1,0:T(8,128)(2,1)S(1)} %pad_maximum_fusion.c0), channel_id=1, source_target_pairs={{0,2},{2,4},{4,6},{6,0},{1,3},{3,5},{5,7},{7,1},{8,10},{10,12},{12... | collective-permute-start | bytes 1179656 | tf_op jit(solution)/shard_map/ppermute | solution.py:30
  34.6 11.8 %collective-permute-start.3 = (bf16[32,768]{1,0:T(8,128)(2,1)S(1)}, bf16[32,768]{1,0:T(8,128)(2,1)S(1)}, u32[]{:S(2)}, u32[]{:S(2)}) collective-permute-start(bf16[32,768]{1,0:T(8,128)(2,1)S(1)} %bitcast.5), channel_id=1, source_target_pairs={{0,2},{2,4},{4,6},{6,0},{1,3},{3,5},{5,7},{7,1},{8,10},{10,12},{12... | collective-permute-start | bytes 147464 | tf_op jit(solution)/shard_map/ppermute | solution.py:30
  46.4 4.8 %collective-permute-start.4 = (bf16[32,768]{1,0:T(8,128)(2,1)S(1)}, bf16[32,768]{1,0:T(8,128)(2,1)S(1)}, u32[]{:S(2)}, u32[]{:S(2)}) collective-permute-start(bf16[32,768]{1,0:T(8,128)(2,1)S(1)} %bitcast.6), channel_id=1, source_target_pairs={{0,4},{2,6},{4,0},{6,2},{1,5},{3,7},{5,1},{7,3},{8,12},{10,14},{12... | collective-permute-start | bytes 147464 | tf_op jit(solution)/shard_map/ppermute | solution.py:31
  51.2 3.1 %collective-permute-start.5 = (bf16[32,768]{1,0:T(8,128)(2,1)S(1)}, bf16[32,768]{1,0:T(8,128)(2,1)S(1)}, u32[]{:S(2)}, u32[]{:S(2)}) collective-permute-start(bf16[32,768]{1,0:T(8,128)(2,1)S(1)} %bitcast.7), channel_id=1, source_target_pairs={{0,6},{2,0},{4,2},{6,4},{1,7},{3,1},{5,3},{7,5},{8,14},{10,8},{12,... | collective-permute-start | bytes 147464 | tf_op jit(solution)/shard_map/ppermute | solution.py:32
  54.3 8.1 %collective-permute-start.7 = (bf16[96,2048]{1,0:T(8,128)(2,1)S(1)}, bf16[96,2048]{1,0:T(8,128)(2,1)S(1)}, u32[]{:S(2)}, u32[]{:S(2)}) collective-permute-start(bf16[96,2048]{1,0:T(8,128)(2,1)S(1)} %pad_maximum_fusion.c0), channel_id=1, source_target_pairs={{0,4},{2,6},{4,0},{6,2},{1,5},{3,7},{5,1},{7,3},{8,12},{10,14},{12... | collective-permute-start | bytes 1179656 | tf_op jit(solution)/shard_map/ppermute | solution.py:31
  55.2 18.4 %collective-permute-start.8 = (bf16[96,2048]{1,0:T(8,128)(2,1)S(1)}, bf16[96,2048]{1,0:T(8,128)(2,1)S(1)}, u32[]{:S(2)}, u32[]{:S(2)}) collective-permute-start(bf16[96,2048]{1,0:T(8,128)(2,1)S(1)} %pad_maximum_fusion.c0), channel_id=1, source_target_pairs={{0,6},{2,0},{4,2},{6,4},{1,7},{3,1},{5,3},{7,5},{8,14},{10,8},{12,... | collective-permute-start | bytes 1179656 | tf_op jit(solution)/shard_map/ppermute | solution.py:32
  62.4 13.3 %collective-permute-start.9 = (bf16[96,2048]{1,0:T(8,128)(2,1)S(1)}, bf16[96,2048]{1,0:T(8,128)(2,1)S(1)}, u32[]{:S(2)}, u32[]{:S(2)}) collective-permute-start(bf16[96,2048]{1,0:T(8,128)(2,1)S(1)} %pad_maximum_fusion.c0), channel_id=1, source_target_pairs={{0,1},{1,0},{2,3},{3,2},{4,5},{5,4},{6,7},{7,6},{8,9},{9,8},{10,11... | collective-permute-start | bytes 1179656 | tf_op jit(solution)/shard_map/ppermute | solution.py:517
  73.6 3.5 %collective-permute-start.10 = (bf16[96,2048]{1,0:T(8,128)(2,1)S(1)}, bf16[96,2048]{1,0:T(8,128)(2,1)S(1)}, u32[]{:S(2)}, u32[]{:S(2)}) collective-permute-start(bf16[96,2048]{1,0:T(8,128)(2,1)S(1)} %collective-permute-done.6.c1), channel_id=1, source_target_pairs={{0,1},{1,0},{2,3},{3,2},{4,5},{5,4},{6,7},{7,6},{8,9},{9,8},{10,11... | collective-permute-start | bytes 1179656 | tf_op jit(solution)/shard_map/ppermute | solution.py:517
  75.8 14.8 %collective-permute-start.11 = (bf16[96,2048]{1,0:T(8,128)(2,1)S(1)}, bf16[96,2048]{1,0:T(8,128)(2,1)S(1)}, u32[]{:S(2)}, u32[]{:S(2)}) collective-permute-start(bf16[96,2048]{1,0:T(8,128)(2,1)S(1)} %collective-permute-done.7.c2), channel_id=1, source_target_pairs={{0,1},{1,0},{2,3},{3,2},{4,5},{5,4},{6,7},{7,6},{8,9},{9,8},{10,11... | collective-permute-start | bytes 1179656 | tf_op jit(solution)/shard_map/ppermute | solution.py:517
  77.1 13.4 %collective-permute-start.12 = (bf16[96,2048]{1,0:T(8,128)(2,1)S(1)}, bf16[96,2048]{1,0:T(8,128)(2,1)S(1)}, u32[]{:S(2)}, u32[]{:S(2)}) collective-permute-start(bf16[96,2048]{1,0:T(8,128)(2,1)S(1)} %collective-permute-done.8.c3), channel_id=1, source_target_pairs={{0,1},{1,0},{2,3},{3,2},{4,5},{5,4},{6,7},{7,6},{8,9},{9,8},{10,11... | collective-permute-start | bytes 1179656 | tf_op jit(solution)/shard_map/ppermute | solution.py:517
  83.3 33.2 %copy-start.4 = (bf16[2048]{0:T(1024)(128)(2,1)S(1)}, bf16[2048]{0:T(1024)(128)(2,1)}, u32[]{:S(2)}) copy-start(bf16[2048]{0:T(1024)(128)(2,1)} %gain.5) | copy-start | bytes 12292
  83.4 33.1 %copy-start.5 = (bf16[2048]{0:T(1024)(128)(2,1)S(1)}, bf16[2048]{0:T(1024)(128)(2,1)}, u32[]{:S(2)}) copy-start(bf16[2048]{0:T(1024)(128)(2,1)} %branch.1) | copy-start | bytes 12292
  83.4 15.9 %all-to-all-start.2 = ((bf16[16,16,768]{2,1,0:T(8,128)(2,1)}), bf16[16,16,768]{2,1,0:T(8,128)(2,1)}, u32[]{:S(2)}, u32[]{:S(2)}) async-start(bf16[16,16,768]{2,1,0:T(8,128)(2,1)} %get-tuple-element.56), calls=%async_computation.2 | async-start | bytes 786432 | tf_op jit(solution)/shard_map/all_to_all | solution.py:445
  89.9 0.6 copy-start.2
  99.2 17.3 %copy-start.3 = (bf16[128,128]{1,0:T(8,128)(2,1)S(1)}, bf16[128,128]{1,0:T(8,128)(2,1)}, u32[]{:S(2)}) copy-start(bf16[128,128]{1,0:T(8,128)(2,1)} %copy-done.2) | copy-start | bytes 98308
  100.6 2.5 %collective-permute-start.16 = (bf16[16,8,128]{2,1,0:T(8,128)(2,1)S(1)}, bf16[16,8,128]{2,1,0:T(8,128)(2,1)S(1)}, u32[]{:S(2)}, u32[]{:S(2)}) collective-permute-start(bf16[16,8,128]{2,1,0:T(8,128)(2,1)S(1)} %get-tuple-element.67), channel_id=1, source_target_pairs={{0,1},{1,0},{2,3},{3,2},{4,5},{5,4},{6,7},{7,6},{8,9},{9,8},{10,11... | collective-permute-start | bytes 98312 | tf_op jit(solution)/shard_map/ppermute | solution.py:526
  117.2 8.0 %collective-permute-start.17 = (bf16[32,2048]{1,0:T(8,128)(2,1)S(1)}, bf16[32,2048]{1,0:T(8,128)(2,1)S(1)}, u32[]{:S(2)}, u32[]{:S(2)}) collective-permute-start(bf16[32,2048]{1,0:T(8,128)(2,1)S(1)} %get-tuple-element.82), channel_id=1, source_target_pairs={{0,2},{2,4},{4,6},{6,0},{1,3},{3,5},{5,7},{7,1},{8,10},{10,12},{12... | collective-permute-start | bytes 393224 | tf_op jit(solution)/shard_map/ppermute | solution.py:533
  117.2 8.0 %collective-permute-start.18 = (bf16[32,2048]{1,0:T(8,128)(2,1)S(1)}, bf16[32,2048]{1,0:T(8,128)(2,1)S(1)}, u32[]{:S(2)}, u32[]{:S(2)}) collective-permute-start(bf16[32,2048]{1,0:T(8,128)(2,1)S(1)} %get-tuple-element.83), channel_id=1, source_target_pairs={{0,4},{2,6},{4,0},{6,2},{1,5},{3,7},{5,1},{7,3},{8,12},{10,14},{12... | collective-permute-start | bytes 393224 | tf_op jit(solution)/shard_map/ppermute | solution.py:534
  120.5 4.7 %collective-permute-start.19 = (bf16[32,2048]{1,0:T(8,128)(2,1)S(1)}, bf16[32,2048]{1,0:T(8,128)(2,1)S(1)}, u32[]{:S(2)}, u32[]{:S(2)}) collective-permute-start(bf16[32,2048]{1,0:T(8,128)(2,1)S(1)} %get-tuple-element.84), channel_id=1, source_target_pairs={{0,6},{2,0},{4,2},{6,4},{1,7},{3,1},{5,3},{7,5},{8,14},{10,8},{12,... | collective-permute-start | bytes 393224 | tf_op jit(solution)/shard_map/ppermute | solution.py:535
  127.1 7.2 %collective-permute-start.20 = (bf16[32,2048]{1,0:T(8,128)(2,1)S(1)}, bf16[32,2048]{1,0:T(8,128)(2,1)S(1)}, u32[]{:S(2)}, u32[]{:S(2)}) collective-permute-start(bf16[32,2048]{1,0:T(8,128)(2,1)S(1)} %get-tuple-element.95), channel_id=1, source_target_pairs={{0,6},{2,0},{4,2},{6,4},{1,7},{3,1},{5,3},{7,5},{8,14},{10,8},{12,... | collective-permute-start | bytes 393224 | tf_op jit(solution)/shard_map/ppermute | solution.py:543
  130.7 5.4 %collective-permute-start.21 = (bf16[32,2048]{1,0:T(8,128)(2,1)S(1)}, bf16[32,2048]{1,0:T(8,128)(2,1)S(1)}, u32[]{:S(2)}, u32[]{:S(2)}) collective-permute-start(bf16[32,2048]{1,0:T(8,128)(2,1)S(1)} %get-tuple-element.96), channel_id=1, source_target_pairs={{0,4},{2,6},{4,0},{6,2},{1,5},{3,7},{5,1},{7,3},{8,12},{10,14},{12... | collective-permute-start | bytes 393224 | tf_op jit(solution)/shard_map/ppermute | solution.py:544
  130.7 6.9 %collective-permute-start.22 = (bf16[32,2048]{1,0:T(8,128)(2,1)S(1)}, bf16[32,2048]{1,0:T(8,128)(2,1)S(1)}, u32[]{:S(2)}, u32[]{:S(2)}) collective-permute-start(bf16[32,2048]{1,0:T(8,128)(2,1)S(1)} %get-tuple-element.97), channel_id=1, source_target_pairs={{0,2},{2,4},{4,6},{6,0},{1,3},{3,5},{5,7},{7,1},{8,10},{10,12},{12... | collective-permute-start | bytes 393224 | tf_op jit(solution)/shard_map/ppermute | solution.py:545
  154.3 8.3 %collective-permute-start.23 = (bf16[8,2048]{1,0:T(8,128)(2,1)S(1)}, bf16[8,2048]{1,0:T(8,128)(2,1)S(1)}, u32[]{:S(2)}, u32[]{:S(2)}) collective-permute-start(bf16[8,2048]{1,0:T(8,128)(2,1)S(1)} %add_convert_fusion), channel_id=1, source_target_pairs={{0,1},{1,0},{2,3},{3,2},{4,5},{5,4},{6,7},{7,6},{8,9},{9,8},{10,11... | collective-permute-start | bytes 98312 | tf_op jit(solution)/shard_map/ppermute | solution.py:551

commit v3 on v2

--- a/solution.py
+++ b/solution.py
@@ -1,3 +1,5 @@
+import functools
+
 import jax
 import jax.numpy as jnp
 import numpy as np
@@ -111,6 +113,7 @@
 
 PER_STEP = 2
 STEPS = 16 // PER_STEP
+AHEAD = 8
 FREQUENCY = np.tile(10000.0 ** (-np.arange(64) * 2.0 / 128), 2).astype(np.float32)
 TURN = np.repeat([-1.0, 1.0], 64).astype(np.float32)
 GAMMA = [float(np.exp(np.log1p(-(2.0 ** (-5.0 - 5.0 * h / (HEADS - 1)))))) for h in range(HEADS)]
@@ -145,7 +148,7 @@
             state_ref.at[some_rows(i)], buf.at[some_rows(i)], sems.at[i]
         )
 
-    for i in range(STEPS):
+    for i in range(AHEAD):
         fetch(i).start()
     gamma = gammas()
     for c in fetch_turns:
@@ -173,6 +176,11 @@
 
     def some(i, carry):
         fetch(i).wait()
+
+        @pl.when(i + AHEAD < STEPS)
+        def _():
+            fetch(i + AHEAD).start()
+
         for j in range(PER_STEP):
             t = i * PER_STEP + j
             for h in range(6):
@@ -215,18 +223,20 @@
     )(parts, cosine, sine, gain, state)
 
 
-def renew_body(keys, values, state_ref, new_state, buf, sems):
+def renew_body(first, keys, values, state_ref, *rest):
+    new_state, buf, sems = rest[-3:]
+
     def fetch(i):
         return pltpu.make_async_copy(
-            state_ref.at[some_rows(i)], buf.at[some_rows(i)], sems.at[i]
+            state_ref.at[some_rows(first + i)], buf.at[some_rows(i)], sems.at[i]
         )
 
     def store(i):
         return pltpu.make_async_copy(
-            buf.at[some_rows(i)], new_state.at[some_rows(i)], sems.at[STEPS + i]
+            buf.at[some_rows(i)], new_state.at[some_rows(first + i)], sems.at[HALF + i]
         )
 
-    for i in range(STEPS):
+    for i in range(HALF):
         fetch(i).start()
     gamma = gammas()
 
@@ -234,30 +244,34 @@
         fetch(i).wait()
         for j in range(PER_STEP):
             t = i * PER_STEP + j
+            at = first * PER_STEP + t
             for h in range(6):
-                k_full = as_columns(keys[t, h : h + 1, :])
-                buf[t, h] = gamma[h] * buf[t, h] + k_full * values[t, h : h + 1, :]
+                k_full = as_columns(keys[at, h : h + 1, :])
+                buf[t, h] = gamma[h] * buf[t, h] + k_full * values[at, h : h + 1, :]
         store(i).start()
         return carry
 
-    lax.fori_loop(0, STEPS, some, 0)
-    for i in range(STEPS):
+    lax.fori_loop(0, HALF, some, 0)
+    for i in range(HALF):
         store(i).wait()
 
 
-def renew(keys, values, state):
-    return pl.pallas_call(
-        renew_body,
-        in_specs=[VMEM, VMEM, HBM],
+HALF = STEPS // 2
+
+
+def renew(keys, values, state, half, *before):
+    return pl.pallas_call(
+        functools.partial(renew_body, half * HALF),
+        in_specs=[VMEM, VMEM, HBM] + [HBM] * len(before),
         out_specs=HBM,
         out_shape=jax.ShapeDtypeStruct((16, 6, 128, 128), F32),
+        input_output_aliases={3: 0} if before else {},
         scratch_shapes=[
-            pltpu.VMEM((16, 6, 128, 128), F32),
-            pltpu.SemaphoreType.DMA((2 * STEPS,)),
+            pltpu.VMEM((16 // 2, 6, 128, 128), F32),
+            pltpu.SemaphoreType.DMA((2 * HALF,)),
         ],
         compiler_params=pltpu.CompilerParams(vmem_limit_bytes=57 * 2**20),
-        name="renew",
-    )(keys, values, state)
+    )(keys, values, state, *before)
 
 
 def mix_body(kept, c0, c1, c2, c3, keep, give, wide, mixed):
@@ -338,11 +352,12 @@
     )(res, gain, branch, pick)
 
 
-def dense_body(plane, c0, c1, c2, c3, c4, c5, c6, c7, hidden, gate, up):
+def dense_body(plane, c0, c1, c2, c3, c4, c5, c6, c7, hidden, down, gate, up):
     for r, chunk in enumerate((c0, c1, c2, c3, c4, c5, c6, c7)):
         at = slice(r * 32, (r + 1) * 32)
         gate[at, :] = chunk[0:32, :]
         up[at, :] = chunk[32:64, :]
+        down[at, :] = chunk[64:96, :]
     x = plane[...]
     g = lax.dot_general(x, gate[...], NT, preferred_element_type=F32)
     u = lax.dot_general(x, up[...], NT, preferred_element_type=F32)
@@ -352,7 +367,10 @@
 def dense_first(plane, chunks):
     return pl.pallas_call(
         dense_body,
-        out_shape=jax.ShapeDtypeStruct((128, 256), BF16),
+        out_shape=[
+            jax.ShapeDtypeStruct((128, 256), BF16),
+            jax.ShapeDtypeStruct((256, D), BF16),
+        ],
         scratch_shapes=[pltpu.VMEM((256, D), BF16), pltpu.VMEM((256, D), BF16)],
         compiler_params=pltpu.CompilerParams(vmem_limit_bytes=12 * 2**20),
         name="dense_first",
@@ -389,11 +407,7 @@
     )(*arrived, *weights)
 
 
-def combine_body(
-    hidden, c0, c1, c2, c3, c4, c5, c6, c7, opening, weigh, b0, b1, b2, b3, out, down, back
-):
-    for r, chunk in enumerate((c0, c1, c2, c3, c4, c5, c6, c7)):
-        down[r * 32 : (r + 1) * 32, :] = chunk[64:96, :]
+def combine_body(hidden, down, opening, weigh, b0, b1, b2, b3, out, back):
     for k, b in enumerate((b0, b1, b2, b3)):
         back[k * 32 : (k + 1) * 32, :] = b[...]
         back[128 + k * 32 : 128 + (k + 1) * 32, :] = b[...]
@@ -405,14 +419,14 @@
         out[:, :, at] = term.astype(BF16).reshape(16, 8, 512)
 
 
-def combine(hidden, chunks, opening, weigh, back):
+def combine(hidden, down, opening, weigh, back):
     return pl.pallas_call(
         combine_body,
         out_shape=jax.ShapeDtypeStruct((16, 8, D), BF16),
-        scratch_shapes=[pltpu.VMEM((256, D), BF16), pltpu.VMEM((256, D), BF16)],
+        scratch_shapes=[pltpu.VMEM((256, D), BF16)],
         compiler_params=pltpu.CompilerParams(vmem_limit_bytes=12 * 2**20),
         name="combine",
-    )(hidden, *chunks, opening, weigh, *back)
+    )(hidden, down, opening, weigh, *back)
 
 
 def hoist_body(*refs):
@@ -500,32 +514,32 @@
     chunks = ring_gather(w4)
     got = plane_exchange(sent)
 
+    partial = project(got, chunks)
+    partial, positions, dense_gate, dense_up, dense_down = lax.optimization_barrier(
+        (partial, positions, dense_gate, dense_up, dense_down)
+    )
     angles = positions.astype(F32)[:, None] * FREQUENCY[None, :]
     cosine = jnp.cos(angles)
     sine = jnp.sin(angles) * TURN[None, :]
     dense = jnp.concatenate([dense_gate.T, dense_up.T, dense_down], axis=0)
-    partial = project(got, chunks)
-    partial, got, cosine, sine, dense = lax.optimization_barrier(
-        (partial, got, cosine, sine, dense)
-    )
     expert_own = (exp_gate, exp_up, exp_down)
     parts = plane_exchange(partial)
 
     out_chunks = ring_gather(w_out.T)
     dense_chunks = ring_gather(dense)
     expert_other = tuple(lax.ppermute(w, "tp", SWAP) for w in expert_own)
-    dense_chunks = dense_chunks + tuple(lax.ppermute(c, "tp", SWAP) for c in dense_chunks)
-    pick, weigh = routing(got)
-
     kept, keys, values = recall(parts, cosine, sine, head_gain, ret_state)
     kept = plane_exchange(kept)
-    kept, out_chunks, dense_chunks, expert_other, pick, weigh = lax.optimization_barrier(
-        (kept, out_chunks, dense_chunks, expert_other, pick, weigh)
-    )
+    pick, weigh = routing(got)
+    kept, out_chunks, dense_chunks, expert_other = lax.optimization_barrier(
+        (kept, out_chunks, dense_chunks, expert_other)
+    )
+    dense_chunks = dense_chunks + tuple(lax.ppermute(c, "tp", SWAP) for c in dense_chunks)
+
     keep, give = mix(kept, out_chunks)
     settled = settle(keep, lax.ppermute(give, "tp", SWAP), got)
     res = plane_exchange(settled)
-    new_state = renew(keys, values, ret_state)
+    new_state = renew(keys, values, ret_state, 0)
 
     plane, s0, s1, s2, s3, opening, own_res = spread(res, norm_ffn, branch_gate, pick)
     arrived = (
@@ -534,7 +548,9 @@
         lax.ppermute(s2, "x", ACROSS),
         lax.ppermute(s3, "x", LEFT),
     )
-    hidden = dense_first(plane, dense_chunks)
+    new_state = renew(keys, values, ret_state, 1, new_state)
+    plane, new_state = lax.optimization_barrier((plane, new_state))
+    hidden, down = dense_first(plane, dense_chunks)
     weights = tuple(w for pair in zip(expert_own, expert_other) for w in pair)
     weights = hoist(*weights)
     r0, r1, r2, r3 = experts(arrived, weights)
@@ -544,7 +560,7 @@
         lax.ppermute(r2, "x", ACROSS),
         lax.ppermute(r3, "x", RIGHT),
     )
-    branch = combine(hidden, dense_chunks, opening, weigh, back)
+    branch = combine(hidden, down, opening, weigh, back)
     terms = plane_exchange(branch)
     summed = jnp.sum(terms.astype(F32), axis=0)
     mine = (own_res.astype(F32) + summed).astype(BF16)

time: 164 us -> 150 us (0.915)
  waiting for transfers between devices: 49.9 us -> 39.7 us
  other arithmetic: 3.85 us -> 1.48 us
  blocking collectives: 29.6 us -> 27.7 us
  Pallas kernels: 25.2 us -> 27 us
    ppermute x1, starting transfers between devices: 1.65 us -> 12 us  [on_device(): settled = settle(keep, lax.ppermute(give, 'tp', SWAP), got)]
    all_to_all x3, waiting for transfers between devices: 9.18 us -> 19 us  [plane_exchange(): return lax.all_to_all(array, PLANE, split_axis=0, concat_axis=0, tiled=True)]
    ppermute x3, waiting for transfers between devices: 11.7 us -> 3.32 us  [ring_gather(): lax.ppermute(own, 'x', LEFT)]
    all_to_all x3, starting transfers between devices: 21.1 us -> 14.6 us  [plane_exchange(): return lax.all_to_all(array, PLANE, split_axis=0, concat_axis=0, tiled=True)]
    ppermute x3, waiting for transfers between devices: 10.4 us -> 4.32 us  [ring_gather(): lax.ppermute(own, 'x', ACROSS)]
    ppermute x1, starting transfers between devices: 3.56 us -> 0.3 us  [on_device(): lax.ppermute(r1, 'x', LEFT)]
    ppermute x1, starting transfers between devices: 0.01 us -> 2.69 us  [on_device(): lax.ppermute(r2, 'x', ACROSS)]
    ppermute x1, waiting for transfers between devices: 2.1 us -> 0.01 us  [on_device(): lax.ppermute(r1, 'x', LEFT)]
  transfers between devices with their start and end apart: 27 -> 27, of which waited for: 13 -> 10; matrix products, arithmetic and copies ran while one was open for 2% -> 0% of each run, Pallas kernels for 12% -> 15%
where the time goes in v3:
time: 150 us
  starting transfers between devices  51.8 us (35%)
  waiting for transfers between devices  39.7 us (26%)
  blocking collectives  27.7 us (18%)
  Pallas kernels  27 us (18%)
    all_to_all x2, blocking collectives, plane_exchange(): return lax.all_to_all(array, PLANE, split_axis=0, concat_axis=0, tiled=True)  27.7 us
    all_to_all x3, waiting for transfers between devices, plane_exchange(): return lax.all_to_all(array, PLANE, split_axis=0, concat_axis=0, tiled=True)  19 us
    all_to_all x3, starting transfers between devices, plane_exchange(): return lax.all_to_all(array, PLANE, split_axis=0, concat_axis=0, tiled=True)  14.6 us
    ppermute x1, starting transfers between devices, on_device(): settled = settle(keep, lax.ppermute(give, 'tp', SWAP), got)  12 us
    ppermute x3, waiting for transfers between devices, ring_gather(): lax.ppermute(own, 'x', RIGHT)  9.84 us
    pallas_call x2, Pallas kernels, renew(): pl.pallas_call(functools.partial(renew_body, half * HALF), in_specs=[VMEM...  8.1 us
    ppermute x4, starting transfers between devices, on_device(): lax.ppermute(c, 'tp', SWAP)  7.82 us
    pallas_call x1, Pallas kernels, recall(): pl.pallas_call(recall_body, in_specs=[VMEM, HBM, HBM, VMEM, HBM], out_spe...  5.86 us
  transfers between devices with their start and end apart: 27, of which 10 were waited for; matrix products, arithmetic and copies ran while one was open for 0% of the time, Pallas kernels for 15%

profile of v3, /device:TPU:1, one launch (start us, length us, event | category | flops | bytes accessed | tf_op | source)
XLA Modules:
  0.0 149.7 jit_solution(8217182599726234350)
XLA Ops:
  0.6 1.7 %prepare.1 = (bf16[16,32,128]{2,1,0:T(8,128)(2,1)}, bf16[4,32,768]{2,1,0:T(8,128)(2,1)}) custom-call(bf16[16,2048]{1,0:T(8,128)(2,1)} %x_ref.1, bf16[2048]{0:T(1024)(128)(2,1)} %gain.3, s32[4,16]{1,0:T(4,128)} %bitcast.11, bf16[4,16]{1,0:T(4,128)(2,1)} %bitcast.12, bf16[32,768]{1,0:T(8,128)(2,1)} %wq.1, bf16[32,768]{1,0:T(8,128)(2,1)} %wk.1, ...), custom_call_target="tpu_custom_call" | custom-call | tf_op jit(solution)/shard_map/prepare/pallas_call | solution.py:69
  2.3 2.0 %collective-permute-start = (bf16[4,32,768]{2,1,0:T(8,128)(2,1)}, bf16[4,32,768]{2,1,0:T(8,128)(2,1)S(1)}, u32[]{:S(2)}, u32[]{:S(2)}) collective-permute-start(bf16[4,32,768]{2,1,0:T(8,128)(2,1)} %get-tuple-element.50.c0), channel_id=1, source_target_pairs={{0,2},{2,4},{4,6},{6,0},{1,3},{3,5},{5,7},{7,1},{8,10},{10,12},{12... | collective-permute-start | bytes 589832 | tf_op jit(solution)/shard_map/ppermute | solution.py:32
  4.4 1.0 collective-permute-start.10
  5.3 0.5 collective-permute-start.9
  5.8 2.5 %collective-permute-start.1 = (bf16[4,32,768]{2,1,0:T(8,128)(2,1)}, bf16[4,32,768]{2,1,0:T(8,128)(2,1)S(1)}, u32[]{:S(2)}, u32[]{:S(2)}) collective-permute-start(bf16[4,32,768]{2,1,0:T(8,128)(2,1)} %get-tuple-element.50.c0), channel_id=1, source_target_pairs={{0,4},{2,6},{4,0},{6,2},{1,5},{3,7},{5,1},{7,3},{8,12},{10,14},{12... | collective-permute-start | bytes 589832 | tf_op jit(solution)/shard_map/ppermute | solution.py:33
  8.3 1.8 %collective-permute-done.c1 = bf16[4,32,768]{2,1,0:T(8,128)(2,1)S(1)} collective-permute-done((bf16[4,32,768]{2,1,0:T(8,128)(2,1)}, bf16[4,32,768]{2,1,0:T(8,128)(2,1)S(1)}, u32[]{:S(2)}, u32[]{:S(2)}) %collective-permute-start) | collective-permute-done | bytes 196640 | tf_op jit(solution)/shard_map/ppermute | solution.py:32
  10.1 1.6 %collective-permute-start.2 = (bf16[4,32,768]{2,1,0:T(8,128)(2,1)}, bf16[4,32,768]{2,1,0:T(8,128)(2,1)S(1)}, u32[]{:S(2)}, u32[]{:S(2)}) collective-permute-start(bf16[4,32,768]{2,1,0:T(8,128)(2,1)} %get-tuple-element.50.c0), channel_id=1, source_target_pairs={{0,6},{2,0},{4,2},{6,4},{1,7},{3,1},{5,3},{7,5},{8,14},{10,8},{12,... | collective-permute-start | bytes 589832 | tf_op jit(solution)/shard_map/ppermute | solution.py:34
  11.6 14.6 %all_to_all.25.x_ref.got = bf16[16,32,128]{2,1,0:T(8,128)(2,1)S(1)} all-to-all(bf16[16,32,128]{2,1,0:T(8,128)(2,1)} %get-tuple-element.49), channel_id=1, replica_groups=mesh['z'=4,'y'=4,'x'=4,'tp'=2] {'z','y'}, dimensions={0} | all-to-all | bytes 262144 | tf_op jit(solution)/shard_map/all_to_all | solution.py:459
  26.3 0.9 copy-done
  27.2 1.5 project.1
  28.7 0.0 copy-start.4
  28.7 0.0 copy-start.5
  28.7 0.0 copy-start.6
  28.7 0.0 copy-start.1
  28.7 0.0 copy-start.9
  28.7 0.0 copy-start.7
  28.7 0.0 copy-start.8
  28.8 4.5 %all-to-all-start.1 = ((bf16[16,16,3072]{2,1,0:T(8,128)(2,1)}), bf16[16,16,3072]{2,1,0:T(8,128)(2,1)}, u32[]{:S(2)}, u32[]{:S(2)}) async-start(bf16[16,16,3072]{2,1,0:T(8,128)(2,1)} %project.1), calls=%async_computation.1 | async-start | bytes 3145728 | tf_op jit(solution)/shard_map/all_to_all | solution.py:459
  33.4 0.3 collective-permute-start.6
  33.7 0.1 collective-permute-start.3
  33.8 8.0 %collective-permute-done.3.c1 = bf16[32,768]{1,0:T(8,128)(2,1)S(1)} collective-permute-done((bf16[32,768]{1,0:T(8,128)(2,1)S(1)}, bf16[32,768]{1,0:T(8,128)(2,1)S(1)}, u32[]{:S(2)}, u32[]{:S(2)}) %collective-permute-start.3) | collective-permute-done | bytes 49184 | tf_op jit(solution)/shard_map/ppermute | solution.py:32
  41.8 0.5 collective-permute-start.4
  42.3 4.3 %collective-permute-done.4.c2 = bf16[32,768]{1,0:T(8,128)(2,1)S(1)} collective-permute-done((bf16[32,768]{1,0:T(8,128)(2,1)S(1)}, bf16[32,768]{1,0:T(8,128)(2,1)S(1)}, u32[]{:S(2)}, u32[]{:S(2)}) %collective-permute-start.4) | collective-permute-done | bytes 49184 | tf_op jit(solution)/shard_map/ppermute | solution.py:33
  46.6 0.5 collective-permute-start.5
  47.1 3.3 %collective-permute-done.5.c3 = bf16[32,768]{1,0:T(8,128)(2,1)S(1)} collective-permute-done((bf16[32,768]{1,0:T(8,128)(2,1)S(1)}, bf16[32,768]{1,0:T(8,128)(2,1)S(1)}, u32[]{:S(2)}, u32[]{:S(2)}) %collective-permute-start.5) | collective-permute-done | bytes 49184 | tf_op jit(solution)/shard_map/ppermute | solution.py:34
  50.4 0.6 collective-permute-start.7
  51.0 1.2 collective-permute-start.8
  52.2 0.7 fusion
  52.9 0.0 all-to-all-done.1.parts
  52.9 5.9 %recall.1 = (bf16[16,16,768]{2,1,0:T(8,128)(2,1)}, f32[16,8,128]{2,1,0:T(8,128)}, f32[16,8,128]{2,1,0:T(8,128)}) custom-call(bf16[16,16,3072]{2,1,0:T(8,128)(2,1)} %all-to-all-done.1.parts, f32[16,128]{1,0:T(8,128)} %get-tuple-element.99.cosine_ref, f32[16,128]{1,0:T(8,128)} %get-tuple-element.98.sine_ref, bf16[768]{0:T(1024)(128)(2,1)} %gain.4, ...), custom_call_target="tpu_custom_call" | custom-call | tf_op jit(solution)/shard_map/recall/pallas_call | solution.py:204
  58.8 0.0 copy-start.2
  58.8 0.0 copy-start.3
  58.8 6.5 %all-to-all-start.2 = ((bf16[16,16,768]{2,1,0:T(8,128)(2,1)}), bf16[16,16,768]{2,1,0:T(8,128)(2,1)S(1)}, u32[]{:S(2)}, u32[]{:S(2)}) async-start(bf16[16,16,768]{2,1,0:T(8,128)(2,1)} %get-tuple-element.53), calls=%async_computation.2 | async-start | bytes 786432 | tf_op jit(solution)/shard_map/all_to_all | solution.py:459
  65.4 8.2 %all-to-all-done.2.kept = bf16[16,16,768]{2,1,0:T(8,128)(2,1)S(1)} async-done(((bf16[16,16,768]{2,1,0:T(8,128)(2,1)}), bf16[16,16,768]{2,1,0:T(8,128)(2,1)S(1)}, u32[]{:S(2)}, u32[]{:S(2)}) %all-to-all-start.2) | async-done | bytes 393248 | tf_op jit(solution)/shard_map/all_to_all | solution.py:459
  73.6 0.3 mix.1
  73.9 12.0 %collective-permute-start.12 = (bf16[16,8,128]{2,1,0:T(8,128)(2,1)S(1)}, bf16[16,8,128]{2,1,0:T(8,128)(2,1)S(1)}, u32[]{:S(2)}, u32[]{:S(2)}) collective-permute-start(bf16[16,8,128]{2,1,0:T(8,128)(2,1)S(1)} %get-tuple-element.63), channel_id=1, source_target_pairs={{0,1},{1,0},{2,3},{3,2},{4,5},{5,4},{6,7},{7,6},{8,9},{9,8},{10,11... | collective-permute-start | bytes 98312 | tf_op jit(solution)/shard_map/ppermute | solution.py:540
  86.0 0.9 collective-permute-done.12.other
  86.8 0.8 settle.1
  87.7 3.6 %all-to-all-start.3 = ((bf16[16,128,128]{2,1,0:T(8,128)(2,1)}), bf16[16,128,128]{2,1,0:T(8,128)(2,1)S(1)}, u32[]{:S(2)}, u32[]{:S(2)}) async-start(bf16[16,128,128]{2,1,0:T(8,128)(2,1)} %settle.1), calls=%async_computation.3 | async-start | bytes 1048576 | tf_op jit(solution)/shard_map/all_to_all | solution.py:459
  91.3 0.2 routing.1
  91.5 10.8 %all-to-all-done.3.res = bf16[16,128,128]{2,1,0:T(8,128)(2,1)S(1)} async-done(((bf16[16,128,128]{2,1,0:T(8,128)(2,1)}), bf16[16,128,128]{2,1,0:T(8,128)(2,1)S(1)}, u32[]{:S(2)}, u32[]{:S(2)}) %all-to-all-start.3) | async-done | bytes 524320 | tf_op jit(solution)/shard_map/all_to_all | solution.py:459
  102.2 0.6 spread.1
  102.9 0.1 collective-permute-start.17
  102.9 1.6 %collective-permute-start.13 = (bf16[96,2048]{1,0:T(8,128)(2,1)S(1)}, bf16[96,2048]{1,0:T(8,128)(2,1)S(1)}, u32[]{:S(2)}, u32[]{:S(2)}) collective-permute-start(bf16[96,2048]{1,0:T(8,128)(2,1)S(1)} %pad_maximum_fusion.c0), channel_id=1, source_target_pairs={{0,1},{1,0},{2,3},{3,2},{4,5},{5,4},{6,7},{7,6},{8,9},{9,8},{10,11... | collective-permute-start | bytes 1179656 | tf_op jit(solution)/shard_map/ppermute | solution.py:537
  104.5 0.1 collective-permute-start.14
  104.6 1.5 collective-permute-start.18
  106.1 0.7 collective-permute-start.15
  106.8 1.2 collective-permute-done.17.a1
  108.0 5.5 %collective-permute-start.16 = (bf16[96,2048]{1,0:T(8,128)(2,1)S(1)}, bf16[96,2048]{1,0:T(8,128)(2,1)S(1)}, u32[]{:S(2)}, u32[]{:S(2)}) collective-permute-start(bf16[96,2048]{1,0:T(8,128)(2,1)S(1)} %collective-permute-done.8.c3), channel_id=1, source_target_pairs={{0,1},{1,0},{2,3},{3,2},{4,5},{5,4},{6,7},{7,6},{8,9},{9,8},{10,11... | collective-permute-start | bytes 1179656 | tf_op jit(solution)/shard_map/ppermute | solution.py:537
  113.4 0.0 collective-permute-start.19
  113.4 4.7 %hoist.1 = (bf16[1,2048,512]{2,1,0:T(8,128)(2,1)S(1)}, bf16[1,2048,512]{2,1,0:T(8,128)(2,1)S(1)}, bf16[1,2048,512]{2,1,0:T(8,128)(2,1)S(1)}, bf16[1,2048,512]{2,...) custom-call(bf16[1,2048,512]{2,1,0:T(8,128)(2,1)} %refs_0_.1, ...), custom_call_target="tpu_custom_call" | custom-call | tf_op jit(solution)/shard_map/hoist/pallas_call | solution.py:447
  118.2 0.3 collective-permute-done.19.a3
  118.5 1.9 %experts.1 = (bf16[32,2048]{1,0:T(8,128)(2,1)S(1)}, bf16[32,2048]{1,0:T(8,128)(2,1)S(1)}, bf16[32,2048]{1,0:T(8,128)(2,1)S(1)}, bf16[32,2048]{1,0:T(8,128)(2,1)S(1)}) custom-call(bf16[32,2048]{1,0:T(8,128)(2,1)S(1)} %get-tuple-element.78.a0, bf16[32,2048]{1,0:T(8,128)(2,1)S(1)} %collective-permute-done.17.a1, ...), custom_call_target="tpu_custom_call" | custom-call | tf_op jit(solution)/shard_map/experts/pallas_call | solution.py:400
  120.4 0.3 collective-permute-start.20
  120.7 2.7 %collective-permute-start.21 = (bf16[32,2048]{1,0:T(8,128)(2,1)S(1)}, bf16[32,2048]{1,0:T(8,128)(2,1)S(1)}, u32[]{:S(2)}, u32[]{:S(2)}) collective-permute-start(bf16[32,2048]{1,0:T(8,128)(2,1)S(1)} %get-tuple-element.93), channel_id=1, source_target_pairs={{0,4},{2,6},{4,0},{6,2},{1,5},{3,7},{5,1},{7,3},{8,12},{10,14},{12... | collective-permute-start | bytes 393224 | tf_op jit(solution)/shard_map/ppermute | solution.py:560
  123.4 4.0 %shard_map.221.rest_0_ = f32[16,6,128,128]{3,2,1,0:T(8,128)} custom-call(f32[16,8,128]{2,1,0:T(8,128)} %get-tuple-element.67.keys, f32[16,8,128]{2,1,0:T(8,128)} %get-tuple-element.68.values, f32[16,6,128,128]{3,2,1,0:T(8,128)} %state_ref.5), custom_call_target="tpu_custom_call" | custom-call | tf_op jit(solution)/shard_map/pallas_call | solution.py:263
  127.5 4.0 %shard_map.222 = f32[16,6,128,128]{3,2,1,0:T(8,128)} custom-call(f32[16,8,128]{2,1,0:T(8,128)} %get-tuple-element.67.keys, f32[16,8,128]{2,1,0:T(8,128)} %get-tuple-element.68.values, f32[16,6,128,128]{3,2,1,0:T(8,128)} %state_ref.5, f32[16,6,128,128]{3,2,1,0:T(8,128)} %shard_map.221.rest_0_), custom_call_target="tpu_custom_call", output_to_operand_aliasing={{}: (3, {})} | custom-call | tf_op jit(solution)/shard_map/pallas_call | solution.py:263
  131.5 0.8 dense_first.1
  132.4 0.5 combine.1
  132.9 13.1 %all_to_all.26 = bf16[16,8,2048]{2,1,0:T(8,128)(2,1)S(1)} all-to-all(bf16[16,8,2048]{2,1,0:T(8,128)(2,1)S(1)} %combine.1), channel_id=1, replica_groups=mesh['z'=4,'y'=4,'x'=4,'tp'=2] {'z','y'}, dimensions={0} | all-to-all | bytes 1048576 | tf_op jit(solution)/shard_map/all_to_all | solution.py:459
  145.9 0.1 convert_reduce_fusion
  146.0 2.1 %collective-permute-start.23 = (bf16[8,2048]{1,0:T(8,128)(2,1)S(1)}, bf16[8,2048]{1,0:T(8,128)(2,1)S(1)}, u32[]{:S(2)}, u32[]{:S(2)}) collective-permute-start(bf16[8,2048]{1,0:T(8,128)(2,1)S(1)} %add_convert_fusion), channel_id=1, source_target_pairs={{0,1},{1,0},{2,3},{3,2},{4,5},{5,4},{6,7},{7,6},{8,9},{9,8},{10,11... | collective-permute-start | bytes 98312 | tf_op jit(solution)/shard_map/ppermute | solution.py:567
  148.2 0.9 collective-permute-done.23
  149.0 0.6 pad_maximum_fusion.1
  (32 shorter events, 0.1 us)
Async XLA Ops:
  2.3 7.7 %collective-permute-start = (bf16[4,32,768]{2,1,0:T(8,128)(2,1)}, bf16[4,32,768]{2,1,0:T(8,128)(2,1)S(1)}, u32[]{:S(2)}, u32[]{:S(2)}) collective-permute-start(bf16[4,32,768]{2,1,0:T(8,128)(2,1)} %get-tuple-element.50.c0), channel_id=1, source_target_pairs={{0,2},{2,4},{4,6},{6,0},{1,3},{3,5},{5,7},{7,1},{8,10},{10,12},{12... | collective-permute-start | bytes 589832 | tf_op jit(solution)/shard_map/ppermute | solution.py:32
  4.4 69.3 %collective-permute-start.10 = (bf16[1,2048,512]{2,1,0:T(8,128)(2,1)}, bf16[1,2048,512]{2,1,0:T(8,128)(2,1)}, u32[]{:S(2)}, u32[]{:S(2)}) collective-permute-start(bf16[1,2048,512]{2,1,0:T(8,128)(2,1)} %refs_2_.1), channel_id=1, source_target_pairs={{0,1},{1,0},{2,3},{3,2},{4,5},{5,4},{6,7},{7,6},{8,9},{9,8},{10,11... | collective-permute-start | bytes 6291464 | tf_op jit(solution)/shard_map/ppermute | solution.py:530
  5.3 68.3 %collective-permute-start.11 = (bf16[1,512,2048]{2,1,0:T(8,128)(2,1)}, bf16[1,512,2048]{2,1,0:T(8,128)(2,1)}, u32[]{:S(2)}, u32[]{:S(2)}) collective-permute-start(bf16[1,512,2048]{2,1,0:T(8,128)(2,1)} %refs_4_.1), channel_id=1, source_target_pairs={{0,1},{1,0},{2,3},{3,2},{4,5},{5,4},{6,7},{7,6},{8,9},{9,8},{10,11... | collective-permute-start | bytes 6291464 | tf_op jit(solution)/shard_map/ppermute | solution.py:530
  5.3 68.3 %collective-permute-start.9 = (bf16[1,2048,512]{2,1,0:T(8,128)(2,1)}, bf16[1,2048,512]{2,1,0:T(8,128)(2,1)}, u32[]{:S(2)}, u32[]{:S(2)}) collective-permute-start(bf16[1,2048,512]{2,1,0:T(8,128)(2,1)} %refs_0_.1), channel_id=1, source_target_pairs={{0,1},{1,0},{2,3},{3,2},{4,5},{5,4},{6,7},{7,6},{8,9},{9,8},{10,11... | collective-permute-start | bytes 6291464 | tf_op jit(solution)/shard_map/ppermute | solution.py:530
  5.8 20.4 %collective-permute-start.1 = (bf16[4,32,768]{2,1,0:T(8,128)(2,1)}, bf16[4,32,768]{2,1,0:T(8,128)(2,1)S(1)}, u32[]{:S(2)}, u32[]{:S(2)}) collective-permute-start(bf16[4,32,768]{2,1,0:T(8,128)(2,1)} %get-tuple-element.50.c0), channel_id=1, source_target_pairs={{0,4},{2,6},{4,0},{6,2},{1,5},{3,7},{5,1},{7,3},{8,12},{10,14},{12... | collective-permute-start | bytes 589832 | tf_op jit(solution)/shard_map/ppermute | solution.py:33
  10.1 16.2 %collective-permute-start.2 = (bf16[4,32,768]{2,1,0:T(8,128)(2,1)}, bf16[4,32,768]{2,1,0:T(8,128)(2,1)S(1)}, u32[]{:S(2)}, u32[]{:S(2)}) collective-permute-start(bf16[4,32,768]{2,1,0:T(8,128)(2,1)} %get-tuple-element.50.c0), channel_id=1, source_target_pairs={{0,6},{2,0},{4,2},{6,4},{1,7},{3,1},{5,3},{7,5},{8,14},{10,8},{12,... | collective-permute-start | bytes 589832 | tf_op jit(solution)/shard_map/ppermute | solution.py:34
  26.3 0.9 copy-start
  28.7 4.6 %copy-start.4 = (bf16[32,2048]{1,0:T(8,128)(2,1)S(1)}, bf16[32,2048]{1,0:T(8,128)(2,1)}, u32[]{:S(2)}) copy-start(bf16[32,2048]{1,0:T(8,128)(2,1)} %param.40) | copy-start | bytes 393220
  28.7 4.6 %copy-start.5 = (bf16[2048,32]{0,1:T(8,128)(2,1)S(1)}, bf16[2048,32]{0,1:T(8,128)(2,1)}, u32[]{:S(2)}) copy-start(bf16[2048,32]{0,1:T(8,128)(2,1)} %param.39) | copy-start | bytes 393220
  28.7 4.6 %copy-start.6 = (bf16[2048,32]{0,1:T(8,128)(2,1)S(1)}, bf16[2048,32]{0,1:T(8,128)(2,1)}, u32[]{:S(2)}) copy-start(bf16[2048,32]{0,1:T(8,128)(2,1)} %param.38) | copy-start | bytes 393220
  28.7 5.0 %copy-start.1 = (bf16[768,32]{0,1:T(8,128)(2,1)S(1)}, bf16[768,32]{0,1:T(8,128)(2,1)}, u32[]{:S(2)}) copy-start(bf16[768,32]{0,1:T(8,128)(2,1)} %param.31) | copy-start | bytes 147460
  28.7 18.4 %copy-start.9 = (s32[16]{0:T(128)S(1)}, s32[16]{0:T(128)}, u32[]{:S(2)}) copy-start(s32[16]{0:T(128)} %param.23) | copy-start | bytes 196
  28.7 23.5 %copy-start.7 = (f32[128]{0:T(128)S(1)}, f32[128]{0:T(128)}, u32[]{:S(2)}) copy-start(f32[128]{0:T(128)} %constant.30) | copy-start | bytes 1540
  28.7 23.5 %copy-start.8 = (f32[128]{0:T(128)S(1)}, f32[128]{0:T(128)}, u32[]{:S(2)}) copy-start(f32[128]{0:T(128)} %constant.31) | copy-start | bytes 1540
  28.8 24.2 %all-to-all-start.1 = ((bf16[16,16,3072]{2,1,0:T(8,128)(2,1)}), bf16[16,16,3072]{2,1,0:T(8,128)(2,1)}, u32[]{:S(2)}, u32[]{:S(2)}) async-start(bf16[16,16,3072]{2,1,0:T(8,128)(2,1)} %project.1), calls=%async_computation.1 | async-start | bytes 3145728 | tf_op jit(solution)/shard_map/all_to_all | solution.py:459
  33.4 17.7 %collective-permute-start.6 = (bf16[96,2048]{1,0:T(8,128)(2,1)S(1)}, bf16[96,2048]{1,0:T(8,128)(2,1)S(1)}, u32[]{:S(2)}, u32[]{:S(2)}) collective-permute-start(bf16[96,2048]{1,0:T(8,128)(2,1)S(1)} %pad_maximum_fusion.c0), channel_id=1, source_target_pairs={{0,2},{2,4},{4,6},{6,0},{1,3},{3,5},{5,7},{7,1},{8,10},{10,12},{12... | collective-permute-start | bytes 1179656 | tf_op jit(solution)/shard_map/ppermute | solution.py:32
  33.7 8.1 %collective-permute-start.3 = (bf16[32,768]{1,0:T(8,128)(2,1)S(1)}, bf16[32,768]{1,0:T(8,128)(2,1)S(1)}, u32[]{:S(2)}, u32[]{:S(2)}) collective-permute-start(bf16[32,768]{1,0:T(8,128)(2,1)S(1)} %bitcast.5), channel_id=1, source_target_pairs={{0,2},{2,4},{4,6},{6,0},{1,3},{3,5},{5,7},{7,1},{8,10},{10,12},{12... | collective-permute-start | bytes 147464 | tf_op jit(solution)/shard_map/ppermute | solution.py:32
  41.8 4.8 %collective-permute-start.4 = (bf16[32,768]{1,0:T(8,128)(2,1)S(1)}, bf16[32,768]{1,0:T(8,128)(2,1)S(1)}, u32[]{:S(2)}, u32[]{:S(2)}) collective-permute-start(bf16[32,768]{1,0:T(8,128)(2,1)S(1)} %bitcast.6), channel_id=1, source_target_pairs={{0,4},{2,6},{4,0},{6,2},{1,5},{3,7},{5,1},{7,3},{8,12},{10,14},{12... | collective-permute-start | bytes 147464 | tf_op jit(solution)/shard_map/ppermute | solution.py:33
  46.6 3.8 %collective-permute-start.5 = (bf16[32,768]{1,0:T(8,128)(2,1)S(1)}, bf16[32,768]{1,0:T(8,128)(2,1)S(1)}, u32[]{:S(2)}, u32[]{:S(2)}) collective-permute-start(bf16[32,768]{1,0:T(8,128)(2,1)S(1)} %bitcast.7), channel_id=1, source_target_pairs={{0,6},{2,0},{4,2},{6,4},{1,7},{3,1},{5,3},{7,5},{8,14},{10,8},{12,... | collective-permute-start | bytes 147464 | tf_op jit(solution)/shard_map/ppermute | solution.py:34
  50.4 14.9 %collective-permute-start.7 = (bf16[96,2048]{1,0:T(8,128)(2,1)S(1)}, bf16[96,2048]{1,0:T(8,128)(2,1)S(1)}, u32[]{:S(2)}, u32[]{:S(2)}) collective-permute-start(bf16[96,2048]{1,0:T(8,128)(2,1)S(1)} %pad_maximum_fusion.c0), channel_id=1, source_target_pairs={{0,4},{2,6},{4,0},{6,2},{1,5},{3,7},{5,1},{7,3},{8,12},{10,14},{12... | collective-permute-start | bytes 1179656 | tf_op jit(solution)/shard_map/ppermute | solution.py:33
  51.0 14.4 %collective-permute-start.8 = (bf16[96,2048]{1,0:T(8,128)(2,1)S(1)}, bf16[96,2048]{1,0:T(8,128)(2,1)S(1)}, u32[]{:S(2)}, u32[]{:S(2)}) collective-permute-start(bf16[96,2048]{1,0:T(8,128)(2,1)S(1)} %pad_maximum_fusion.c0), channel_id=1, source_target_pairs={{0,6},{2,0},{4,2},{6,4},{1,7},{3,1},{5,3},{7,5},{8,14},{10,8},{12,... | collective-permute-start | bytes 1179656 | tf_op jit(solution)/shard_map/ppermute | solution.py:34
  58.8 43.4 %copy-start.2 = (bf16[2048]{0:T(1024)(128)(2,1)S(1)}, bf16[2048]{0:T(1024)(128)(2,1)}, u32[]{:S(2)}) copy-start(bf16[2048]{0:T(1024)(128)(2,1)} %gain.5) | copy-start | bytes 12292
  58.8 43.4 %copy-start.3 = (bf16[2048]{0:T(1024)(128)(2,1)S(1)}, bf16[2048]{0:T(1024)(128)(2,1)}, u32[]{:S(2)}) copy-start(bf16[2048]{0:T(1024)(128)(2,1)} %branch.1) | copy-start | bytes 12292
  58.8 14.8 %all-to-all-start.2 = ((bf16[16,16,768]{2,1,0:T(8,128)(2,1)}), bf16[16,16,768]{2,1,0:T(8,128)(2,1)S(1)}, u32[]{:S(2)}, u32[]{:S(2)}) async-start(bf16[16,16,768]{2,1,0:T(8,128)(2,1)} %get-tuple-element.53), calls=%async_computation.2 | async-start | bytes 786432 | tf_op jit(solution)/shard_map/all_to_all | solution.py:459
  73.9 12.9 %collective-permute-start.12 = (bf16[16,8,128]{2,1,0:T(8,128)(2,1)S(1)}, bf16[16,8,128]{2,1,0:T(8,128)(2,1)S(1)}, u32[]{:S(2)}, u32[]{:S(2)}) collective-permute-start(bf16[16,8,128]{2,1,0:T(8,128)(2,1)S(1)} %get-tuple-element.63), channel_id=1, source_target_pairs={{0,1},{1,0},{2,3},{3,2},{4,5},{5,4},{6,7},{7,6},{8,9},{9,8},{10,11... | collective-permute-start | bytes 98312 | tf_op jit(solution)/shard_map/ppermute | solution.py:540
  87.7 14.5 %all-to-all-start.3 = ((bf16[16,128,128]{2,1,0:T(8,128)(2,1)}), bf16[16,128,128]{2,1,0:T(8,128)(2,1)S(1)}, u32[]{:S(2)}, u32[]{:S(2)}) async-start(bf16[16,128,128]{2,1,0:T(8,128)(2,1)} %settle.1), calls=%async_computation.3 | async-start | bytes 1048576 | tf_op jit(solution)/shard_map/all_to_all | solution.py:459
  102.9 5.1 %collective-permute-start.17 = (bf16[32,2048]{1,0:T(8,128)(2,1)S(1)}, bf16[32,2048]{1,0:T(8,128)(2,1)S(1)}, u32[]{:S(2)}, u32[]{:S(2)}) collective-permute-start(bf16[32,2048]{1,0:T(8,128)(2,1)S(1)} %get-tuple-element.79), channel_id=1, source_target_pairs={{0,2},{2,4},{4,6},{6,0},{1,3},{3,5},{5,7},{7,1},{8,10},{10,12},{12... | collective-permute-start | bytes 393224 | tf_op jit(solution)/shard_map/ppermute | solution.py:547
  102.9 17.8 %collective-permute-start.13 = (bf16[96,2048]{1,0:T(8,128)(2,1)S(1)}, bf16[96,2048]{1,0:T(8,128)(2,1)S(1)}, u32[]{:S(2)}, u32[]{:S(2)}) collective-permute-start(bf16[96,2048]{1,0:T(8,128)(2,1)S(1)} %pad_maximum_fusion.c0), channel_id=1, source_target_pairs={{0,1},{1,0},{2,3},{3,2},{4,5},{5,4},{6,7},{7,6},{8,9},{9,8},{10,11... | collective-permute-start | bytes 1179656 | tf_op jit(solution)/shard_map/ppermute | solution.py:537
  104.5 18.9 %collective-permute-start.14 = (bf16[96,2048]{1,0:T(8,128)(2,1)S(1)}, bf16[96,2048]{1,0:T(8,128)(2,1)S(1)}, u32[]{:S(2)}, u32[]{:S(2)}) collective-permute-start(bf16[96,2048]{1,0:T(8,128)(2,1)S(1)} %collective-permute-done.6.c1), channel_id=1, source_target_pairs={{0,1},{1,0},{2,3},{3,2},{4,5},{5,4},{6,7},{7,6},{8,9},{9,8},{10,11... | collective-permute-start | bytes 1179656 | tf_op jit(solution)/shard_map/ppermute | solution.py:537
  104.6 8.8 %collective-permute-start.18 = (bf16[32,2048]{1,0:T(8,128)(2,1)S(1)}, bf16[32,2048]{1,0:T(8,128)(2,1)S(1)}, u32[]{:S(2)}, u32[]{:S(2)}) collective-permute-start(bf16[32,2048]{1,0:T(8,128)(2,1)S(1)} %get-tuple-element.80), channel_id=1, source_target_pairs={{0,4},{2,6},{4,0},{6,2},{1,5},{3,7},{5,1},{7,3},{8,12},{10,14},{12... | collective-permute-start | bytes 393224 | tf_op jit(solution)/shard_map/ppermute | solution.py:548
  106.1 25.4 %collective-permute-start.15 = (bf16[96,2048]{1,0:T(8,128)(2,1)S(1)}, bf16[96,2048]{1,0:T(8,128)(2,1)S(1)}, u32[]{:S(2)}, u32[]{:S(2)}) collective-permute-start(bf16[96,2048]{1,0:T(8,128)(2,1)S(1)} %collective-permute-done.7.c2), channel_id=1, source_target_pairs={{0,1},{1,0},{2,3},{3,2},{4,5},{5,4},{6,7},{7,6},{8,9},{9,8},{10,11... | collective-permute-start | bytes 1179656 | tf_op jit(solution)/shard_map/ppermute | solution.py:537
  108.0 23.6 %collective-permute-start.16 = (bf16[96,2048]{1,0:T(8,128)(2,1)S(1)}, bf16[96,2048]{1,0:T(8,128)(2,1)S(1)}, u32[]{:S(2)}, u32[]{:S(2)}) collective-permute-start(bf16[96,2048]{1,0:T(8,128)(2,1)S(1)} %collective-permute-done.8.c3), channel_id=1, source_target_pairs={{0,1},{1,0},{2,3},{3,2},{4,5},{5,4},{6,7},{7,6},{8,9},{9,8},{10,11... | collective-permute-start | bytes 1179656 | tf_op jit(solution)/shard_map/ppermute | solution.py:537
  113.4 5.1 %collective-permute-start.19 = (bf16[32,2048]{1,0:T(8,128)(2,1)S(1)}, bf16[32,2048]{1,0:T(8,128)(2,1)S(1)}, u32[]{:S(2)}, u32[]{:S(2)}) collective-permute-start(bf16[32,2048]{1,0:T(8,128)(2,1)S(1)} %get-tuple-element.81), channel_id=1, source_target_pairs={{0,6},{2,0},{4,2},{6,4},{1,7},{3,1},{5,3},{7,5},{8,14},{10,8},{12,... | collective-permute-start | bytes 393224 | tf_op jit(solution)/shard_map/ppermute | solution.py:549
  120.4 12.0 %collective-permute-start.20 = (bf16[32,2048]{1,0:T(8,128)(2,1)S(1)}, bf16[32,2048]{1,0:T(8,128)(2,1)S(1)}, u32[]{:S(2)}, u32[]{:S(2)}) collective-permute-start(bf16[32,2048]{1,0:T(8,128)(2,1)S(1)} %get-tuple-element.92), channel_id=1, source_target_pairs={{0,6},{2,0},{4,2},{6,4},{1,7},{3,1},{5,3},{7,5},{8,14},{10,8},{12,... | collective-permute-start | bytes 393224 | tf_op jit(solution)/shard_map/ppermute | solution.py:559
  120.7 11.7 %collective-permute-start.21 = (bf16[32,2048]{1,0:T(8,128)(2,1)S(1)}, bf16[32,2048]{1,0:T(8,128)(2,1)S(1)}, u32[]{:S(2)}, u32[]{:S(2)}) collective-permute-start(bf16[32,2048]{1,0:T(8,128)(2,1)S(1)} %get-tuple-element.93), channel_id=1, source_target_pairs={{0,4},{2,6},{4,0},{6,2},{1,5},{3,7},{5,1},{7,3},{8,12},{10,14},{12... | collective-permute-start | bytes 393224 | tf_op jit(solution)/shard_map/ppermute | solution.py:560
  123.4 9.0 %collective-permute-start.22 = (bf16[32,2048]{1,0:T(8,128)(2,1)S(1)}, bf16[32,2048]{1,0:T(8,128)(2,1)S(1)}, u32[]{:S(2)}, u32[]{:S(2)}) collective-permute-start(bf16[32,2048]{1,0:T(8,128)(2,1)S(1)} %get-tuple-element.94), channel_id=1, source_target_pairs={{0,2},{2,4},{4,6},{6,0},{1,3},{3,5},{5,7},{7,1},{8,10},{10,12},{12... | collective-permute-start | bytes 393224 | tf_op jit(solution)/shard_map/ppermute | solution.py:561
  146.0 3.0 %collective-permute-start.23 = (bf16[8,2048]{1,0:T(8,128)(2,1)S(1)}, bf16[8,2048]{1,0:T(8,128)(2,1)S(1)}, u32[]{:S(2)}, u32[]{:S(2)}) collective-permute-start(bf16[8,2048]{1,0:T(8,128)(2,1)S(1)} %add_convert_fusion), channel_id=1, source_target_pairs={{0,1},{1,0},{2,3},{3,2},{4,5},{5,4},{6,7},{7,6},{8,9},{9,8},{10,11... | collective-permute-start | bytes 98312 | tf_op jit(solution)/shard_map/ppermute | solution.py:567

commit v4 on v2

--- a/solution.py
+++ b/solution.py
@@ -109,8 +109,9 @@
     )(got, *chunks)
 
 
-PER_STEP = 2
+PER_STEP = 4
 STEPS = 16 // PER_STEP
+AHEAD = 4
 FREQUENCY = np.tile(10000.0 ** (-np.arange(64) * 2.0 / 128), 2).astype(np.float32)
 TURN = np.repeat([-1.0, 1.0], 64).astype(np.float32)
 GAMMA = [float(np.exp(np.log1p(-(2.0 ** (-5.0 - 5.0 * h / (HEADS - 1)))))) for h in range(HEADS)]
@@ -145,7 +146,7 @@
             state_ref.at[some_rows(i)], buf.at[some_rows(i)], sems.at[i]
         )
 
-    for i in range(STEPS):
+    for i in range(AHEAD):
         fetch(i).start()
     gamma = gammas()
     for c in fetch_turns:
@@ -173,6 +174,11 @@
 
     def some(i, carry):
         fetch(i).wait()
+
+        @pl.when(i + AHEAD < STEPS)
+        def _():
+            fetch(i + AHEAD).start()
+
         for j in range(PER_STEP):
             t = i * PER_STEP + j
             for h in range(6):
@@ -338,11 +344,14 @@
     )(res, gain, branch, pick)
 
 
-def dense_body(plane, c0, c1, c2, c3, c4, c5, c6, c7, hidden, gate, up):
-    for r, chunk in enumerate((c0, c1, c2, c3, c4, c5, c6, c7)):
-        at = slice(r * 32, (r + 1) * 32)
-        gate[at, :] = chunk[0:32, :]
-        up[at, :] = chunk[32:64, :]
+def dense_body(plane, c0, c1, c2, c3, hidden, down, gate, up):
+    for r, chunk in enumerate((c0, c1, c2, c3)):
+        for q in range(2):
+            at = slice((2 * r + q) * 32, (2 * r + q + 1) * 32)
+            low = q * 96
+            gate[at, :] = chunk[low : low + 32, :]
+            up[at, :] = chunk[low + 32 : low + 64, :]
+            down[at, :] = chunk[low + 64 : low + 96, :]
     x = plane[...]
     g = lax.dot_general(x, gate[...], NT, preferred_element_type=F32)
     u = lax.dot_general(x, up[...], NT, preferred_element_type=F32)
@@ -352,7 +361,10 @@
 def dense_first(plane, chunks):
     return pl.pallas_call(
         dense_body,
-        out_shape=jax.ShapeDtypeStruct((128, 256), BF16),
+        out_shape=[
+            jax.ShapeDtypeStruct((128, 256), BF16),
+            jax.ShapeDtypeStruct((256, D), BF16),
+        ],
         scratch_shapes=[pltpu.VMEM((256, D), BF16), pltpu.VMEM((256, D), BF16)],
         compiler_params=pltpu.CompilerParams(vmem_limit_bytes=12 * 2**20),
         name="dense_first",
@@ -389,11 +401,7 @@
     )(*arrived, *weights)
 
 
-def combine_body(
-    hidden, c0, c1, c2, c3, c4, c5, c6, c7, opening, weigh, b0, b1, b2, b3, out, down, back
-):
-    for r, chunk in enumerate((c0, c1, c2, c3, c4, c5, c6, c7)):
-        down[r * 32 : (r + 1) * 32, :] = chunk[64:96, :]
+def combine_body(hidden, down, opening, weigh, b0, b1, b2, b3, out, back):
     for k, b in enumerate((b0, b1, b2, b3)):
         back[k * 32 : (k + 1) * 32, :] = b[...]
         back[128 + k * 32 : 128 + (k + 1) * 32, :] = b[...]
@@ -405,14 +413,14 @@
         out[:, :, at] = term.astype(BF16).reshape(16, 8, 512)
 
 
-def combine(hidden, chunks, opening, weigh, back):
+def combine(hidden, down, opening, weigh, back):
     return pl.pallas_call(
         combine_body,
         out_shape=jax.ShapeDtypeStruct((16, 8, D), BF16),
-        scratch_shapes=[pltpu.VMEM((256, D), BF16), pltpu.VMEM((256, D), BF16)],
+        scratch_shapes=[pltpu.VMEM((256, D), BF16)],
         compiler_params=pltpu.CompilerParams(vmem_limit_bytes=12 * 2**20),
         name="combine",
-    )(hidden, *chunks, opening, weigh, *back)
+    )(hidden, down, opening, weigh, *back)
 
 
 def hoist_body(*refs):
@@ -500,31 +508,29 @@
     chunks = ring_gather(w4)
     got = plane_exchange(sent)
 
+    partial = project(got, chunks)
+    partial, positions, dense_gate, dense_up, dense_down = lax.optimization_barrier(
+        (partial, positions, dense_gate, dense_up, dense_down)
+    )
     angles = positions.astype(F32)[:, None] * FREQUENCY[None, :]
     cosine = jnp.cos(angles)
     sine = jnp.sin(angles) * TURN[None, :]
     dense = jnp.concatenate([dense_gate.T, dense_up.T, dense_down], axis=0)
-    partial = project(got, chunks)
-    partial, got, cosine, sine, dense = lax.optimization_barrier(
-        (partial, got, cosine, sine, dense)
-    )
     expert_own = (exp_gate, exp_up, exp_down)
     parts = plane_exchange(partial)
 
+    dense_other = lax.ppermute(dense, "tp", SWAP)
     out_chunks = ring_gather(w_out.T)
-    dense_chunks = ring_gather(dense)
+    dense_chunks = ring_gather(jnp.concatenate([dense, dense_other], axis=0))
     expert_other = tuple(lax.ppermute(w, "tp", SWAP) for w in expert_own)
-    dense_chunks = dense_chunks + tuple(lax.ppermute(c, "tp", SWAP) for c in dense_chunks)
-    pick, weigh = routing(got)
-
     kept, keys, values = recall(parts, cosine, sine, head_gain, ret_state)
     kept = plane_exchange(kept)
-    kept, out_chunks, dense_chunks, expert_other, pick, weigh = lax.optimization_barrier(
-        (kept, out_chunks, dense_chunks, expert_other, pick, weigh)
-    )
+    pick, weigh = routing(got)
+    kept, out_chunks, expert_other = lax.optimization_barrier((kept, out_chunks, expert_other))
     keep, give = mix(kept, out_chunks)
     settled = settle(keep, lax.ppermute(give, "tp", SWAP), got)
     res = plane_exchange(settled)
+    res, dense_chunks = lax.optimization_barrier((res, dense_chunks))
     new_state = renew(keys, values, ret_state)
 
     plane, s0, s1, s2, s3, opening, own_res = spread(res, norm_ffn, branch_gate, pick)
@@ -534,7 +540,7 @@
         lax.ppermute(s2, "x", ACROSS),
         lax.ppermute(s3, "x", LEFT),
     )
-    hidden = dense_first(plane, dense_chunks)
+    hidden, down = dense_first(plane, dense_chunks)
     weights = tuple(w for pair in zip(expert_own, expert_other) for w in pair)
     weights = hoist(*weights)
     r0, r1, r2, r3 = experts(arrived, weights)
@@ -544,7 +550,7 @@
         lax.ppermute(r2, "x", ACROSS),
         lax.ppermute(r3, "x", RIGHT),
     )
-    branch = combine(hidden, dense_chunks, opening, weigh, back)
+    branch = combine(hidden, down, opening, weigh, back)
     terms = plane_exchange(branch)
     summed = jnp.sum(terms.astype(F32), axis=0)
     mine = (own_res.astype(F32) + summed).astype(BF16)

time: 164 us -> 156 us (0.951)
  blocking collectives: 29.6 us -> 17.2 us
  waiting for transfers between devices: 49.9 us -> 53.4 us
    all_to_all x3 -> x4, waiting for transfers between devices: 9.18 us -> 23.1 us  [plane_exchange(): return lax.all_to_all(array, PLANE, split_axis=0, concat_axis=0, tiled=True)]
    all_to_all x2 -> x1, blocking collectives: 29.6 us -> 17.2 us  [plane_exchange(): return lax.all_to_all(array, PLANE, split_axis=0, concat_axis=0, tiled=True)]
    ppermute x3, waiting for transfers between devices: 11 us -> 0.87 us  [ring_gather(): lax.ppermute(own, 'x', RIGHT)]
    ppermute x3, waiting for transfers between devices: 11.7 us -> 3.04 us  [ring_gather(): lax.ppermute(own, 'x', LEFT)]
    ppermute x3, waiting for transfers between devices: 10.4 us -> 17.9 us  [ring_gather(): lax.ppermute(own, 'x', ACROSS)]
    ppermute x4 -> x1, starting transfers between devices: 7.43 us -> 2.37 us  [on_device(): dense_other = lax.ppermute(dense, 'tp', SWAP)]
    all_to_all x3 -> x4, starting transfers between devices: 21.1 us -> 23.5 us  [plane_exchange(): return lax.all_to_all(array, PLANE, split_axis=0, concat_axis=0, tiled=True)]
    ppermute x1, waiting for transfers between devices: 1.48 us -> 3.29 us  [on_device(): lax.ppermute(r3, 'x', RIGHT)]
  transfers between devices with their start and end apart: 27 -> 25, of which waited for: 13 -> 12; matrix products, arithmetic and copies ran while one was open for 2% -> 1% of each run, Pallas kernels for 12% -> 15%
where the time goes in v4:
time: 156 us; the launch traced here: 155 us
  starting transfers between devices  53.4 us (34%)
  waiting for transfers between devices  53.4 us (34%)
  Pallas kernels  25.6 us (16%)
  blocking collectives  17.2 us (11%)
  other arithmetic  2.53 us (2%)
  local copies, waits for them, and re-layouts  2.13 us (1%)
    all_to_all x4, starting transfers between devices, plane_exchange(): return lax.all_to_all(array, PLANE, split_axis=0, concat_axis=0, tiled=True)  23.5 us
    all_to_all x4, waiting for transfers between devices, plane_exchange(): return lax.all_to_all(array, PLANE, split_axis=0, concat_axis=0, tiled=True)  23.1 us
    ppermute x3, waiting for transfers between devices, ring_gather(): lax.ppermute(own, 'x', ACROSS)  17.9 us
    all_to_all x1, blocking collectives, plane_exchange(): return lax.all_to_all(array, PLANE, split_axis=0, concat_axis=0, tiled=True)  17.2 us
    pallas_call x1, Pallas kernels, recall(): pl.pallas_call(recall_body, in_specs=[VMEM, HBM, HBM, VMEM, HBM], out_spe...  5.79 us
    pallas_call x1, Pallas kernels, renew(): pl.pallas_call(renew_body, in_specs=[VMEM, VMEM, HBM], out_specs=HBM, out...  5.52 us
    pallas_call x1, Pallas kernels, hoist(): pl.pallas_call(hoist_body, in_specs=[HBM] * len(arrays), out_specs=[VMEM]...  4.7 us
    ppermute x3, starting transfers between devices, ring_gather(): lax.ppermute(own, 'x', ACROSS)  4.54 us
  transfers between devices with their start and end apart: 25, of which 12 were waited for; matrix products, arithmetic and copies ran while one was open for 1% of the time, Pallas kernels for 15%

profile of v4, /device:TPU:1, one launch (start us, length us, event | category | flops | bytes accessed | tf_op | source)
XLA Modules:
  0.0 155.1 jit_solution(4434184042878868188)
XLA Ops:
  0.6 1.5 collective-permute-start.6
  2.1 1.7 %prepare.1 = (bf16[16,32,128]{2,1,0:T(8,128)(2,1)}, bf16[4,32,768]{2,1,0:T(8,128)(2,1)}) custom-call(bf16[16,2048]{1,0:T(8,128)(2,1)} %x_ref.1, bf16[2048]{0:T(1024)(128)(2,1)} %gain.3, s32[4,16]{1,0:T(4,128)} %bitcast.13, bf16[4,16]{1,0:T(4,128)(2,1)} %bitcast.14, bf16[32,768]{1,0:T(8,128)(2,1)} %wq.1, bf16[32,768]{1,0:T(8,128)(2,1)} %wk.1, ...), custom_call_target="tpu_custom_call" | custom-call | tf_op jit(solution)/shard_map/prepare/pallas_call | solution.py:67
  3.8 1.3 collective-permute-start
  5.1 2.5 %collective-permute-start.1 = (bf16[4,32,768]{2,1,0:T(8,128)(2,1)}, bf16[4,32,768]{2,1,0:T(8,128)(2,1)S(1)}, u32[]{:S(2)}, u32[]{:S(2)}) collective-permute-start(bf16[4,32,768]{2,1,0:T(8,128)(2,1)} %get-tuple-element.49.c0), channel_id=1, source_target_pairs={{0,4},{2,6},{4,0},{6,2},{1,5},{3,7},{5,1},{7,3},{8,12},{10,14},{12... | collective-permute-start | bytes 589832 | tf_op jit(solution)/shard_map/ppermute | solution.py:31
  7.6 1.2 collective-permute-start.2
  8.7 7.8 %all-to-all-start = ((bf16[16,32,128]{2,1,0:T(8,128)(2,1)}), bf16[16,32,128]{2,1,0:T(8,128)(2,1)S(1)}, u32[]{:S(2)}, u32[]{:S(2)}) async-start(bf16[16,32,128]{2,1,0:T(8,128)(2,1)} %get-tuple-element.48), calls=%async_computation | async-start | bytes 262144 | tf_op jit(solution)/shard_map/all_to_all | solution.py:453
  16.5 1.2 collective-permute-start.7
  17.7 0.1 collective-permute-start.8
  17.8 5.5 %all-to-all-done.x_ref.got = bf16[16,32,128]{2,1,0:T(8,128)(2,1)S(1)} async-done(((bf16[16,32,128]{2,1,0:T(8,128)(2,1)}), bf16[16,32,128]{2,1,0:T(8,128)(2,1)S(1)}, u32[]{:S(2)}, u32[]{:S(2)}) %all-to-all-start) | async-done | bytes 131104 | tf_op jit(solution)/shard_map/all_to_all | solution.py:453
  23.3 0.0 collective-permute-done.1.c2
  23.4 0.9 copy-done
  24.3 1.5 project.1
  25.8 0.0 copy-start.5
  25.8 0.0 copy-start.6
  25.8 0.0 copy-start.7
  25.8 0.0 copy-start.1
  25.8 0.0 copy-start.10
  25.8 0.0 copy-start.8
  25.8 0.0 copy-start.9
  25.9 3.9 %all-to-all-start.1 = ((bf16[16,16,3072]{2,1,0:T(8,128)(2,1)}), bf16[16,16,3072]{2,1,0:T(8,128)(2,1)S(1)}, u32[]{:S(2)}, u32[]{:S(2)}) async-start(bf16[16,16,3072]{2,1,0:T(8,128)(2,1)} %project.1), calls=%async_computation.1 | async-start | bytes 3145728 | tf_op jit(solution)/shard_map/all_to_all | solution.py:453
  29.8 2.4 %collective-permute-start.10 = (bf16[96,2048]{1,0:T(8,128)(2,1)S(1)}, bf16[96,2048]{1,0:T(8,128)(2,1)}, u32[]{:S(2)}, u32[]{:S(2)}) collective-permute-start(bf16[96,2048]{1,0:T(8,128)(2,1)S(1)} %pad_maximum_fusion.1), channel_id=1, source_target_pairs={{0,1},{1,0},{2,3},{3,2},{4,5},{5,4},{6,7},{7,6},{8,9},{9,8},{10,11... | collective-permute-start | bytes 1179656 | tf_op jit(solution)/shard_map/ppermute | solution.py:522
  32.2 0.3 collective-permute-start.3
  32.5 0.7 fusion
  33.2 16.8 %all-to-all-done.1.parts = bf16[16,16,3072]{2,1,0:T(8,128)(2,1)S(1)} async-done(((bf16[16,16,3072]{2,1,0:T(8,128)(2,1)}), bf16[16,16,3072]{2,1,0:T(8,128)(2,1)S(1)}, u32[]{:S(2)}, u32[]{:S(2)}) %all-to-all-start.1) | async-done | bytes 1572896 | tf_op jit(solution)/shard_map/all_to_all | solution.py:453
  50.0 1.1 copy-done.4
  51.2 5.8 %recall.1 = (bf16[16,16,768]{2,1,0:T(8,128)(2,1)}, f32[16,8,128]{2,1,0:T(8,128)}, f32[16,8,128]{2,1,0:T(8,128)}) custom-call(bf16[16,16,3072]{2,1,0:T(8,128)(2,1)} %copy-done.4, f32[16,128]{1,0:T(8,128)} %get-tuple-element.97.cosine_ref, f32[16,128]{1,0:T(8,128)} %get-tuple-element.96.sine_ref, bf16[768]{0:T(1024)(128)(2,1)} %gain.4, ...), custom_call_target="tpu_custom_call" | custom-call | tf_op jit(solution)/shard_map/recall/pallas_call | solution.py:202
  57.0 5.4 %all-to-all-start.2 = ((bf16[16,16,768]{2,1,0:T(8,128)(2,1)}), bf16[16,16,768]{2,1,0:T(8,128)(2,1)S(1)}, u32[]{:S(2)}, u32[]{:S(2)}) async-start(bf16[16,16,768]{2,1,0:T(8,128)(2,1)} %get-tuple-element.52), calls=%async_computation.2 | async-start | bytes 786432 | tf_op jit(solution)/shard_map/all_to_all | solution.py:453
  62.3 0.0 copy-start.2
  62.3 0.0 copy-start.3
  62.4 0.3 collective-permute-start.4
  62.7 2.5 %collective-permute-start.5 = (bf16[32,768]{1,0:T(8,128)(2,1)S(1)}, bf16[32,768]{1,0:T(8,128)(2,1)S(1)}, u32[]{:S(2)}, u32[]{:S(2)}) collective-permute-start(bf16[32,768]{1,0:T(8,128)(2,1)S(1)} %bitcast.7), channel_id=1, source_target_pairs={{0,6},{2,0},{4,2},{6,4},{1,7},{3,1},{5,3},{7,5},{8,14},{10,8},{12,... | collective-permute-start | bytes 147464 | tf_op jit(solution)/shard_map/ppermute | solution.py:32
  65.1 1.0 pad_maximum_fusion.c0
  66.2 0.7 collective-permute-done.4.c2
  66.9 0.4 collective-permute-start.11
  67.3 1.8 %collective-permute-start.12 = (bf16[192,2048]{1,0:T(8,128)(2,1)S(1)}, bf16[192,2048]{1,0:T(8,128)(2,1)S(1)}, u32[]{:S(2)}, u32[]{:S(2)}) collective-permute-start(bf16[192,2048]{1,0:T(8,128)(2,1)S(1)} %pad_maximum_fusion.c0), channel_id=1, source_target_pairs={{0,4},{2,6},{4,0},{6,2},{1,5},{3,7},{5,1},{7,3},{8,12},{10,14},{12... | collective-permute-start | bytes 2359304 | tf_op jit(solution)/shard_map/ppermute | solution.py:31
  69.1 0.8 collective-permute-start.13
  69.9 0.7 all-to-all-done.2.kept
  70.7 0.3 mix.1
  71.0 3.4 %collective-permute-start.9 = (bf16[16,8,128]{2,1,0:T(8,128)(2,1)S(1)}, bf16[16,8,128]{2,1,0:T(8,128)(2,1)S(1)}, u32[]{:S(2)}, u32[]{:S(2)}) collective-permute-start(bf16[16,8,128]{2,1,0:T(8,128)(2,1)S(1)} %get-tuple-element.59), channel_id=1, source_target_pairs={{0,1},{1,0},{2,3},{3,2},{4,5},{5,4},{6,7},{7,6},{8,9},{9,8},{10,11... | collective-permute-start | bytes 98312 | tf_op jit(solution)/shard_map/ppermute | solution.py:531
  74.4 0.9 collective-permute-done.9.other
  75.3 0.8 settle.1
  76.1 6.6 %all-to-all-start.3 = ((bf16[16,128,128]{2,1,0:T(8,128)(2,1)}), bf16[16,128,128]{2,1,0:T(8,128)(2,1)S(1)}, u32[]{:S(2)}, u32[]{:S(2)}) async-start(bf16[16,128,128]{2,1,0:T(8,128)(2,1)} %settle.1), calls=%async_computation.3 | async-start | bytes 1048576 | tf_op jit(solution)/shard_map/all_to_all | solution.py:453
  82.7 0.2 routing.1
  82.9 0.9 collective-permute-done.11.c1
  83.7 17.2 %collective-permute-done.12.c2 = bf16[192,2048]{1,0:T(8,128)(2,1)S(1)} collective-permute-done((bf16[192,2048]{1,0:T(8,128)(2,1)S(1)}, bf16[192,2048]{1,0:T(8,128)(2,1)S(1)}, u32[]{:S(2)}, u32[]{:S(2)}) %collective-permute-start.12) | collective-permute-done | bytes 786464 | tf_op jit(solution)/shard_map/ppermute | solution.py:31
  101.0 3.0 %collective-permute-done.13.c3 = bf16[192,2048]{1,0:T(8,128)(2,1)} collective-permute-done((bf16[192,2048]{1,0:T(8,128)(2,1)S(1)}, bf16[192,2048]{1,0:T(8,128)(2,1)}, u32[]{:S(2)}, u32[]{:S(2)}) %collective-permute-start.13) | collective-permute-done | bytes 786464 | tf_op jit(solution)/shard_map/ppermute | solution.py:32
  104.0 0.6 spread.1
  104.6 1.5 collective-permute-start.14
  106.2 3.3 %collective-permute-start.15 = (bf16[32,2048]{1,0:T(8,128)(2,1)S(1)}, bf16[32,2048]{1,0:T(8,128)(2,1)S(1)}, u32[]{:S(2)}, u32[]{:S(2)}) collective-permute-start(bf16[32,2048]{1,0:T(8,128)(2,1)S(1)} %get-tuple-element.77), channel_id=1, source_target_pairs={{0,4},{2,6},{4,0},{6,2},{1,5},{3,7},{5,1},{7,3},{8,12},{10,14},{12... | collective-permute-start | bytes 393224 | tf_op jit(solution)/shard_map/ppermute | solution.py:540
  109.4 4.7 %hoist.1 = (bf16[1,2048,512]{2,1,0:T(8,128)(2,1)S(1)}, bf16[1,2048,512]{2,1,0:T(8,128)(2,1)S(1)}, bf16[1,2048,512]{2,1,0:T(8,128)(2,1)S(1)}, bf16[1,2048,512]{2,...) custom-call(bf16[1,2048,512]{2,1,0:T(8,128)(2,1)} %refs_0_.1, ...), custom_call_target="tpu_custom_call" | custom-call | tf_op jit(solution)/shard_map/hoist/pallas_call | solution.py:441
  114.1 1.2 collective-permute-done.15.a2
  115.3 1.9 %experts.1 = (bf16[32,2048]{1,0:T(8,128)(2,1)S(1)}, bf16[32,2048]{1,0:T(8,128)(2,1)S(1)}, bf16[32,2048]{1,0:T(8,128)(2,1)S(1)}, bf16[32,2048]{1,0:T(8,128)(2,1)S(1)}) custom-call(bf16[32,2048]{1,0:T(8,128)(2,1)S(1)} %get-tuple-element.75.a0, bf16[32,2048]{1,0:T(8,128)(2,1)S(1)} %collective-permute-done.14.a1, ...), custom_call_target="tpu_custom_call" | custom-call | tf_op jit(solution)/shard_map/experts/pallas_call | solution.py:394
  117.3 2.8 %collective-permute-start.17 = (bf16[32,2048]{1,0:T(8,128)(2,1)S(1)}, bf16[32,2048]{1,0:T(8,128)(2,1)S(1)}, u32[]{:S(2)}, u32[]{:S(2)}) collective-permute-start(bf16[32,2048]{1,0:T(8,128)(2,1)S(1)} %get-tuple-element.89), channel_id=1, source_target_pairs={{0,6},{2,0},{4,2},{6,4},{1,7},{3,1},{5,3},{7,5},{8,14},{10,8},{12,... | collective-permute-start | bytes 393224 | tf_op jit(solution)/shard_map/ppermute | solution.py:549
  120.1 0.7 collective-permute-start.19
  120.7 2.0 %dense_first.1 = (bf16[128,256]{1,0:T(8,128)(2,1)S(1)}, bf16[256,2048]{1,0:T(8,128)(2,1)S(1)}) custom-call(bf16[128,2048]{1,0:T(8,128)(2,1)S(1)} %get-tuple-element.66.plane, bf16[192,2048]{1,0:T(8,128)(2,1)S(1)} %pad_maximum_fusion.c0, bf16[192,2048]{1,0:T(8,128)(2,1)S(1)} %collective-permute-done.11.c1, bf16[192,2048]{1,0:T(8,128)(2,1)S(1)} %collective-permute-done.12.c2, ...), custom_call_target="tpu_custom_call" | custom-call | tf_op jit(solution)/shard_map/dense_first/pallas_call | solution.py:362
  122.8 2.6 %collective-permute-done.17.b1 = bf16[32,2048]{1,0:T(8,128)(2,1)S(1)} collective-permute-done((bf16[32,2048]{1,0:T(8,128)(2,1)S(1)}, bf16[32,2048]{1,0:T(8,128)(2,1)S(1)}, u32[]{:S(2)}, u32[]{:S(2)}) %collective-permute-start.17) | collective-permute-done | bytes 131104 | tf_op jit(solution)/shard_map/ppermute | solution.py:549
  125.4 0.6 collective-permute-done.18.b2
  125.9 3.3 %collective-permute-done.19.b3 = bf16[32,2048]{1,0:T(8,128)(2,1)S(1)} collective-permute-done((bf16[32,2048]{1,0:T(8,128)(2,1)S(1)}, bf16[32,2048]{1,0:T(8,128)(2,1)S(1)}, u32[]{:S(2)}, u32[]{:S(2)}) %collective-permute-start.19) | collective-permute-done | bytes 131104 | tf_op jit(solution)/shard_map/ppermute | solution.py:551
  129.2 0.5 combine.1
  129.7 17.2 %all_to_all.25 = bf16[16,8,2048]{2,1,0:T(8,128)(2,1)S(1)} all-to-all(bf16[16,8,2048]{2,1,0:T(8,128)(2,1)S(1)} %combine.1), channel_id=1, replica_groups=mesh['z'=4,'y'=4,'x'=4,'tp'=2] {'z','y'}, dimensions={0} | all-to-all | bytes 1048576 | tf_op jit(solution)/shard_map/all_to_all | solution.py:453
  146.8 0.1 convert_reduce_fusion
  146.9 2.0 %collective-permute-start.20 = (bf16[8,2048]{1,0:T(8,128)(2,1)S(1)}, bf16[8,2048]{1,0:T(8,128)(2,1)S(1)}, u32[]{:S(2)}, u32[]{:S(2)}) collective-permute-start(bf16[8,2048]{1,0:T(8,128)(2,1)S(1)} %add_convert_fusion), channel_id=1, source_target_pairs={{0,1},{1,0},{2,3},{3,2},{4,5},{5,4},{6,7},{7,6},{8,9},{9,8},{10,11... | collective-permute-start | bytes 98312 | tf_op jit(solution)/shard_map/ppermute | solution.py:557
  148.9 5.5 %renew.1 = f32[16,6,128,128]{3,2,1,0:T(8,128)} custom-call(f32[16,8,128]{2,1,0:T(8,128)} %get-tuple-element.92.keys, f32[16,8,128]{2,1,0:T(8,128)} %get-tuple-element.93.values, f32[16,6,128,128]{3,2,1,0:T(8,128)} %state_ref.3), custom_call_target="tpu_custom_call" | custom-call | tf_op jit(solution)/shard_map/renew/pallas_call | solution.py:255
  154.4 0.6 pad_maximum_fusion.2
  (29 shorter events, 0.1 us)
Async XLA Ops:
  0.6 68.5 %collective-permute-start.6 = (bf16[1,2048,512]{2,1,0:T(8,128)(2,1)}, bf16[1,2048,512]{2,1,0:T(8,128)(2,1)}, u32[]{:S(2)}, u32[]{:S(2)}) collective-permute-start(bf16[1,2048,512]{2,1,0:T(8,128)(2,1)} %refs_0_.1), channel_id=1, source_target_pairs={{0,1},{1,0},{2,3},{3,2},{4,5},{5,4},{6,7},{7,6},{8,9},{9,8},{10,11... | collective-permute-start | bytes 6291464 | tf_op jit(solution)/shard_map/ppermute | solution.py:525
  3.8 13.9 %collective-permute-start = (bf16[4,32,768]{2,1,0:T(8,128)(2,1)}, bf16[4,32,768]{2,1,0:T(8,128)(2,1)S(1)}, u32[]{:S(2)}, u32[]{:S(2)}) collective-permute-start(bf16[4,32,768]{2,1,0:T(8,128)(2,1)} %get-tuple-element.49.c0), channel_id=1, source_target_pairs={{0,2},{2,4},{4,6},{6,0},{1,3},{3,5},{5,7},{7,1},{8,10},{10,12},{12... | collective-permute-start | bytes 589832 | tf_op jit(solution)/shard_map/ppermute | solution.py:30
  5.1 18.2 %collective-permute-start.1 = (bf16[4,32,768]{2,1,0:T(8,128)(2,1)}, bf16[4,32,768]{2,1,0:T(8,128)(2,1)S(1)}, u32[]{:S(2)}, u32[]{:S(2)}) collective-permute-start(bf16[4,32,768]{2,1,0:T(8,128)(2,1)} %get-tuple-element.49.c0), channel_id=1, source_target_pairs={{0,4},{2,6},{4,0},{6,2},{1,5},{3,7},{5,1},{7,3},{8,12},{10,14},{12... | collective-permute-start | bytes 589832 | tf_op jit(solution)/shard_map/ppermute | solution.py:31
  7.6 15.8 %collective-permute-start.2 = (bf16[4,32,768]{2,1,0:T(8,128)(2,1)}, bf16[4,32,768]{2,1,0:T(8,128)(2,1)S(1)}, u32[]{:S(2)}, u32[]{:S(2)}) collective-permute-start(bf16[4,32,768]{2,1,0:T(8,128)(2,1)} %get-tuple-element.49.c0), channel_id=1, source_target_pairs={{0,6},{2,0},{4,2},{6,4},{1,7},{3,1},{5,3},{7,5},{8,14},{10,8},{12,... | collective-permute-start | bytes 589832 | tf_op jit(solution)/shard_map/ppermute | solution.py:32
  8.7 14.6 %all-to-all-start = ((bf16[16,32,128]{2,1,0:T(8,128)(2,1)}), bf16[16,32,128]{2,1,0:T(8,128)(2,1)S(1)}, u32[]{:S(2)}, u32[]{:S(2)}) async-start(bf16[16,32,128]{2,1,0:T(8,128)(2,1)} %get-tuple-element.48), calls=%async_computation | async-start | bytes 262144 | tf_op jit(solution)/shard_map/all_to_all | solution.py:453
  16.5 54.1 %collective-permute-start.7 = (bf16[1,2048,512]{2,1,0:T(8,128)(2,1)}, bf16[1,2048,512]{2,1,0:T(8,128)(2,1)}, u32[]{:S(2)}, u32[]{:S(2)}) collective-permute-start(bf16[1,2048,512]{2,1,0:T(8,128)(2,1)} %refs_2_.1), channel_id=1, source_target_pairs={{0,1},{1,0},{2,3},{3,2},{4,5},{5,4},{6,7},{7,6},{8,9},{9,8},{10,11... | collective-permute-start | bytes 6291464 | tf_op jit(solution)/shard_map/ppermute | solution.py:525
  17.7 52.9 %collective-permute-start.8 = (bf16[1,512,2048]{2,1,0:T(8,128)(2,1)}, bf16[1,512,2048]{2,1,0:T(8,128)(2,1)}, u32[]{:S(2)}, u32[]{:S(2)}) collective-permute-start(bf16[1,512,2048]{2,1,0:T(8,128)(2,1)} %refs_4_.1), channel_id=1, source_target_pairs={{0,1},{1,0},{2,3},{3,2},{4,5},{5,4},{6,7},{7,6},{8,9},{9,8},{10,11... | collective-permute-start | bytes 6291464 | tf_op jit(solution)/shard_map/ppermute | solution.py:525
  23.4 0.9 copy-start
  25.8 3.9 %copy-start.5 = (bf16[32,2048]{1,0:T(8,128)(2,1)S(1)}, bf16[32,2048]{1,0:T(8,128)(2,1)}, u32[]{:S(2)}) copy-start(bf16[32,2048]{1,0:T(8,128)(2,1)} %param.40) | copy-start | bytes 393220
  25.8 3.9 %copy-start.6 = (bf16[2048,32]{0,1:T(8,128)(2,1)S(1)}, bf16[2048,32]{0,1:T(8,128)(2,1)}, u32[]{:S(2)}) copy-start(bf16[2048,32]{0,1:T(8,128)(2,1)} %param.39) | copy-start | bytes 393220
  25.8 3.9 %copy-start.7 = (bf16[2048,32]{0,1:T(8,128)(2,1)S(1)}, bf16[2048,32]{0,1:T(8,128)(2,1)}, u32[]{:S(2)}) copy-start(bf16[2048,32]{0,1:T(8,128)(2,1)} %param.38) | copy-start | bytes 393220
  25.8 6.3 %copy-start.1 = (bf16[768,32]{0,1:T(8,128)(2,1)S(1)}, bf16[768,32]{0,1:T(8,128)(2,1)}, u32[]{:S(2)}) copy-start(bf16[768,32]{0,1:T(8,128)(2,1)} %param.31) | copy-start | bytes 147460
  25.8 6.6 %copy-start.10 = (s32[16]{0:T(128)S(1)}, s32[16]{0:T(128)}, u32[]{:S(2)}) copy-start(s32[16]{0:T(128)} %param.23) | copy-start | bytes 196
  25.8 6.6 %copy-start.8 = (f32[128]{0:T(128)S(1)}, f32[128]{0:T(128)}, u32[]{:S(2)}) copy-start(f32[128]{0:T(128)} %constant.30) | copy-start | bytes 1540
  25.8 6.6 %copy-start.9 = (f32[128]{0:T(128)S(1)}, f32[128]{0:T(128)}, u32[]{:S(2)}) copy-start(f32[128]{0:T(128)} %constant.31) | copy-start | bytes 1540
  25.9 24.2 %all-to-all-start.1 = ((bf16[16,16,3072]{2,1,0:T(8,128)(2,1)}), bf16[16,16,3072]{2,1,0:T(8,128)(2,1)S(1)}, u32[]{:S(2)}, u32[]{:S(2)}) async-start(bf16[16,16,3072]{2,1,0:T(8,128)(2,1)} %project.1), calls=%async_computation.1 | async-start | bytes 3145728 | tf_op jit(solution)/shard_map/all_to_all | solution.py:453
  29.8 32.9 %collective-permute-start.10 = (bf16[96,2048]{1,0:T(8,128)(2,1)S(1)}, bf16[96,2048]{1,0:T(8,128)(2,1)}, u32[]{:S(2)}, u32[]{:S(2)}) collective-permute-start(bf16[96,2048]{1,0:T(8,128)(2,1)S(1)} %pad_maximum_fusion.1), channel_id=1, source_target_pairs={{0,1},{1,0},{2,3},{3,2},{4,5},{5,4},{6,7},{7,6},{8,9},{9,8},{10,11... | collective-permute-start | bytes 1179656 | tf_op jit(solution)/shard_map/ppermute | solution.py:522
  32.2 30.2 %collective-permute-start.3 = (bf16[32,768]{1,0:T(8,128)(2,1)S(1)}, bf16[32,768]{1,0:T(8,128)(2,1)S(1)}, u32[]{:S(2)}, u32[]{:S(2)}) collective-permute-start(bf16[32,768]{1,0:T(8,128)(2,1)S(1)} %bitcast.5), channel_id=1, source_target_pairs={{0,2},{2,4},{4,6},{6,0},{1,3},{3,5},{5,7},{7,1},{8,10},{10,12},{12... | collective-permute-start | bytes 147464 | tf_op jit(solution)/shard_map/ppermute | solution.py:30
  50.0 1.1 copy-start.4
  57.0 13.7 %all-to-all-start.2 = ((bf16[16,16,768]{2,1,0:T(8,128)(2,1)}), bf16[16,16,768]{2,1,0:T(8,128)(2,1)S(1)}, u32[]{:S(2)}, u32[]{:S(2)}) async-start(bf16[16,16,768]{2,1,0:T(8,128)(2,1)} %get-tuple-element.52), calls=%async_computation.2 | async-start | bytes 786432 | tf_op jit(solution)/shard_map/all_to_all | solution.py:453
  62.3 41.7 %copy-start.2 = (bf16[2048]{0:T(1024)(128)(2,1)S(1)}, bf16[2048]{0:T(1024)(128)(2,1)}, u32[]{:S(2)}) copy-start(bf16[2048]{0:T(1024)(128)(2,1)} %gain.5) | copy-start | bytes 12292
  62.3 41.7 %copy-start.3 = (bf16[2048]{0:T(1024)(128)(2,1)S(1)}, bf16[2048]{0:T(1024)(128)(2,1)}, u32[]{:S(2)}) copy-start(bf16[2048]{0:T(1024)(128)(2,1)} %branch.1) | copy-start | bytes 12292
  62.4 4.5 %collective-permute-start.4 = (bf16[32,768]{1,0:T(8,128)(2,1)S(1)}, bf16[32,768]{1,0:T(8,128)(2,1)S(1)}, u32[]{:S(2)}, u32[]{:S(2)}) collective-permute-start(bf16[32,768]{1,0:T(8,128)(2,1)S(1)} %bitcast.6), channel_id=1, source_target_pairs={{0,4},{2,6},{4,0},{6,2},{1,5},{3,7},{5,1},{7,3},{8,12},{10,14},{12... | collective-permute-start | bytes 147464 | tf_op jit(solution)/shard_map/ppermute | solution.py:31
  62.7 4.6 %collective-permute-start.5 = (bf16[32,768]{1,0:T(8,128)(2,1)S(1)}, bf16[32,768]{1,0:T(8,128)(2,1)S(1)}, u32[]{:S(2)}, u32[]{:S(2)}) collective-permute-start(bf16[32,768]{1,0:T(8,128)(2,1)S(1)} %bitcast.7), channel_id=1, source_target_pairs={{0,6},{2,0},{4,2},{6,4},{1,7},{3,1},{5,3},{7,5},{8,14},{10,8},{12,... | collective-permute-start | bytes 147464 | tf_op jit(solution)/shard_map/ppermute | solution.py:32
  66.9 16.8 %collective-permute-start.11 = (bf16[192,2048]{1,0:T(8,128)(2,1)S(1)}, bf16[192,2048]{1,0:T(8,128)(2,1)S(1)}, u32[]{:S(2)}, u32[]{:S(2)}) collective-permute-start(bf16[192,2048]{1,0:T(8,128)(2,1)S(1)} %pad_maximum_fusion.c0), channel_id=1, source_target_pairs={{0,2},{2,4},{4,6},{6,0},{1,3},{3,5},{5,7},{7,1},{8,10},{10,12},{12... | collective-permute-start | bytes 2359304 | tf_op jit(solution)/shard_map/ppermute | solution.py:30
  67.3 33.7 %collective-permute-start.12 = (bf16[192,2048]{1,0:T(8,128)(2,1)S(1)}, bf16[192,2048]{1,0:T(8,128)(2,1)S(1)}, u32[]{:S(2)}, u32[]{:S(2)}) collective-permute-start(bf16[192,2048]{1,0:T(8,128)(2,1)S(1)} %pad_maximum_fusion.c0), channel_id=1, source_target_pairs={{0,4},{2,6},{4,0},{6,2},{1,5},{3,7},{5,1},{7,3},{8,12},{10,14},{12... | collective-permute-start | bytes 2359304 | tf_op jit(solution)/shard_map/ppermute | solution.py:31
  69.1 34.9 %collective-permute-start.13 = (bf16[192,2048]{1,0:T(8,128)(2,1)S(1)}, bf16[192,2048]{1,0:T(8,128)(2,1)}, u32[]{:S(2)}, u32[]{:S(2)}) collective-permute-start(bf16[192,2048]{1,0:T(8,128)(2,1)S(1)} %pad_maximum_fusion.c0), channel_id=1, source_target_pairs={{0,6},{2,0},{4,2},{6,4},{1,7},{3,1},{5,3},{7,5},{8,14},{10,8},{12,... | collective-permute-start | bytes 2359304 | tf_op jit(solution)/shard_map/ppermute | solution.py:32
  71.0 4.3 %collective-permute-start.9 = (bf16[16,8,128]{2,1,0:T(8,128)(2,1)S(1)}, bf16[16,8,128]{2,1,0:T(8,128)(2,1)S(1)}, u32[]{:S(2)}, u32[]{:S(2)}) collective-permute-start(bf16[16,8,128]{2,1,0:T(8,128)(2,1)S(1)} %get-tuple-element.59), channel_id=1, source_target_pairs={{0,1},{1,0},{2,3},{3,2},{4,5},{5,4},{6,7},{7,6},{8,9},{9,8},{10,11... | collective-permute-start | bytes 98312 | tf_op jit(solution)/shard_map/ppermute | solution.py:531
  76.1 27.9 %all-to-all-start.3 = ((bf16[16,128,128]{2,1,0:T(8,128)(2,1)}), bf16[16,128,128]{2,1,0:T(8,128)(2,1)S(1)}, u32[]{:S(2)}, u32[]{:S(2)}) async-start(bf16[16,128,128]{2,1,0:T(8,128)(2,1)} %settle.1), calls=%async_computation.3 | async-start | bytes 1048576 | tf_op jit(solution)/shard_map/all_to_all | solution.py:453
  104.6 9.5 %collective-permute-start.14 = (bf16[32,2048]{1,0:T(8,128)(2,1)S(1)}, bf16[32,2048]{1,0:T(8,128)(2,1)S(1)}, u32[]{:S(2)}, u32[]{:S(2)}) collective-permute-start(bf16[32,2048]{1,0:T(8,128)(2,1)S(1)} %get-tuple-element.76), channel_id=1, source_target_pairs={{0,2},{2,4},{4,6},{6,0},{1,3},{3,5},{5,7},{7,1},{8,10},{10,12},{12... | collective-permute-start | bytes 393224 | tf_op jit(solution)/shard_map/ppermute | solution.py:539
  106.2 9.2 %collective-permute-start.15 = (bf16[32,2048]{1,0:T(8,128)(2,1)S(1)}, bf16[32,2048]{1,0:T(8,128)(2,1)S(1)}, u32[]{:S(2)}, u32[]{:S(2)}) collective-permute-start(bf16[32,2048]{1,0:T(8,128)(2,1)S(1)} %get-tuple-element.77), channel_id=1, source_target_pairs={{0,4},{2,6},{4,0},{6,2},{1,5},{3,7},{5,1},{7,3},{8,12},{10,14},{12... | collective-permute-start | bytes 393224 | tf_op jit(solution)/shard_map/ppermute | solution.py:540
  109.4 5.9 %collective-permute-start.16 = (bf16[32,2048]{1,0:T(8,128)(2,1)S(1)}, bf16[32,2048]{1,0:T(8,128)(2,1)S(1)}, u32[]{:S(2)}, u32[]{:S(2)}) collective-permute-start(bf16[32,2048]{1,0:T(8,128)(2,1)S(1)} %get-tuple-element.78), channel_id=1, source_target_pairs={{0,6},{2,0},{4,2},{6,4},{1,7},{3,1},{5,3},{7,5},{8,14},{10,8},{12,... | collective-permute-start | bytes 393224 | tf_op jit(solution)/shard_map/ppermute | solution.py:541
  117.3 8.1 %collective-permute-start.17 = (bf16[32,2048]{1,0:T(8,128)(2,1)S(1)}, bf16[32,2048]{1,0:T(8,128)(2,1)S(1)}, u32[]{:S(2)}, u32[]{:S(2)}) collective-permute-start(bf16[32,2048]{1,0:T(8,128)(2,1)S(1)} %get-tuple-element.89), channel_id=1, source_target_pairs={{0,6},{2,0},{4,2},{6,4},{1,7},{3,1},{5,3},{7,5},{8,14},{10,8},{12,... | collective-permute-start | bytes 393224 | tf_op jit(solution)/shard_map/ppermute | solution.py:549
  120.1 5.9 %collective-permute-start.18 = (bf16[32,2048]{1,0:T(8,128)(2,1)S(1)}, bf16[32,2048]{1,0:T(8,128)(2,1)S(1)}, u32[]{:S(2)}, u32[]{:S(2)}) collective-permute-start(bf16[32,2048]{1,0:T(8,128)(2,1)S(1)} %get-tuple-element.90), channel_id=1, source_target_pairs={{0,4},{2,6},{4,0},{6,2},{1,5},{3,7},{5,1},{7,3},{8,12},{10,14},{12... | collective-permute-start | bytes 393224 | tf_op jit(solution)/shard_map/ppermute | solution.py:550
  120.1 9.1 %collective-permute-start.19 = (bf16[32,2048]{1,0:T(8,128)(2,1)S(1)}, bf16[32,2048]{1,0:T(8,128)(2,1)S(1)}, u32[]{:S(2)}, u32[]{:S(2)}) collective-permute-start(bf16[32,2048]{1,0:T(8,128)(2,1)S(1)} %get-tuple-element.91), channel_id=1, source_target_pairs={{0,2},{2,4},{4,6},{6,0},{1,3},{3,5},{5,7},{7,1},{8,10},{10,12},{12... | collective-permute-start | bytes 393224 | tf_op jit(solution)/shard_map/ppermute | solution.py:551
  146.9 7.5 %collective-permute-start.20 = (bf16[8,2048]{1,0:T(8,128)(2,1)S(1)}, bf16[8,2048]{1,0:T(8,128)(2,1)S(1)}, u32[]{:S(2)}, u32[]{:S(2)}) collective-permute-start(bf16[8,2048]{1,0:T(8,128)(2,1)S(1)} %add_convert_fusion), channel_id=1, source_target_pairs={{0,1},{1,0},{2,3},{3,2},{4,5},{5,4},{6,7},{7,6},{8,9},{9,8},{10,11... | collective-permute-start | bytes 98312 | tf_op jit(solution)/shard_map/ppermute | solution.py:557

commit v5 on v4

--- a/solution.py
+++ b/solution.py
@@ -427,9 +427,7 @@
     n = len(refs) // 2
     ins, outs, sems = refs[:n], refs[n : 2 * n], refs[2 * n]
     moves = [
-        pltpu.make_async_copy(a.at[0, half], b.at[0, half], sems.at[2 * i + j])
-        for i, (a, b) in enumerate(zip(ins, outs))
-        for j, half in enumerate((pl.ds(0, a.shape[1] // 2), pl.ds(a.shape[1] // 2, a.shape[1] // 2)))
+        pltpu.make_async_copy(a, b, sems.at[i]) for i, (a, b) in enumerate(zip(ins, outs))
     ]
     for m in moves:
         m.start()
@@ -443,7 +441,7 @@
         in_specs=[HBM] * len(arrays),
         out_specs=[VMEM] * len(arrays),
         out_shape=[jax.ShapeDtypeStruct(a.shape, a.dtype) for a in arrays],
-        scratch_shapes=[pltpu.SemaphoreType.DMA((2 * len(arrays),))],
+        scratch_shapes=[pltpu.SemaphoreType.DMA((len(arrays),))],
         compiler_params=pltpu.CompilerParams(vmem_limit_bytes=40 * 2**20),
         name="hoist",
     )(*arrays)

time: 156 us -> 156 us (level)
  no operation moved by 1% of the time
where the time goes in v5:
time: 156 us; the launch traced here: 155 us
  starting transfers between devices  53.4 us (34%)
  waiting for transfers between devices  53.4 us (34%)
  Pallas kernels  25.6 us (16%)
  blocking collectives  17.2 us (11%)
  other arithmetic  2.53 us (2%)
  local copies, waits for them, and re-layouts  2.13 us (1%)
    all_to_all x4, starting transfers between devices, plane_exchange(): return lax.all_to_all(array, PLANE, split_axis=0, concat_axis=0, tiled=True)  23.5 us
    all_to_all x4, waiting for transfers between devices, plane_exchange(): return lax.all_to_all(array, PLANE, split_axis=0, concat_axis=0, tiled=True)  23.1 us
    ppermute x3, waiting for transfers between devices, ring_gather(): lax.ppermute(own, 'x', ACROSS)  17.9 us
    all_to_all x1, blocking collectives, plane_exchange(): return lax.all_to_all(array, PLANE, split_axis=0, concat_axis=0, tiled=True)  17.2 us
    pallas_call x1, Pallas kernels, recall(): pl.pallas_call(recall_body, in_specs=[VMEM, HBM, HBM, VMEM, HBM], out_spe...  5.79 us
    pallas_call x1, Pallas kernels, renew(): pl.pallas_call(renew_body, in_specs=[VMEM, VMEM, HBM], out_specs=HBM, out...  5.52 us
    pallas_call x1, Pallas kernels, hoist(): pl.pallas_call(hoist_body, in_specs=[HBM] * len(arrays), out_specs=[VMEM]...  4.71 us
    ppermute x3, starting transfers between devices, ring_gather(): lax.ppermute(own, 'x', ACROSS)  4.54 us
  transfers between devices with their start and end apart: 25, of which 12 were waited for; matrix products, arithmetic and copies ran while one was open for 1% of the time, Pallas kernels for 15%

profile of v5, /device:TPU:1, one launch (start us, length us, event | category | flops | bytes accessed | tf_op | source)
XLA Modules:
  0.0 155.1 jit_solution(501146099527465866)
XLA Ops:
  0.6 1.5 collective-permute-start.6
  2.1 1.7 %prepare.1 = (bf16[16,32,128]{2,1,0:T(8,128)(2,1)}, bf16[4,32,768]{2,1,0:T(8,128)(2,1)}) custom-call(bf16[16,2048]{1,0:T(8,128)(2,1)} %x_ref.1, bf16[2048]{0:T(1024)(128)(2,1)} %gain.3, s32[4,16]{1,0:T(4,128)} %bitcast.13, bf16[4,16]{1,0:T(4,128)(2,1)} %bitcast.14, bf16[32,768]{1,0:T(8,128)(2,1)} %wq.1, bf16[32,768]{1,0:T(8,128)(2,1)} %wk.1, ...), custom_call_target="tpu_custom_call" | custom-call | tf_op jit(solution)/shard_map/prepare/pallas_call | solution.py:67
  3.8 1.3 collective-permute-start
  5.1 2.5 %collective-permute-start.1 = (bf16[4,32,768]{2,1,0:T(8,128)(2,1)}, bf16[4,32,768]{2,1,0:T(8,128)(2,1)S(1)}, u32[]{:S(2)}, u32[]{:S(2)}) collective-permute-start(bf16[4,32,768]{2,1,0:T(8,128)(2,1)} %get-tuple-element.49.c0), channel_id=1, source_target_pairs={{0,4},{2,6},{4,0},{6,2},{1,5},{3,7},{5,1},{7,3},{8,12},{10,14},{12... | collective-permute-start | bytes 589832 | tf_op jit(solution)/shard_map/ppermute | solution.py:31
  7.6 1.2 collective-permute-start.2
  8.7 7.8 %all-to-all-start = ((bf16[16,32,128]{2,1,0:T(8,128)(2,1)}), bf16[16,32,128]{2,1,0:T(8,128)(2,1)S(1)}, u32[]{:S(2)}, u32[]{:S(2)}) async-start(bf16[16,32,128]{2,1,0:T(8,128)(2,1)} %get-tuple-element.48), calls=%async_computation | async-start | bytes 262144 | tf_op jit(solution)/shard_map/all_to_all | solution.py:451
  16.5 1.2 collective-permute-start.7
  17.7 0.1 collective-permute-start.8
  17.8 5.5 %all-to-all-done.x_ref.got = bf16[16,32,128]{2,1,0:T(8,128)(2,1)S(1)} async-done(((bf16[16,32,128]{2,1,0:T(8,128)(2,1)}), bf16[16,32,128]{2,1,0:T(8,128)(2,1)S(1)}, u32[]{:S(2)}, u32[]{:S(2)}) %all-to-all-start) | async-done | bytes 131104 | tf_op jit(solution)/shard_map/all_to_all | solution.py:451
  23.3 0.0 collective-permute-done.1.c2
  23.4 0.9 copy-done
  24.3 1.5 project.1
  25.8 0.0 copy-start.5
  25.8 0.0 copy-start.6
  25.8 0.0 copy-start.7
  25.8 0.0 copy-start.1
  25.8 0.0 copy-start.10
  25.8 0.0 copy-start.8
  25.8 0.0 copy-start.9
  25.9 3.9 %all-to-all-start.1 = ((bf16[16,16,3072]{2,1,0:T(8,128)(2,1)}), bf16[16,16,3072]{2,1,0:T(8,128)(2,1)S(1)}, u32[]{:S(2)}, u32[]{:S(2)}) async-start(bf16[16,16,3072]{2,1,0:T(8,128)(2,1)} %project.1), calls=%async_computation.1 | async-start | bytes 3145728 | tf_op jit(solution)/shard_map/all_to_all | solution.py:451
  29.8 2.4 %collective-permute-start.10 = (bf16[96,2048]{1,0:T(8,128)(2,1)S(1)}, bf16[96,2048]{1,0:T(8,128)(2,1)}, u32[]{:S(2)}, u32[]{:S(2)}) collective-permute-start(bf16[96,2048]{1,0:T(8,128)(2,1)S(1)} %pad_maximum_fusion.1), channel_id=1, source_target_pairs={{0,1},{1,0},{2,3},{3,2},{4,5},{5,4},{6,7},{7,6},{8,9},{9,8},{10,11... | collective-permute-start | bytes 1179656 | tf_op jit(solution)/shard_map/ppermute | solution.py:520
  32.2 0.3 collective-permute-start.3
  32.5 0.7 fusion
  33.2 16.8 %all-to-all-done.1.parts = bf16[16,16,3072]{2,1,0:T(8,128)(2,1)S(1)} async-done(((bf16[16,16,3072]{2,1,0:T(8,128)(2,1)}), bf16[16,16,3072]{2,1,0:T(8,128)(2,1)S(1)}, u32[]{:S(2)}, u32[]{:S(2)}) %all-to-all-start.1) | async-done | bytes 1572896 | tf_op jit(solution)/shard_map/all_to_all | solution.py:451
  50.0 1.1 copy-done.4
  51.2 5.8 %recall.1 = (bf16[16,16,768]{2,1,0:T(8,128)(2,1)}, f32[16,8,128]{2,1,0:T(8,128)}, f32[16,8,128]{2,1,0:T(8,128)}) custom-call(bf16[16,16,3072]{2,1,0:T(8,128)(2,1)} %copy-done.4, f32[16,128]{1,0:T(8,128)} %get-tuple-element.97.cosine_ref, f32[16,128]{1,0:T(8,128)} %get-tuple-element.96.sine_ref, bf16[768]{0:T(1024)(128)(2,1)} %gain.4, ...), custom_call_target="tpu_custom_call" | custom-call | tf_op jit(solution)/shard_map/recall/pallas_call | solution.py:202
  57.0 5.4 %all-to-all-start.2 = ((bf16[16,16,768]{2,1,0:T(8,128)(2,1)}), bf16[16,16,768]{2,1,0:T(8,128)(2,1)S(1)}, u32[]{:S(2)}, u32[]{:S(2)}) async-start(bf16[16,16,768]{2,1,0:T(8,128)(2,1)} %get-tuple-element.52), calls=%async_computation.2 | async-start | bytes 786432 | tf_op jit(solution)/shard_map/all_to_all | solution.py:451
  62.3 0.0 copy-start.2
  62.3 0.0 copy-start.3
  62.4 0.3 collective-permute-start.4
  62.7 2.5 %collective-permute-start.5 = (bf16[32,768]{1,0:T(8,128)(2,1)S(1)}, bf16[32,768]{1,0:T(8,128)(2,1)S(1)}, u32[]{:S(2)}, u32[]{:S(2)}) collective-permute-start(bf16[32,768]{1,0:T(8,128)(2,1)S(1)} %bitcast.7), channel_id=1, source_target_pairs={{0,6},{2,0},{4,2},{6,4},{1,7},{3,1},{5,3},{7,5},{8,14},{10,8},{12,... | collective-permute-start | bytes 147464 | tf_op jit(solution)/shard_map/ppermute | solution.py:32
  65.1 1.0 pad_maximum_fusion.c0
  66.2 0.7 collective-permute-done.4.c2
  66.9 0.4 collective-permute-start.11
  67.3 1.8 %collective-permute-start.12 = (bf16[192,2048]{1,0:T(8,128)(2,1)S(1)}, bf16[192,2048]{1,0:T(8,128)(2,1)S(1)}, u32[]{:S(2)}, u32[]{:S(2)}) collective-permute-start(bf16[192,2048]{1,0:T(8,128)(2,1)S(1)} %pad_maximum_fusion.c0), channel_id=1, source_target_pairs={{0,4},{2,6},{4,0},{6,2},{1,5},{3,7},{5,1},{7,3},{8,12},{10,14},{12... | collective-permute-start | bytes 2359304 | tf_op jit(solution)/shard_map/ppermute | solution.py:31
  69.1 0.8 collective-permute-start.13
  69.9 0.7 all-to-all-done.2.kept
  70.7 0.3 mix.1
  71.0 3.4 %collective-permute-start.9 = (bf16[16,8,128]{2,1,0:T(8,128)(2,1)S(1)}, bf16[16,8,128]{2,1,0:T(8,128)(2,1)S(1)}, u32[]{:S(2)}, u32[]{:S(2)}) collective-permute-start(bf16[16,8,128]{2,1,0:T(8,128)(2,1)S(1)} %get-tuple-element.59), channel_id=1, source_target_pairs={{0,1},{1,0},{2,3},{3,2},{4,5},{5,4},{6,7},{7,6},{8,9},{9,8},{10,11... | collective-permute-start | bytes 98312 | tf_op jit(solution)/shard_map/ppermute | solution.py:529
  74.4 0.9 collective-permute-done.9.other
  75.3 0.8 settle.1
  76.1 6.6 %all-to-all-start.3 = ((bf16[16,128,128]{2,1,0:T(8,128)(2,1)}), bf16[16,128,128]{2,1,0:T(8,128)(2,1)S(1)}, u32[]{:S(2)}, u32[]{:S(2)}) async-start(bf16[16,128,128]{2,1,0:T(8,128)(2,1)} %settle.1), calls=%async_computation.3 | async-start | bytes 1048576 | tf_op jit(solution)/shard_map/all_to_all | solution.py:451
  82.7 0.2 routing.1
  82.9 0.9 collective-permute-done.11.c1
  83.7 17.2 %collective-permute-done.12.c2 = bf16[192,2048]{1,0:T(8,128)(2,1)S(1)} collective-permute-done((bf16[192,2048]{1,0:T(8,128)(2,1)S(1)}, bf16[192,2048]{1,0:T(8,128)(2,1)S(1)}, u32[]{:S(2)}, u32[]{:S(2)}) %collective-permute-start.12) | collective-permute-done | bytes 786464 | tf_op jit(solution)/shard_map/ppermute | solution.py:31
  101.0 3.0 %collective-permute-done.13.c3 = bf16[192,2048]{1,0:T(8,128)(2,1)} collective-permute-done((bf16[192,2048]{1,0:T(8,128)(2,1)S(1)}, bf16[192,2048]{1,0:T(8,128)(2,1)}, u32[]{:S(2)}, u32[]{:S(2)}) %collective-permute-start.13) | collective-permute-done | bytes 786464 | tf_op jit(solution)/shard_map/ppermute | solution.py:32
  104.0 0.6 spread.1
  104.6 1.5 collective-permute-start.14
  106.2 3.3 %collective-permute-start.15 = (bf16[32,2048]{1,0:T(8,128)(2,1)S(1)}, bf16[32,2048]{1,0:T(8,128)(2,1)S(1)}, u32[]{:S(2)}, u32[]{:S(2)}) collective-permute-start(bf16[32,2048]{1,0:T(8,128)(2,1)S(1)} %get-tuple-element.77), channel_id=1, source_target_pairs={{0,4},{2,6},{4,0},{6,2},{1,5},{3,7},{5,1},{7,3},{8,12},{10,14},{12... | collective-permute-start | bytes 393224 | tf_op jit(solution)/shard_map/ppermute | solution.py:538
  109.4 4.7 %hoist.1 = (bf16[1,2048,512]{2,1,0:T(8,128)(2,1)S(1)}, bf16[1,2048,512]{2,1,0:T(8,128)(2,1)S(1)}, bf16[1,2048,512]{2,1,0:T(8,128)(2,1)S(1)}, bf16[1,2048,512]{2,...) custom-call(bf16[1,2048,512]{2,1,0:T(8,128)(2,1)} %refs_0_.1, ...), custom_call_target="tpu_custom_call" | custom-call | tf_op jit(solution)/shard_map/hoist/pallas_call | solution.py:439
  114.2 1.2 collective-permute-done.15.a2
  115.3 1.9 %experts.1 = (bf16[32,2048]{1,0:T(8,128)(2,1)S(1)}, bf16[32,2048]{1,0:T(8,128)(2,1)S(1)}, bf16[32,2048]{1,0:T(8,128)(2,1)S(1)}, bf16[32,2048]{1,0:T(8,128)(2,1)S(1)}) custom-call(bf16[32,2048]{1,0:T(8,128)(2,1)S(1)} %get-tuple-element.75.a0, bf16[32,2048]{1,0:T(8,128)(2,1)S(1)} %collective-permute-done.14.a1, ...), custom_call_target="tpu_custom_call" | custom-call | tf_op jit(solution)/shard_map/experts/pallas_call | solution.py:394
  117.3 2.8 %collective-permute-start.17 = (bf16[32,2048]{1,0:T(8,128)(2,1)S(1)}, bf16[32,2048]{1,0:T(8,128)(2,1)S(1)}, u32[]{:S(2)}, u32[]{:S(2)}) collective-permute-start(bf16[32,2048]{1,0:T(8,128)(2,1)S(1)} %get-tuple-element.89), channel_id=1, source_target_pairs={{0,6},{2,0},{4,2},{6,4},{1,7},{3,1},{5,3},{7,5},{8,14},{10,8},{12,... | collective-permute-start | bytes 393224 | tf_op jit(solution)/shard_map/ppermute | solution.py:547
  120.1 0.7 collective-permute-start.19
  120.7 2.0 %dense_first.1 = (bf16[128,256]{1,0:T(8,128)(2,1)S(1)}, bf16[256,2048]{1,0:T(8,128)(2,1)S(1)}) custom-call(bf16[128,2048]{1,0:T(8,128)(2,1)S(1)} %get-tuple-element.66.plane, bf16[192,2048]{1,0:T(8,128)(2,1)S(1)} %pad_maximum_fusion.c0, bf16[192,2048]{1,0:T(8,128)(2,1)S(1)} %collective-permute-done.11.c1, bf16[192,2048]{1,0:T(8,128)(2,1)S(1)} %collective-permute-done.12.c2, ...), custom_call_target="tpu_custom_call" | custom-call | tf_op jit(solution)/shard_map/dense_first/pallas_call | solution.py:362
  122.8 2.6 %collective-permute-done.17.b1 = bf16[32,2048]{1,0:T(8,128)(2,1)S(1)} collective-permute-done((bf16[32,2048]{1,0:T(8,128)(2,1)S(1)}, bf16[32,2048]{1,0:T(8,128)(2,1)S(1)}, u32[]{:S(2)}, u32[]{:S(2)}) %collective-permute-start.17) | collective-permute-done | bytes 131104 | tf_op jit(solution)/shard_map/ppermute | solution.py:547
  125.4 0.6 collective-permute-done.18.b2
  125.9 3.3 %collective-permute-done.19.b3 = bf16[32,2048]{1,0:T(8,128)(2,1)S(1)} collective-permute-done((bf16[32,2048]{1,0:T(8,128)(2,1)S(1)}, bf16[32,2048]{1,0:T(8,128)(2,1)S(1)}, u32[]{:S(2)}, u32[]{:S(2)}) %collective-permute-start.19) | collective-permute-done | bytes 131104 | tf_op jit(solution)/shard_map/ppermute | solution.py:549
  129.2 0.5 combine.1
  129.7 17.2 %all_to_all.25 = bf16[16,8,2048]{2,1,0:T(8,128)(2,1)S(1)} all-to-all(bf16[16,8,2048]{2,1,0:T(8,128)(2,1)S(1)} %combine.1), channel_id=1, replica_groups=mesh['z'=4,'y'=4,'x'=4,'tp'=2] {'z','y'}, dimensions={0} | all-to-all | bytes 1048576 | tf_op jit(solution)/shard_map/all_to_all | solution.py:451
  146.8 0.1 convert_reduce_fusion
  146.9 2.0 %collective-permute-start.20 = (bf16[8,2048]{1,0:T(8,128)(2,1)S(1)}, bf16[8,2048]{1,0:T(8,128)(2,1)S(1)}, u32[]{:S(2)}, u32[]{:S(2)}) collective-permute-start(bf16[8,2048]{1,0:T(8,128)(2,1)S(1)} %add_convert_fusion), channel_id=1, source_target_pairs={{0,1},{1,0},{2,3},{3,2},{4,5},{5,4},{6,7},{7,6},{8,9},{9,8},{10,11... | collective-permute-start | bytes 98312 | tf_op jit(solution)/shard_map/ppermute | solution.py:555
  148.9 5.5 %renew.1 = f32[16,6,128,128]{3,2,1,0:T(8,128)} custom-call(f32[16,8,128]{2,1,0:T(8,128)} %get-tuple-element.92.keys, f32[16,8,128]{2,1,0:T(8,128)} %get-tuple-element.93.values, f32[16,6,128,128]{3,2,1,0:T(8,128)} %state_ref.3), custom_call_target="tpu_custom_call" | custom-call | tf_op jit(solution)/shard_map/renew/pallas_call | solution.py:255
  154.4 0.6 pad_maximum_fusion.2
  (29 shorter events, 0.1 us)
Async XLA Ops:
  0.6 68.5 %collective-permute-start.6 = (bf16[1,2048,512]{2,1,0:T(8,128)(2,1)}, bf16[1,2048,512]{2,1,0:T(8,128)(2,1)}, u32[]{:S(2)}, u32[]{:S(2)}) collective-permute-start(bf16[1,2048,512]{2,1,0:T(8,128)(2,1)} %refs_0_.1), channel_id=1, source_target_pairs={{0,1},{1,0},{2,3},{3,2},{4,5},{5,4},{6,7},{7,6},{8,9},{9,8},{10,11... | collective-permute-start | bytes 6291464 | tf_op jit(solution)/shard_map/ppermute | solution.py:523
  3.8 13.9 %collective-permute-start = (bf16[4,32,768]{2,1,0:T(8,128)(2,1)}, bf16[4,32,768]{2,1,0:T(8,128)(2,1)S(1)}, u32[]{:S(2)}, u32[]{:S(2)}) collective-permute-start(bf16[4,32,768]{2,1,0:T(8,128)(2,1)} %get-tuple-element.49.c0), channel_id=1, source_target_pairs={{0,2},{2,4},{4,6},{6,0},{1,3},{3,5},{5,7},{7,1},{8,10},{10,12},{12... | collective-permute-start | bytes 589832 | tf_op jit(solution)/shard_map/ppermute | solution.py:30
  5.1 18.2 %collective-permute-start.1 = (bf16[4,32,768]{2,1,0:T(8,128)(2,1)}, bf16[4,32,768]{2,1,0:T(8,128)(2,1)S(1)}, u32[]{:S(2)}, u32[]{:S(2)}) collective-permute-start(bf16[4,32,768]{2,1,0:T(8,128)(2,1)} %get-tuple-element.49.c0), channel_id=1, source_target_pairs={{0,4},{2,6},{4,0},{6,2},{1,5},{3,7},{5,1},{7,3},{8,12},{10,14},{12... | collective-permute-start | bytes 589832 | tf_op jit(solution)/shard_map/ppermute | solution.py:31
  7.6 15.8 %collective-permute-start.2 = (bf16[4,32,768]{2,1,0:T(8,128)(2,1)}, bf16[4,32,768]{2,1,0:T(8,128)(2,1)S(1)}, u32[]{:S(2)}, u32[]{:S(2)}) collective-permute-start(bf16[4,32,768]{2,1,0:T(8,128)(2,1)} %get-tuple-element.49.c0), channel_id=1, source_target_pairs={{0,6},{2,0},{4,2},{6,4},{1,7},{3,1},{5,3},{7,5},{8,14},{10,8},{12,... | collective-permute-start | bytes 589832 | tf_op jit(solution)/shard_map/ppermute | solution.py:32
  8.7 14.6 %all-to-all-start = ((bf16[16,32,128]{2,1,0:T(8,128)(2,1)}), bf16[16,32,128]{2,1,0:T(8,128)(2,1)S(1)}, u32[]{:S(2)}, u32[]{:S(2)}) async-start(bf16[16,32,128]{2,1,0:T(8,128)(2,1)} %get-tuple-element.48), calls=%async_computation | async-start | bytes 262144 | tf_op jit(solution)/shard_map/all_to_all | solution.py:451
  16.5 54.1 %collective-permute-start.7 = (bf16[1,2048,512]{2,1,0:T(8,128)(2,1)}, bf16[1,2048,512]{2,1,0:T(8,128)(2,1)}, u32[]{:S(2)}, u32[]{:S(2)}) collective-permute-start(bf16[1,2048,512]{2,1,0:T(8,128)(2,1)} %refs_2_.1), channel_id=1, source_target_pairs={{0,1},{1,0},{2,3},{3,2},{4,5},{5,4},{6,7},{7,6},{8,9},{9,8},{10,11... | collective-permute-start | bytes 6291464 | tf_op jit(solution)/shard_map/ppermute | solution.py:523
  17.7 52.9 %collective-permute-start.8 = (bf16[1,512,2048]{2,1,0:T(8,128)(2,1)}, bf16[1,512,2048]{2,1,0:T(8,128)(2,1)}, u32[]{:S(2)}, u32[]{:S(2)}) collective-permute-start(bf16[1,512,2048]{2,1,0:T(8,128)(2,1)} %refs_4_.1), channel_id=1, source_target_pairs={{0,1},{1,0},{2,3},{3,2},{4,5},{5,4},{6,7},{7,6},{8,9},{9,8},{10,11... | collective-permute-start | bytes 6291464 | tf_op jit(solution)/shard_map/ppermute | solution.py:523
  23.4 0.9 copy-start
  25.8 3.9 %copy-start.5 = (bf16[32,2048]{1,0:T(8,128)(2,1)S(1)}, bf16[32,2048]{1,0:T(8,128)(2,1)}, u32[]{:S(2)}) copy-start(bf16[32,2048]{1,0:T(8,128)(2,1)} %param.40) | copy-start | bytes 393220
  25.8 3.9 %copy-start.6 = (bf16[2048,32]{0,1:T(8,128)(2,1)S(1)}, bf16[2048,32]{0,1:T(8,128)(2,1)}, u32[]{:S(2)}) copy-start(bf16[2048,32]{0,1:T(8,128)(2,1)} %param.39) | copy-start | bytes 393220
  25.8 3.9 %copy-start.7 = (bf16[2048,32]{0,1:T(8,128)(2,1)S(1)}, bf16[2048,32]{0,1:T(8,128)(2,1)}, u32[]{:S(2)}) copy-start(bf16[2048,32]{0,1:T(8,128)(2,1)} %param.38) | copy-start | bytes 393220
  25.8 6.3 %copy-start.1 = (bf16[768,32]{0,1:T(8,128)(2,1)S(1)}, bf16[768,32]{0,1:T(8,128)(2,1)}, u32[]{:S(2)}) copy-start(bf16[768,32]{0,1:T(8,128)(2,1)} %param.31) | copy-start | bytes 147460
  25.8 6.6 %copy-start.10 = (s32[16]{0:T(128)S(1)}, s32[16]{0:T(128)}, u32[]{:S(2)}) copy-start(s32[16]{0:T(128)} %param.23) | copy-start | bytes 196
  25.8 6.6 %copy-start.8 = (f32[128]{0:T(128)S(1)}, f32[128]{0:T(128)}, u32[]{:S(2)}) copy-start(f32[128]{0:T(128)} %constant.30) | copy-start | bytes 1540
  25.8 6.6 %copy-start.9 = (f32[128]{0:T(128)S(1)}, f32[128]{0:T(128)}, u32[]{:S(2)}) copy-start(f32[128]{0:T(128)} %constant.31) | copy-start | bytes 1540
  25.9 24.2 %all-to-all-start.1 = ((bf16[16,16,3072]{2,1,0:T(8,128)(2,1)}), bf16[16,16,3072]{2,1,0:T(8,128)(2,1)S(1)}, u32[]{:S(2)}, u32[]{:S(2)}) async-start(bf16[16,16,3072]{2,1,0:T(8,128)(2,1)} %project.1), calls=%async_computation.1 | async-start | bytes 3145728 | tf_op jit(solution)/shard_map/all_to_all | solution.py:451
  29.8 32.9 %collective-permute-start.10 = (bf16[96,2048]{1,0:T(8,128)(2,1)S(1)}, bf16[96,2048]{1,0:T(8,128)(2,1)}, u32[]{:S(2)}, u32[]{:S(2)}) collective-permute-start(bf16[96,2048]{1,0:T(8,128)(2,1)S(1)} %pad_maximum_fusion.1), channel_id=1, source_target_pairs={{0,1},{1,0},{2,3},{3,2},{4,5},{5,4},{6,7},{7,6},{8,9},{9,8},{10,11... | collective-permute-start | bytes 1179656 | tf_op jit(solution)/shard_map/ppermute | solution.py:520
  32.2 30.2 %collective-permute-start.3 = (bf16[32,768]{1,0:T(8,128)(2,1)S(1)}, bf16[32,768]{1,0:T(8,128)(2,1)S(1)}, u32[]{:S(2)}, u32[]{:S(2)}) collective-permute-start(bf16[32,768]{1,0:T(8,128)(2,1)S(1)} %bitcast.5), channel_id=1, source_target_pairs={{0,2},{2,4},{4,6},{6,0},{1,3},{3,5},{5,7},{7,1},{8,10},{10,12},{12... | collective-permute-start | bytes 147464 | tf_op jit(solution)/shard_map/ppermute | solution.py:30
  50.0 1.1 copy-start.4
  57.0 13.7 %all-to-all-start.2 = ((bf16[16,16,768]{2,1,0:T(8,128)(2,1)}), bf16[16,16,768]{2,1,0:T(8,128)(2,1)S(1)}, u32[]{:S(2)}, u32[]{:S(2)}) async-start(bf16[16,16,768]{2,1,0:T(8,128)(2,1)} %get-tuple-element.52), calls=%async_computation.2 | async-start | bytes 786432 | tf_op jit(solution)/shard_map/all_to_all | solution.py:451
  62.3 41.7 %copy-start.2 = (bf16[2048]{0:T(1024)(128)(2,1)S(1)}, bf16[2048]{0:T(1024)(128)(2,1)}, u32[]{:S(2)}) copy-start(bf16[2048]{0:T(1024)(128)(2,1)} %gain.5) | copy-start | bytes 12292
  62.3 41.7 %copy-start.3 = (bf16[2048]{0:T(1024)(128)(2,1)S(1)}, bf16[2048]{0:T(1024)(128)(2,1)}, u32[]{:S(2)}) copy-start(bf16[2048]{0:T(1024)(128)(2,1)} %branch.1) | copy-start | bytes 12292
  62.4 4.5 %collective-permute-start.4 = (bf16[32,768]{1,0:T(8,128)(2,1)S(1)}, bf16[32,768]{1,0:T(8,128)(2,1)S(1)}, u32[]{:S(2)}, u32[]{:S(2)}) collective-permute-start(bf16[32,768]{1,0:T(8,128)(2,1)S(1)} %bitcast.6), channel_id=1, source_target_pairs={{0,4},{2,6},{4,0},{6,2},{1,5},{3,7},{5,1},{7,3},{8,12},{10,14},{12... | collective-permute-start | bytes 147464 | tf_op jit(solution)/shard_map/ppermute | solution.py:31
  62.7 4.6 %collective-permute-start.5 = (bf16[32,768]{1,0:T(8,128)(2,1)S(1)}, bf16[32,768]{1,0:T(8,128)(2,1)S(1)}, u32[]{:S(2)}, u32[]{:S(2)}) collective-permute-start(bf16[32,768]{1,0:T(8,128)(2,1)S(1)} %bitcast.7), channel_id=1, source_target_pairs={{0,6},{2,0},{4,2},{6,4},{1,7},{3,1},{5,3},{7,5},{8,14},{10,8},{12,... | collective-permute-start | bytes 147464 | tf_op jit(solution)/shard_map/ppermute | solution.py:32
  66.9 16.8 %collective-permute-start.11 = (bf16[192,2048]{1,0:T(8,128)(2,1)S(1)}, bf16[192,2048]{1,0:T(8,128)(2,1)S(1)}, u32[]{:S(2)}, u32[]{:S(2)}) collective-permute-start(bf16[192,2048]{1,0:T(8,128)(2,1)S(1)} %pad_maximum_fusion.c0), channel_id=1, source_target_pairs={{0,2},{2,4},{4,6},{6,0},{1,3},{3,5},{5,7},{7,1},{8,10},{10,12},{12... | collective-permute-start | bytes 2359304 | tf_op jit(solution)/shard_map/ppermute | solution.py:30
  67.3 33.7 %collective-permute-start.12 = (bf16[192,2048]{1,0:T(8,128)(2,1)S(1)}, bf16[192,2048]{1,0:T(8,128)(2,1)S(1)}, u32[]{:S(2)}, u32[]{:S(2)}) collective-permute-start(bf16[192,2048]{1,0:T(8,128)(2,1)S(1)} %pad_maximum_fusion.c0), channel_id=1, source_target_pairs={{0,4},{2,6},{4,0},{6,2},{1,5},{3,7},{5,1},{7,3},{8,12},{10,14},{12... | collective-permute-start | bytes 2359304 | tf_op jit(solution)/shard_map/ppermute | solution.py:31
  69.1 34.9 %collective-permute-start.13 = (bf16[192,2048]{1,0:T(8,128)(2,1)S(1)}, bf16[192,2048]{1,0:T(8,128)(2,1)}, u32[]{:S(2)}, u32[]{:S(2)}) collective-permute-start(bf16[192,2048]{1,0:T(8,128)(2,1)S(1)} %pad_maximum_fusion.c0), channel_id=1, source_target_pairs={{0,6},{2,0},{4,2},{6,4},{1,7},{3,1},{5,3},{7,5},{8,14},{10,8},{12,... | collective-permute-start | bytes 2359304 | tf_op jit(solution)/shard_map/ppermute | solution.py:32
  71.0 4.3 %collective-permute-start.9 = (bf16[16,8,128]{2,1,0:T(8,128)(2,1)S(1)}, bf16[16,8,128]{2,1,0:T(8,128)(2,1)S(1)}, u32[]{:S(2)}, u32[]{:S(2)}) collective-permute-start(bf16[16,8,128]{2,1,0:T(8,128)(2,1)S(1)} %get-tuple-element.59), channel_id=1, source_target_pairs={{0,1},{1,0},{2,3},{3,2},{4,5},{5,4},{6,7},{7,6},{8,9},{9,8},{10,11... | collective-permute-start | bytes 98312 | tf_op jit(solution)/shard_map/ppermute | solution.py:529
  76.1 27.9 %all-to-all-start.3 = ((bf16[16,128,128]{2,1,0:T(8,128)(2,1)}), bf16[16,128,128]{2,1,0:T(8,128)(2,1)S(1)}, u32[]{:S(2)}, u32[]{:S(2)}) async-start(bf16[16,128,128]{2,1,0:T(8,128)(2,1)} %settle.1), calls=%async_computation.3 | async-start | bytes 1048576 | tf_op jit(solution)/shard_map/all_to_all | solution.py:451
  104.6 9.5 %collective-permute-start.14 = (bf16[32,2048]{1,0:T(8,128)(2,1)S(1)}, bf16[32,2048]{1,0:T(8,128)(2,1)S(1)}, u32[]{:S(2)}, u32[]{:S(2)}) collective-permute-start(bf16[32,2048]{1,0:T(8,128)(2,1)S(1)} %get-tuple-element.76), channel_id=1, source_target_pairs={{0,2},{2,4},{4,6},{6,0},{1,3},{3,5},{5,7},{7,1},{8,10},{10,12},{12... | collective-permute-start | bytes 393224 | tf_op jit(solution)/shard_map/ppermute | solution.py:537
  106.2 9.2 %collective-permute-start.15 = (bf16[32,2048]{1,0:T(8,128)(2,1)S(1)}, bf16[32,2048]{1,0:T(8,128)(2,1)S(1)}, u32[]{:S(2)}, u32[]{:S(2)}) collective-permute-start(bf16[32,2048]{1,0:T(8,128)(2,1)S(1)} %get-tuple-element.77), channel_id=1, source_target_pairs={{0,4},{2,6},{4,0},{6,2},{1,5},{3,7},{5,1},{7,3},{8,12},{10,14},{12... | collective-permute-start | bytes 393224 | tf_op jit(solution)/shard_map/ppermute | solution.py:538
  109.4 5.9 %collective-permute-start.16 = (bf16[32,2048]{1,0:T(8,128)(2,1)S(1)}, bf16[32,2048]{1,0:T(8,128)(2,1)S(1)}, u32[]{:S(2)}, u32[]{:S(2)}) collective-permute-start(bf16[32,2048]{1,0:T(8,128)(2,1)S(1)} %get-tuple-element.78), channel_id=1, source_target_pairs={{0,6},{2,0},{4,2},{6,4},{1,7},{3,1},{5,3},{7,5},{8,14},{10,8},{12,... | collective-permute-start | bytes 393224 | tf_op jit(solution)/shard_map/ppermute | solution.py:539
  117.3 8.1 %collective-permute-start.17 = (bf16[32,2048]{1,0:T(8,128)(2,1)S(1)}, bf16[32,2048]{1,0:T(8,128)(2,1)S(1)}, u32[]{:S(2)}, u32[]{:S(2)}) collective-permute-start(bf16[32,2048]{1,0:T(8,128)(2,1)S(1)} %get-tuple-element.89), channel_id=1, source_target_pairs={{0,6},{2,0},{4,2},{6,4},{1,7},{3,1},{5,3},{7,5},{8,14},{10,8},{12,... | collective-permute-start | bytes 393224 | tf_op jit(solution)/shard_map/ppermute | solution.py:547
  120.1 5.9 %collective-permute-start.18 = (bf16[32,2048]{1,0:T(8,128)(2,1)S(1)}, bf16[32,2048]{1,0:T(8,128)(2,1)S(1)}, u32[]{:S(2)}, u32[]{:S(2)}) collective-permute-start(bf16[32,2048]{1,0:T(8,128)(2,1)S(1)} %get-tuple-element.90), channel_id=1, source_target_pairs={{0,4},{2,6},{4,0},{6,2},{1,5},{3,7},{5,1},{7,3},{8,12},{10,14},{12... | collective-permute-start | bytes 393224 | tf_op jit(solution)/shard_map/ppermute | solution.py:548
  120.1 9.1 %collective-permute-start.19 = (bf16[32,2048]{1,0:T(8,128)(2,1)S(1)}, bf16[32,2048]{1,0:T(8,128)(2,1)S(1)}, u32[]{:S(2)}, u32[]{:S(2)}) collective-permute-start(bf16[32,2048]{1,0:T(8,128)(2,1)S(1)} %get-tuple-element.91), channel_id=1, source_target_pairs={{0,2},{2,4},{4,6},{6,0},{1,3},{3,5},{5,7},{7,1},{8,10},{10,12},{12... | collective-permute-start | bytes 393224 | tf_op jit(solution)/shard_map/ppermute | solution.py:549
  146.9 7.5 %collective-permute-start.20 = (bf16[8,2048]{1,0:T(8,128)(2,1)S(1)}, bf16[8,2048]{1,0:T(8,128)(2,1)S(1)}, u32[]{:S(2)}, u32[]{:S(2)}) collective-permute-start(bf16[8,2048]{1,0:T(8,128)(2,1)S(1)} %add_convert_fusion), channel_id=1, source_target_pairs={{0,1},{1,0},{2,3},{3,2},{4,5},{5,4},{6,7},{7,6},{8,9},{9,8},{10,11... | collective-permute-start | bytes 98312 | tf_op jit(solution)/shard_map/ppermute | solution.py:555
